TPU v7x, 128 devices: a whole 4x4x4 slice. The times are simulated.
128 devices in a mesh: sp: 64 (over z, y, x), tp: 2 (over core).
Axes of the slice: x: 4, y: 4, z: 4, core: 2. Of those that a mesh axis runs over, the one named last changes fastest.
Arguments:
- stream_mid: bfloat16 [12288, 2048], P('sp'), may hold values from -6 to 6
- d_out: bfloat16 [12288, 2048], P('sp'), may hold values from -16 to 16
- route_ids: int32 [12288, 2], P('sp'), may hold values from 0 to 63, all different within a row; in each aligned block of 192 rows (0 to 191, 192 to 383, ...) at most 12 rows name the same one
- route_weights: float32 [12288, 2], P('sp'), may hold values from 0.3 to 1.5
- gate_pre: bfloat16 [12288, 2048], P('sp', 'tp'), may hold values from -6 to 6
- lru_out: bfloat16 [12288, 2048], P('sp', 'tp'), may hold values from -6 to 6
- log_decay: float32 [12288, 2048], P('sp', 'tp'), may hold values from -2.5 to 0
- w_out: bfloat16 [2048, 2048], P('tp'), may hold values from -0.125 to 0.125
- exp_gate: bfloat16 [64, 2048, 1024], P('sp', None, 'tp'), may hold values from -0.125 to 0.125
- exp_up: bfloat16 [64, 2048, 1024], P('sp', None, 'tp'), may hold values from -0.125 to 0.125
- exp_down: bfloat16 [64, 1024, 2048], P('sp', 'tp'), may hold values from -0.1875 to 0.1875
Outputs:
- grad_exp_gate: float32 [64, 2048, 1024], P('sp', None, 'tp')
- grad_exp_up: float32 [64, 2048, 1024], P('sp', None, 'tp')
- grad_exp_down: float32 [64, 1024, 2048], P('sp', 'tp')
- grad_out_proj: float32 [2048, 2048], P('sp', 'tp')
- d_gate: bfloat16 [12288, 2048], P('sp', 'tp')
- d_drive: float32 [12288, 2048], P('sp', 'tp')
- d_log_decay: float32 [12288, 2048], P('sp', 'tp')
Inputs may be any that keep to these rules, and one draw needn't show every extreme that they name: `route_ids`: each row names 2 different experts; among the rows of one index of sp no expert is named by more than 12 rows, and in every draw some expert is named by exactly 12 of them.
All inputs are finite; a program needn't handle non-finite values.
Results may differ from a plain program's by a relative error of at most 0.0069.
Values may be sent and summed in bfloat16 or wider, within the bound.
No kernel may reach another device: no remote copies, remote signals or barrier semaphores. Data moves between devices by JAX's collectives and lax.ppermute only.
A program may use at most 128 MiB of HBM per device.

v0:
```python
import functools

import jax
import jax.numpy as jnp
import numpy as np
from jax import lax
from jax.experimental import pallas as pl
from jax.experimental.pallas import tpu as pltpu
from jax.sharding import Mesh, PartitionSpec as P

BF = jnp.bfloat16
F32 = jnp.float32
SP = ("z", "y", "x")
TOK = 192
D = 2048
HALF = 1024
BLK = 256
CAP = 12
CHUNK = 24
NSP = 64
SLOTS = NSP * CHUNK
ROWS = NSP * CAP
FF = 512
GROUP = 8 * CHUNK

_perm = np.zeros((GROUP, GROUP), np.float32)
for _s in range(8):
    for _h in range(2):
        for _r in range(CAP):
            _perm[_h * 96 + _s * CAP + _r, _s * CHUNK + _h * CAP + _r] = 1.0


def dot(a, b):
    return lax.dot_general(a, b, (((1,), (0,)), ((), ())), preferred_element_type=F32)


def dot_cols(a, b):
    return lax.dot_general(a, b, (((1,), (1,)), ((), ())), preferred_element_type=F32)


def dot_rows(a, b):
    return lax.dot_general(a, b, (((0,), (0,)), ((), ())), preferred_element_type=F32)


def vm(mib):
    return pltpu.CompilerParams(vmem_limit_bytes=mib * 1024 * 1024)


def lanes(index, width=BLK):
    return pl.ds(pl.multiple_of(index * width, width), width)


def slot_columns(ids_ref):
    lane = lax.broadcasted_iota(jnp.int32, (TOK, NSP), 1)
    ids0, ids1 = ids_ref[:, 0:1], ids_ref[:, 1:2]
    hot0 = jnp.where(lane == ids0, 1.0, 0.0)
    hot1 = jnp.where(lane == ids1, 1.0, 0.0)
    row = lax.broadcasted_iota(jnp.int32, (TOK, TOK), 0)
    col = lax.broadcasted_iota(jnp.int32, (TOK, TOK), 1)
    before = jnp.where(col < row, 1.0, 0.0).astype(BF)
    rank0 = dot(before, hot0.astype(BF))
    rank1 = dot(before, hot1.astype(BF)) + jnp.sum(hot0, axis=0, keepdims=True)
    first0 = jnp.sum(hot0 * rank0, axis=1, keepdims=True)
    first1 = jnp.sum(hot1 * rank1, axis=1, keepdims=True)
    return ids0.astype(F32) * CHUNK + first0, ids1.astype(F32) * CHUNK + first1


def as_row(column):
    row = lax.broadcasted_iota(jnp.int32, (TOK, TOK), 0)
    col = lax.broadcasted_iota(jnp.int32, (TOK, TOK), 1)
    return jnp.sum(jnp.where(row == col, column, 0.0), axis=0, keepdims=True)


def pack_kernel(meta, ids_ref, w_ref, x_ref, d_ref, out_ref, sx, s0, s1):
    @pl.when(pl.program_id(0) == 0)
    def _():
        c0, c1 = slot_columns(ids_ref)
        r0, r1 = as_row(c0).astype(jnp.int32), as_row(c1).astype(jnp.int32)
        slot = lax.broadcasted_iota(jnp.int32, (SLOTS, TOK), 0)
        sx[...] = jnp.where((slot == r0) | (slot == r1), 1.0, 0.0).astype(BF)
        s0[...] = jnp.where(slot == r0 + CAP, 1.0, 0.0).astype(BF)
        s1[...] = jnp.where(slot == r1 + CAP, 1.0, 0.0).astype(BF)

    d = d_ref[...].astype(F32)
    scaled0 = (w_ref[:, 0:1] * d).astype(BF)
    scaled1 = (w_ref[:, 1:2] * d).astype(BF)
    out = dot(sx[...], x_ref[...]) + dot(s0[...], scaled0) + dot(s1[...], scaled1)
    out_ref[...] = out.astype(BF)


def pack(meta, ids, weights, stream, d_out):
    return pl.pallas_call(
        pack_kernel,
        name="pack",
        grid_spec=pltpu.PrefetchScalarGridSpec(
            num_scalar_prefetch=1,
            grid=(4,),
            in_specs=[
                pl.BlockSpec((TOK, 2), lambda j, m: (0, 0)),
                pl.BlockSpec((TOK, 2), lambda j, m: (0, 0)),
                pl.BlockSpec((TOK, BLK), lambda j, m: (0, 2 * j + m[0])),
                pl.BlockSpec((TOK, BLK), lambda j, m: (0, 2 * j + m[0])),
            ],
            out_specs=pl.BlockSpec((SLOTS, BLK), lambda j, m: (0, j)),
            scratch_shapes=[pltpu.VMEM((SLOTS, TOK), BF)] * 3,
        ),
        out_shape=jax.ShapeDtypeStruct((SLOTS, HALF), BF),
        compiler_params=vm(24),
    )(meta, ids, weights, stream, d_out)


def expert_kernel(
    meta, perm_ref, own_ref, peer_ref, wg_ref, wu_ref, wd_ref,
    hid_ref, gg_ref, gu_ref, pown_ref, ppeer_ref, xs, cs, ys,
):
    tp = meta[0]
    perm = perm_ref[...]
    for src, par in ((own_ref, tp), (peer_ref, 1 - tp)):
        for g in range(2):
            moved = dot(perm, src[g * GROUP : (g + 1) * GROUP, :]).astype(BF)
            for j in range(4):
                part = lanes(2 * j + par)
                xs[g * 96 : (g + 1) * 96, part] = moved[:96, j * BLK : (j + 1) * BLK]
                cs[g * 96 : (g + 1) * 96, part] = moved[96:, j * BLK : (j + 1) * BLK]
    x = xs[...]
    gate = dot(x, wg_ref[...])
    up = dot(x, wu_ref[...])
    back = dot_cols(cs[...], wd_ref[...])
    sig = jax.nn.sigmoid(gate)
    act = gate * sig
    hid_ref[...] = (act * up).astype(BF)
    gg = (back * up * sig * (1.0 + gate * (1.0 - sig))).astype(BF)
    gu = (back * act).astype(BF)
    gg_ref[...] = gg
    gu_ref[...] = gu
    ys[...] = (dot_cols(gg, wg_ref[...]) + dot_cols(gu, wu_ref[...])).astype(BF)
    for dst, par in ((pown_ref, tp), (ppeer_ref, 1 - tp)):
        for g in range(2):
            r = slice(g * 96, (g + 1) * 96)
            low = jnp.concatenate([ys[r, lanes(par)], ys[r, lanes(2 + par)]], axis=1)
            high = jnp.concatenate([ys[r, lanes(4 + par)], ys[r, lanes(6 + par)]], axis=1)
            both = jnp.concatenate([low, high], axis=0)
            dst[g * GROUP : (g + 1) * GROUP, :] = dot_rows(perm, both).astype(BF)


def expert(meta, perm, own, peer, wg, wu, wd):
    step = 2 * GROUP
    rows = 16 * CAP
    return pl.pallas_call(
        expert_kernel,
        name="expert",
        grid_spec=pltpu.PrefetchScalarGridSpec(
            num_scalar_prefetch=1,
            grid=(4,),
            in_specs=[
                pl.BlockSpec((GROUP, GROUP), lambda i, m: (0, 0)),
                pl.BlockSpec((step, HALF), lambda i, m: (i, 0)),
                pl.BlockSpec((step, HALF), lambda i, m: (i, 0)),
                pl.BlockSpec((D, FF), lambda i, m: (0, 0)),
                pl.BlockSpec((D, FF), lambda i, m: (0, 0)),
                pl.BlockSpec((FF, D), lambda i, m: (0, 0)),
            ],
            out_specs=[
                pl.BlockSpec((rows, FF), lambda i, m: (i, 0)),
                pl.BlockSpec((rows, FF), lambda i, m: (i, 0)),
                pl.BlockSpec((rows, FF), lambda i, m: (i, 0)),
                pl.BlockSpec((step, HALF // 2), lambda i, m: (i, 0)),
                pl.BlockSpec((step, HALF // 2), lambda i, m: (i, 0)),
            ],
            scratch_shapes=[pltpu.VMEM((rows, D), BF)] * 3,
        ),
        out_shape=[jax.ShapeDtypeStruct((ROWS, FF), BF)] * 3
        + [jax.ShapeDtypeStruct((SLOTS, HALF // 2), BF)] * 2,
        compiler_params=vm(40),
    )(meta, perm, own, peer, wg, wu, wd)


def weight_kernel(
    meta, perm_ref, own_ref, peer_ref, hid_ref, gg_ref, gu_ref, og_ref, ou_ref, od_ref, xs, cs
):
    h = pl.program_id(1)
    perm = perm_ref[...]
    for g in range(8):
        rows = slice(g * GROUP, (g + 1) * GROUP)
        src = jnp.where(h == 0, own_ref[rows, :], peer_ref[rows, :])
        moved = dot(perm, src).astype(BF)
        xs[g * 96 : (g + 1) * 96, :] = moved[:96]
        cs[g * 96 : (g + 1) * 96, :] = moved[96:]
    x = xs[...]
    og_ref[...] = dot_rows(x, gg_ref[...])
    ou_ref[...] = dot_rows(x, gu_ref[...])
    od_ref[...] = dot_rows(hid_ref[...], cs[...])


def weight_grads(meta, perm, own, peer, hid, gg, gu):
    block = lambda j, h, m: 2 * j + (h + m[0]) % 2
    return pl.pallas_call(
        weight_kernel,
        name="weight_grads",
        grid_spec=pltpu.PrefetchScalarGridSpec(
            num_scalar_prefetch=1,
            grid=(4, 2),
            in_specs=[
                pl.BlockSpec((GROUP, GROUP), lambda j, h, m: (0, 0)),
                pl.BlockSpec((SLOTS, BLK), lambda j, h, m: (0, j)),
                pl.BlockSpec((SLOTS, BLK), lambda j, h, m: (0, j)),
                pl.BlockSpec((ROWS, FF), lambda j, h, m: (0, 0)),
                pl.BlockSpec((ROWS, FF), lambda j, h, m: (0, 0)),
                pl.BlockSpec((ROWS, FF), lambda j, h, m: (0, 0)),
            ],
            out_specs=[
                pl.BlockSpec((BLK, FF), lambda j, h, m: (block(j, h, m), 0)),
                pl.BlockSpec((BLK, FF), lambda j, h, m: (block(j, h, m), 0)),
                pl.BlockSpec((FF, BLK), lambda j, h, m: (0, block(j, h, m))),
            ],
            scratch_shapes=[pltpu.VMEM((ROWS, BLK), BF)] * 2,
        ),
        out_shape=[
            jax.ShapeDtypeStruct((D, FF), F32),
            jax.ShapeDtypeStruct((D, FF), F32),
            jax.ShapeDtypeStruct((FF, D), F32),
        ],
        compiler_params=vm(32),
        cost_estimate=pl.CostEstimate(
            flops=3 * 2 * ROWS * D * FF, bytes_accessed=20_000_000, transcendentals=0
        ),
    )(meta, perm, own, peer, hid, gg, gu)


def combine_kernel(meta, ids_ref, ret_ref, d_ref, dm_ref, b0, b1, b2, b3):
    tp, z = meta[0], meta[1]
    c0, c1 = slot_columns(ids_ref)
    c0, c1 = c0.astype(jnp.int32), c1.astype(jnp.int32)
    slot = lax.broadcasted_iota(jnp.int32, (TOK, SLOTS), 1)
    for side in range(2):
        pick = (slot == c0 + side * CAP) | (slot == c1 + side * CAP)
        back = dot(jnp.where(pick, 1.0, 0.0).astype(BF), ret_ref[...])
        for k in range(2):
            j = 2 * side + k
            own = d_ref[:, lanes(2 * j + tp)].astype(F32)
            dm_ref[:, j * BLK : (j + 1) * BLK] = (own + back[:, k * BLK : (k + 1) * BLK]).astype(BF)
    for k, ref in enumerate((b0, b1, b2, b3)):
        ref[...] = dm_ref[:, lanes(lax.rem(z + k, 4))]


def combine(meta, ids, ret, d_out):
    full = lambda *shape: pl.BlockSpec(shape, lambda i, m: (0, 0))
    return pl.pallas_call(
        combine_kernel,
        name="combine",
        grid_spec=pltpu.PrefetchScalarGridSpec(
            num_scalar_prefetch=1,
            grid=(1,),
            in_specs=[full(TOK, 2), full(SLOTS, HALF // 2), full(TOK, D)],
            out_specs=[full(TOK, HALF)] + [full(TOK, BLK)] * 4,
        ),
        out_shape=[jax.ShapeDtypeStruct((TOK, HALF), BF)]
        + [jax.ShapeDtypeStruct((TOK, BLK), BF)] * 4,
        compiler_params=vm(24),
    )(meta, ids, ret, d_out)


ROOT = 0.7978845608028654
CUBE = 0.044715


def gelu_parts(x):
    t = jnp.tanh(ROOT * (x + CUBE * x * x * x))
    return 0.5 * x * (1.0 + t), t


def early_kernel(gate_ref, lru_ref, decay_ref, gated_ref, block_ref):
    value, _ = gelu_parts(gate_ref[...].astype(F32))
    gated_ref[...] = (value * lru_ref[...].astype(F32)).astype(BF)
    block_ref[...] = jnp.exp(jnp.sum(decay_ref[...], axis=0, keepdims=True))


def early(gate_pre, lru_out, log_decay):
    return pl.pallas_call(
        early_kernel,
        name="early",
        out_shape=[
            jax.ShapeDtypeStruct((TOK, HALF), BF),
            jax.ShapeDtypeStruct((1, HALF), F32),
        ],
        compiler_params=vm(16),
    )(gate_pre, lru_out, log_decay)


def scan_rows(drive_ref, decay_ref, start, visit):
    carry = start
    for tile in reversed(range(TOK // 8)):
        rows = slice(tile * 8, tile * 8 + 8)
        drive, rate = drive_ref[rows, :], decay_ref[rows, :]
        here, later = [None] * 8, [None] * 8
        for r in reversed(range(8)):
            here[r] = drive[r : r + 1] + carry
            carry = rate[r : r + 1] * here[r]
            later[r] = carry
        if visit is not None:
            visit(rows, jnp.concatenate(here, axis=0), jnp.concatenate(later, axis=0))
    return carry


def drive_kernel(
    meta, own_ref, peer_ref, w_ref, gate_ref, lru_ref, decay_ref,
    dgate_ref, drive_ref, head_ref, rate_ref,
):
    tp = meta[0]
    grad = jnp.zeros((TOK, HALF), F32)
    for ref, par in ((own_ref, tp), (peer_ref, 1 - tp)):
        for j in range(4):
            grad += dot_cols(ref[:, j * BLK : (j + 1) * BLK], w_ref[:, lanes(2 * j + par)])
    x = gate_ref[...].astype(F32)
    value, t = gelu_parts(x)
    slope = 0.5 * (1.0 + t) + 0.5 * x * (1.0 - t * t) * (ROOT * (1.0 + 3.0 * CUBE * x * x))
    dgate_ref[...] = (grad * lru_ref[...].astype(F32) * slope).astype(BF)
    drive_ref[...] = grad * value
    rate_ref[...] = jnp.exp(decay_ref[...])
    head_ref[...] = scan_rows(drive_ref, rate_ref, jnp.zeros((1, HALF), F32), None)


def drive(meta, own, peer, w_out, gate_pre, lru_out, log_decay):
    full = lambda *shape: pl.BlockSpec(shape, lambda i, m: (0, 0))
    return pl.pallas_call(
        drive_kernel,
        name="drive",
        grid_spec=pltpu.PrefetchScalarGridSpec(
            num_scalar_prefetch=1,
            grid=(1,),
            in_specs=[full(TOK, HALF), full(TOK, HALF), full(HALF, D)] + [full(TOK, HALF)] * 3,
            out_specs=[full(TOK, HALF), full(TOK, HALF), full(1, HALF)],
            scratch_shapes=[pltpu.VMEM((TOK, HALF), F32)],
        ),
        out_shape=[
            jax.ShapeDtypeStruct((TOK, HALF), BF),
            jax.ShapeDtypeStruct((TOK, HALF), F32),
            jax.ShapeDtypeStruct((1, HALF), F32),
        ],
        compiler_params=vm(32),
    )(meta, own, peer, w_out, gate_pre, lru_out, log_decay)


def finish_kernel(
    meta, links_ref, drive_ref, decay_ref, lru_ref, before_ref, dd_ref, dl_ref, rate_ref, prev_ref
):
    index = meta[2]
    carry = jnp.zeros((1, HALF), F32)
    for r in reversed(range(1, NSP)):
        head = links_ref[2 * r : 2 * r + 1, :]
        block = links_ref[2 * r + 1 : 2 * r + 2, :]
        carry = jnp.where(index < r, head + block * carry, carry)
    rate_ref[...] = jnp.exp(decay_ref[...])
    state = lru_ref[...].astype(F32)
    first = lax.broadcasted_iota(jnp.int32, (TOK, HALF), 0) == 0
    prev_ref[...] = jnp.where(first, before_ref[...].astype(F32), pltpu.roll(state, 1, 0))

    def visit(rows, here, later):
        dd_ref[rows, :] = here
        dl_ref[rows, :] = later * prev_ref[rows, :]

    scan_rows(drive_ref, rate_ref, carry, visit)


def finish(meta, links, drive_value, log_decay, lru_out, before):
    full = lambda *shape: pl.BlockSpec(shape, lambda i, m: (0, 0))
    return pl.pallas_call(
        finish_kernel,
        name="finish",
        grid_spec=pltpu.PrefetchScalarGridSpec(
            num_scalar_prefetch=1,
            grid=(1,),
            in_specs=[full(2 * NSP, HALF)] + [full(TOK, HALF)] * 3 + [full(1, HALF)],
            out_specs=[full(TOK, HALF)] * 2,
            scratch_shapes=[pltpu.VMEM((TOK, HALF), F32)] * 2,
        ),
        out_shape=[jax.ShapeDtypeStruct((TOK, HALF), F32)] * 2,
        compiler_params=vm(24),
    )(meta, links, drive_value, log_decay, lru_out, before)


def outer_kernel(meta, *refs):
    own, peer, gated, out_ref = refs[0:4], refs[4:8], refs[8:12], refs[12]
    tp, z = meta[0], meta[1]
    total_own = dot_rows(own[0][...], gated[0][...])
    total_peer = dot_rows(peer[0][:, lanes(z)], gated[0][...])
    for k in range(1, 4):
        total_own += dot_rows(own[k][...], gated[k][...])
        total_peer += dot_rows(peer[k][...], gated[k][...])
    out_ref[lanes(tp), :] = total_own.astype(BF)
    out_ref[lanes(1 - tp), :] = total_peer.astype(BF)


def outer(meta, own, peer, gated):
    full = lambda a: pl.BlockSpec(a.shape, lambda i, m: (0, 0))
    args = (*own, *peer, *gated)
    return pl.pallas_call(
        outer_kernel,
        name="outer",
        grid_spec=pltpu.PrefetchScalarGridSpec(
            num_scalar_prefetch=1,
            grid=(1,),
            in_specs=[full(a) for a in args],
            out_specs=pl.BlockSpec((2 * BLK, HALF), lambda i, m: (0, 0)),
        ),
        out_shape=jax.ShapeDtypeStruct((2 * BLK, HALF), BF),
        compiler_params=vm(24),
    )(meta, *args)


def swapped(value):
    return lax.ppermute(value, "tp", [(0, 1), (1, 0)])


def turned(value, steps):
    return lax.ppermute(value, "z", [(s, (s + steps) % 4) for s in range(4)])


def on_device(
    stream_mid, d_out, route_ids, route_weights, gate_pre, lru_out, log_decay, w_out,
    exp_gate, exp_up, exp_down,
):
    index = lax.axis_index(SP)
    meta = jnp.stack([lax.axis_index("tp"), lax.axis_index("z"), index]).astype(jnp.int32)
    perm = jnp.asarray(_perm, BF)
    gated, block = early(gate_pre, lru_out, log_decay)
    before = lax.ppermute(lru_out[-1:], SP, [(s, s + 1) for s in range(NSP - 1)])
    sent = pack(meta, route_ids, route_weights, stream_mid, d_out)
    got = lax.all_to_all(sent.reshape(NSP, CHUNK, HALF), SP, 0, 0, tiled=True)
    got = got.reshape(SLOTS, HALF)
    got_peer = swapped(got)
    all_gated = (gated, *(turned(gated, k) for k in (1, 2, 3)))
    hid, gg, gu, part_own, part_peer = expert(
        meta, perm, got, got_peer, exp_gate[0], exp_up[0], exp_down[0]
    )
    other = swapped(part_peer)
    back = (part_own.astype(F32) + other.astype(F32)).astype(BF)
    ret = lax.all_to_all(back.reshape(NSP, CHUNK, HALF // 2), SP, 0, 0, tiled=True)
    grad_gate, grad_up, grad_down = weight_grads(meta, perm, got, got_peer, hid, gg, gu)
    dm, *blocks = combine(meta, route_ids, ret.reshape(SLOTS, HALF // 2), d_out)
    dm_peer = swapped(dm)
    own = (blocks[0], *(turned(blocks[k], k) for k in (1, 2, 3)))
    d_gate, drive_value, head = drive(meta, dm, dm_peer, w_out, gate_pre, lru_out, log_decay)
    pair = jnp.concatenate([head, block], axis=0).reshape(1, 16, 128)
    links = lax.all_to_all(jnp.broadcast_to(pair, (NSP, 16, 128)), SP, 0, 0, tiled=True)
    peer = (dm_peer, *(swapped(own[k]) for k in (1, 2, 3)))
    share = outer(meta, own, peer, all_gated)
    shares = lax.all_to_all(share.reshape(16, 32, HALF), ("y", "x"), 0, 0, tiled=True)
    d_drive, d_log_decay = finish(
        meta, links.reshape(2 * NSP, HALF), drive_value, log_decay, lru_out, before
    )
    grad_out_proj = jnp.sum(shares.astype(F32), axis=0)
    return (
        grad_gate[None], grad_up[None], grad_down[None], grad_out_proj, d_gate, d_drive, d_log_decay,
    )


def solution(mesh):
    fine = Mesh(mesh.devices.reshape(4, 4, 4, 2), ("z", "y", "x", "tp"))
    tokens = P(SP, None)
    both = P(SP, "tp")
    hidden = P(SP, None, "tp")
    in_specs = (
        tokens, tokens, tokens, tokens, both, both, both, P("tp", None),
        hidden, hidden, P(SP, "tp", None),
    )
    out_specs = (hidden, hidden, P(SP, "tp", None), both, both, both, both)
    return jax.shard_map(
        on_device, mesh=fine, in_specs=in_specs, out_specs=out_specs, check_vma=False
    )
```

profile of v0, /device:TPU:1, one launch (start us, length us, event | category | flops | bytes accessed | tf_op | source)
XLA Modules:
  0.0 212.8 jit_solution(17349841641815885133)
XLA Ops:
  0.6 0.8 copy.19.ids_ref
  1.4 0.8 copy.20.w_ref
  2.3 1.1 copy-done.7
  3.5 1.1 copy-done.17
  4.6 6.2 %pack.1 = bf16[1536,1024]{1,0:T(8,128)(2,1)S(1)} custom-call(s32[3]{0:T(128)S(1)} %pad_add_fusion.meta, s32[192,2]{1,0:T(8,128)S(1)} %copy.19.ids_ref, f32[192,2]{1,0:T(8,128)S(1)} %copy.20.w_ref, bf16[192,2048]{1,0:T(8,128)(2,1)S(1)} %copy-done.17, bf16[192,2048]{1,0:T(8,128)(2,1)S(1)} %copy-done.7), custom_call_target="tpu_custom_call" | custom-call | tf_op jit(solution)/shard_map/pack/pallas_call | solution.py:92
  10.8 52.2 %all_to_all.20 = bf16[64,24,1024]{2,1,0:T(8,128)(2,1)S(1)} all-to-all(bf16[64,24,1024]{2,1,0:T(8,128)(2,1)S(1)} %bitcast.14), channel_id=1, replica_groups=mesh['z'=4,'y'=4,'x'=4,'tp'=2] {'z','y','x'}, dimensions={0} | all-to-all | bytes 6291456 | tf_op jit(solution)/shard_map/all_to_all | solution.py:429
  63.1 2.1 collective-permute-start
  65.2 5.3 %collective-permute-done.peer_ref = bf16[1536,1024]{1,0:T(8,128)(2,1)S(1)} collective-permute-done((bf16[1536,1024]{1,0:T(8,128)(2,1)S(1)}, bf16[1536,1024]{1,0:T(8,128)(2,1)S(1)}, u32[]{:S(2)}, u32[]{:S(2)}) %collective-permute-start) | collective-permute-done | bytes 3145760 | tf_op jit(solution)/shard_map/ppermute | solution.py:412
  70.5 1.7 copy-done.9
  72.1 17.8 %expert.1 = (bf16[768,512]{1,0:T(8,128)(2,1)S(1)}, bf16[768,512]{1,0:T(8,128)(2,1)S(1)}, bf16[768,512]{1,0:T(8,128)(2,1)S(1)}, bf16[1536,512]{1,0:T(8,128)(2,1)S(1)}, bf16[1536,512]{1,0:T(8,128)(2,1)S(1)}) custom-call(s32[3]{0:T(128)S(1)} %pad_add_fusion.meta, bf16[192,192]{1,0:T(8,128)(2,1)S(1)} %copy-done.24, bf16[1536,1024]{1,0:T(8,128)(2,1)} %bitcast.16, ...), custom_call_target="tpu_custom_call" | custom-call | tf_op jit(solution)/shard_map/expert/pallas_call | solution.py:149
  90.0 0.4 collective-permute-start.1
  90.4 3.0 %collective-permute-done.1 = bf16[1536,512]{1,0:T(8,128)(2,1)S(1)} collective-permute-done((bf16[1536,512]{1,0:T(8,128)(2,1)S(1)}, bf16[1536,512]{1,0:T(8,128)(2,1)S(1)}, u32[]{:S(2)}, u32[]{:S(2)}) %collective-permute-start.1) | collective-permute-done | bytes 1572896 | tf_op jit(solution)/shard_map/ppermute | solution.py:412
  93.5 0.4 add_convert_fusion
  94.0 28.4 %all_to_all.21 = bf16[64,24,512]{2,1,0:T(8,128)(2,1)S(1)} all-to-all(bf16[64,24,512]{2,1,0:T(8,128)(2,1)S(1)} %bitcast.23), channel_id=1, replica_groups=mesh['z'=4,'y'=4,'x'=4,'tp'=2] {'z','y','x'}, dimensions={0} | all-to-all | bytes 3145728 | tf_op jit(solution)/shard_map/all_to_all | solution.py:438
  122.4 1.8 combine.1
  124.2 1.9 collective-permute-start.5
  126.5 0.7 collective-permute-start.11
  127.5 3.6 %drive.1 = (bf16[192,1024]{1,0:T(8,128)(2,1)}, f32[192,1024]{1,0:T(8,128)S(1)}, f32[1,1024]{1,0:T(1,128)S(1)}) custom-call(s32[3]{0:T(128)S(1)} %pad_add_fusion.meta, bf16[192,1024]{1,0:T(8,128)(2,1)S(1)} %get-tuple-element.39.own_ref, bf16[192,1024]{1,0:T(8,128)(2,1)S(1)} %collective-permute-done.5.refs_4_.peer_ref, bf16[1024,2048]{1,0:T(8,128)(2,1)S(1)} %copy-done.4, ...), custom_call_target="tpu_custom_call" | custom-call | tf_op jit(solution)/shard_map/drive/pallas_call | solution.py:325
  131.1 0.9 copy-done.18
  132.0 0.8 broadcast_in_dim.20
  132.8 5.5 %all-to-all-start.3 = ((f32[64,16,128]{2,1,0:T(8,128)}), f32[64,16,128]{2,1,0:T(8,128)}, u32[]{:S(2)}, u32[]{:S(2)}) async-start(f32[64,16,128]{2,1,0:T(8,128)} %broadcast_in_dim.20), calls=%async_computation.3 | async-start | bytes 1048576 | tf_op jit(solution)/shard_map/all_to_all | solution.py:445
  138.3 2.6 %collective-permute-start.10 = (bf16[192,1024]{1,0:T(8,128)(2,1)S(1)}, bf16[192,1024]{1,0:T(8,128)(2,1)S(1)}, u32[]{:S(2)}, u32[]{:S(2)}) collective-permute-start(bf16[192,1024]{1,0:T(8,128)(2,1)S(1)} %get-tuple-element.40.refs_8_), channel_id=1, source_target_pairs={{0,64},{32,96},{64,0},{96,32},{1,65},{33,97},{65,1},{97,33},{2,66}... | collective-permute-start | bytes 1179656 | tf_op jit(solution)/shard_map/ppermute | solution.py:416
  141.0 0.4 collective-permute-start.9
  141.4 3.4 %collective-permute-start.3 = (bf16[192,256]{1,0:T(8,128)(2,1)S(1)}, bf16[192,256]{1,0:T(8,128)(2,1)S(1)}, u32[]{:S(2)}, u32[]{:S(2)}) collective-permute-start(bf16[192,256]{1,0:T(8,128)(2,1)S(1)} %get-tuple-element.37), channel_id=1, source_target_pairs={{0,64},{32,96},{64,0},{96,32},{1,65},{33,97},{65,1},{97,33},{2,66}... | collective-permute-start | bytes 294920 | tf_op jit(solution)/shard_map/ppermute | solution.py:416
  144.8 0.8 copy-done.22
  145.8 21.9 %collective-permute-done.2.refs_1_ = bf16[192,256]{1,0:T(8,128)(2,1)S(1)} collective-permute-done((bf16[192,256]{1,0:T(8,128)(2,1)S(1)}, bf16[192,256]{1,0:T(8,128)(2,1)S(1)}, u32[]{:S(2)}, u32[]{:S(2)}) %collective-permute-start.2) | collective-permute-done | bytes 98336 | tf_op jit(solution)/shard_map/ppermute | solution.py:416
  167.7 0.4 collective-permute-start.6
  168.5 1.1 collective-permute-start.7
  169.6 0.9 collective-permute-done.7.refs_6_
  170.8 1.0 copy-done.16
  171.8 1.0 copy-done.21
  172.8 1.0 copy-done.23
  173.8 0.9 copy-done.27
  174.7 1.8 outer.1
  176.6 1.0 copy-done.5
  177.5 6.0 %all-to-all-start.2 = ((bf16[16,32,1024]{2,1,0:T(8,128)(2,1)}), bf16[16,32,1024]{2,1,0:T(8,128)(2,1)}, u32[]{:S(2)}, u32[]{:S(2)}) async-start(bf16[16,32,1024]{2,1,0:T(8,128)(2,1)} %bitcast.19), calls=%async_computation.2 | async-start | bytes 2097152 | tf_op jit(solution)/shard_map/all_to_all | solution.py:448
  183.5 3.2 %collective-permute-start.12 = (bf16[1,1024]{1,0:T(2,128)(2,1)S(1)}, bf16[1,1024]{1,0:T(2,128)(2,1)S(1)}, u32[]{:S(2)}, u32[]{:S(2)}) collective-permute-start(bf16[1,1024]{1,0:T(2,128)(2,1)S(1)} %slice.3), channel_id=1, source_target_pairs={{0,2},{2,4},{4,6},{6,8},{8,10},{10,12},{12,14},{14,16},{16,18},{18... | collective-permute-start | bytes 6152 | tf_op jit(solution)/shard_map/ppermute | solution.py:427
  186.8 1.9 copy-done.10
  188.7 0.9 copy-done.25
  189.6 1.1 copy-done.29
  190.7 1.1 copy-done.31
  191.8 1.1 copy-done.33
  193.0 11.3 %weight_grads.1 = (f32[2048,512]{1,0:T(8,128)}, f32[2048,512]{1,0:T(8,128)}, f32[512,2048]{1,0:T(8,128)}) custom-call(s32[3]{0:T(128)S(1)} %pad_add_fusion.meta, bf16[192,192]{1,0:T(8,128)(2,1)S(1)} %copy-done.25, bf16[1536,1024]{1,0:T(8,128)(2,1)S(1)} %bitcast.17, bf16[1536,1024]{1,0:T(8,128)(2,1)S(1)} %copy-done.10, bf16[768,512]{1,0:T(8,128)(2,1)S(1)} %copy-done.29, ...), custom_call_target="tpu_custom_call" | custom-call | flops 4831838208 | bytes 20000000 | tf_op jit(solution)/shard_map/weight_grads/pallas_call | solution.py:197
  204.3 1.1 reshape.39.links_ref
  205.5 1.1 copy-done.3
  206.6 1.1 copy-done.19
  207.7 3.0 %finish.1 = (f32[192,1024]{1,0:T(8,128)}, f32[192,1024]{1,0:T(8,128)}) custom-call(s32[3]{0:T(128)S(1)} %pad_add_fusion.meta, f32[128,1024]{1,0:T(8,128)S(1)} %reshape.39.links_ref, f32[192,1024]{1,0:T(8,128)S(1)} %copy-done.19, f32[192,1024]{1,0:T(8,128)S(1)} %copy-done.3, bf16[192,1024]{1,0:T(8,128)(2,1)S(1)} %copy-done.6, ...), custom_call_target="tpu_custom_call" | custom-call | tf_op jit(solution)/shard_map/finish/pallas_call | solution.py:367
  210.7 2.1 convert_reduce_fusion
  (70 shorter events, 1.8 us)
Async XLA Ops:
  2.3 1.1 copy-start.7
  3.5 1.1 copy-start.17
  4.6 67.5 %copy-start.24 = (bf16[192,192]{1,0:T(8,128)(2,1)S(1)}, bf16[192,192]{1,0:T(8,128)(2,1)}, u32[]{:S(2)}) copy-start(bf16[192,192]{1,0:T(8,128)(2,1)} %constant.23.clone.perm_ref) | copy-start | bytes 221188
  10.8 61.3 %copy-start.11 = (bf16[1,2048,512]{2,1,0:T(8,128)(2,1)S(1)}, bf16[1,2048,512]{2,1,0:T(8,128)(2,1)}, u32[]{:S(2)}) copy-start(bf16[1,2048,512]{2,1,0:T(8,128)(2,1)} %param.20) | copy-start | bytes 6291460
  10.8 61.3 %copy-start.12 = (bf16[1,2048,512]{2,1,0:T(8,128)(2,1)S(1)}, bf16[1,2048,512]{2,1,0:T(8,128)(2,1)}, u32[]{:S(2)}) copy-start(bf16[1,2048,512]{2,1,0:T(8,128)(2,1)} %param.21) | copy-start | bytes 6291460
  10.8 61.3 %copy-start.13 = (bf16[1,512,2048]{2,1,0:T(8,128)(2,1)S(1)}, bf16[1,512,2048]{2,1,0:T(8,128)(2,1)}, u32[]{:S(2)}) copy-start(bf16[1,512,2048]{2,1,0:T(8,128)(2,1)} %param.22) | copy-start | bytes 6291460
  63.1 7.4 %copy-start = (bf16[64,24,1024]{2,1,0:T(8,128)(2,1)}, bf16[64,24,1024]{2,1,0:T(8,128)(2,1)S(1)}, u32[]{:S(2)}) copy-start(bf16[64,24,1024]{2,1,0:T(8,128)(2,1)S(1)} %all_to_all.20) | copy-start | bytes 9437188
  63.1 7.4 %collective-permute-start = (bf16[1536,1024]{1,0:T(8,128)(2,1)S(1)}, bf16[1536,1024]{1,0:T(8,128)(2,1)S(1)}, u32[]{:S(2)}, u32[]{:S(2)}) collective-permute-start(bf16[1536,1024]{1,0:T(8,128)(2,1)S(1)} %bitcast.15), channel_id=1, source_target_pairs={{0,1},{1,0},{2,3},{3,2},{4,5},{5,4},{6,7},{7,6},{8,9},{9,8},{10,11... | collective-permute-start | bytes 9437192 | tf_op jit(solution)/shard_map/ppermute | solution.py:412
  70.5 1.7 copy-start.9
  89.9 4.0 %copy-start.28 = (bf16[768,512]{1,0:T(8,128)(2,1)}, bf16[768,512]{1,0:T(8,128)(2,1)S(1)}, u32[]{:S(2)}) copy-start(bf16[768,512]{1,0:T(8,128)(2,1)S(1)} %get-tuple-element.27.hid_ref) | copy-start | bytes 2359300
  89.9 4.0 %copy-start.30 = (bf16[768,512]{1,0:T(8,128)(2,1)}, bf16[768,512]{1,0:T(8,128)(2,1)S(1)}, u32[]{:S(2)}) copy-start(bf16[768,512]{1,0:T(8,128)(2,1)S(1)} %get-tuple-element.28.gg_ref) | copy-start | bytes 2359300
  90.0 4.0 %copy-start.32 = (bf16[768,512]{1,0:T(8,128)(2,1)}, bf16[768,512]{1,0:T(8,128)(2,1)S(1)}, u32[]{:S(2)}) copy-start(bf16[768,512]{1,0:T(8,128)(2,1)S(1)} %get-tuple-element.29.gu_ref) | copy-start | bytes 2359300
  90.0 3.5 %collective-permute-start.1 = (bf16[1536,512]{1,0:T(8,128)(2,1)S(1)}, bf16[1536,512]{1,0:T(8,128)(2,1)S(1)}, u32[]{:S(2)}, u32[]{:S(2)}) collective-permute-start(bf16[1536,512]{1,0:T(8,128)(2,1)S(1)} %get-tuple-element.34), channel_id=1, source_target_pairs={{0,1},{1,0},{2,3},{3,2},{4,5},{5,4},{6,7},{7,6},{8,9},{9,8},{10,11... | collective-permute-start | bytes 4718600 | tf_op jit(solution)/shard_map/ppermute | solution.py:412
  93.5 28.9 %copy-start.8 = (bf16[192,2048]{1,0:T(8,128)(2,1)S(1)}, bf16[192,2048]{1,0:T(8,128)(2,1)}, u32[]{:S(2)}) copy-start(bf16[192,2048]{1,0:T(8,128)(2,1)} %d_ref.3) | copy-start | bytes 2359300
  93.5 32.7 %copy-start.14 = (bf16[192,1024]{1,0:T(8,128)(2,1)S(1)}, bf16[192,1024]{1,0:T(8,128)(2,1)}, u32[]{:S(2)}) copy-start(bf16[192,1024]{1,0:T(8,128)(2,1)} %gate_ref.3) | copy-start | bytes 1179652
  93.9 32.2 %copy-start.2 = (f32[192,1024]{1,0:T(8,128)S(1)}, f32[192,1024]{1,0:T(8,128)}, u32[]{:S(2)}) copy-start(f32[192,1024]{1,0:T(8,128)} %decay_ref.5) | copy-start | bytes 2359300
  93.9 32.2 %copy-start.6 = (bf16[192,1024]{1,0:T(8,128)(2,1)S(1)}, bf16[192,1024]{1,0:T(8,128)(2,1)}, u32[]{:S(2)}) copy-start(bf16[192,1024]{1,0:T(8,128)(2,1)} %lru_ref.5) | copy-start | bytes 1179652
  94.0 33.5 %copy-start.4 = (bf16[1024,2048]{1,0:T(8,128)(2,1)S(1)}, bf16[1024,2048]{1,0:T(8,128)(2,1)}, u32[]{:S(2)}) copy-start(bf16[1024,2048]{1,0:T(8,128)(2,1)} %w_ref.2) | copy-start | bytes 12582916
  124.2 3.0 %copy-start.26 = (bf16[192,256]{1,0:T(8,128)(2,1)}, bf16[192,256]{1,0:T(8,128)(2,1)S(1)}, u32[]{:S(2)}) copy-start(bf16[192,256]{1,0:T(8,128)(2,1)S(1)} %get-tuple-element.35.refs_0_) | copy-start | bytes 294916
  124.2 3.3 %collective-permute-start.5 = (bf16[192,1024]{1,0:T(8,128)(2,1)S(1)}, bf16[192,1024]{1,0:T(8,128)(2,1)S(1)}, u32[]{:S(2)}, u32[]{:S(2)}) collective-permute-start(bf16[192,1024]{1,0:T(8,128)(2,1)S(1)} %get-tuple-element.39.own_ref), channel_id=1, source_target_pairs={{0,1},{1,0},{2,3},{3,2},{4,5},{5,4},{6,7},{7,6},{8,9},{9,8},{10,11... | collective-permute-start | bytes 1179656 | tf_op jit(solution)/shard_map/ppermute | solution.py:412
  126.5 14.5 %copy-start.20 = (bf16[192,1024]{1,0:T(8,128)(2,1)}, bf16[192,1024]{1,0:T(8,128)(2,1)S(1)}, u32[]{:S(2)}) copy-start(bf16[192,1024]{1,0:T(8,128)(2,1)S(1)} %get-tuple-element.40.refs_8_) | copy-start | bytes 1179652
  126.5 18.3 %collective-permute-start.11 = (bf16[192,1024]{1,0:T(8,128)(2,1)S(1)}, bf16[192,1024]{1,0:T(8,128)(2,1)S(1)}, u32[]{:S(2)}, u32[]{:S(2)}) collective-permute-start(bf16[192,1024]{1,0:T(8,128)(2,1)S(1)} %get-tuple-element.40.refs_8_), channel_id=1, source_target_pairs={{0,96},{32,0},{64,32},{96,64},{1,97},{33,1},{65,33},{97,65},{2,98}... | collective-permute-start | bytes 1179656 | tf_op jit(solution)/shard_map/ppermute | solution.py:416
  127.5 3.6 %copy-start.15 = (bf16[192,1024]{1,0:T(8,128)(2,1)}, bf16[192,1024]{1,0:T(8,128)(2,1)S(1)}, u32[]{:S(2)}) copy-start(bf16[192,1024]{1,0:T(8,128)(2,1)S(1)} %collective-permute-done.5.refs_4_.peer_ref) | copy-start | bytes 1179652
  131.1 0.9 copy-start.18
  132.8 44.7 %all-to-all-start.3 = ((f32[64,16,128]{2,1,0:T(8,128)}), f32[64,16,128]{2,1,0:T(8,128)}, u32[]{:S(2)}, u32[]{:S(2)}) async-start(f32[64,16,128]{2,1,0:T(8,128)} %broadcast_in_dim.20), calls=%async_computation.3 | async-start | bytes 1048576 | tf_op jit(solution)/shard_map/all_to_all | solution.py:445
  138.3 31.2 %collective-permute-start.10 = (bf16[192,1024]{1,0:T(8,128)(2,1)S(1)}, bf16[192,1024]{1,0:T(8,128)(2,1)S(1)}, u32[]{:S(2)}, u32[]{:S(2)}) collective-permute-start(bf16[192,1024]{1,0:T(8,128)(2,1)S(1)} %get-tuple-element.40.refs_8_), channel_id=1, source_target_pairs={{0,64},{32,96},{64,0},{96,32},{1,65},{33,97},{65,1},{97,33},{2,66}... | collective-permute-start | bytes 1179656 | tf_op jit(solution)/shard_map/ppermute | solution.py:416
  141.0 28.6 %collective-permute-start.9 = (bf16[192,1024]{1,0:T(8,128)(2,1)S(1)}, bf16[192,1024]{1,0:T(8,128)(2,1)S(1)}, u32[]{:S(2)}, u32[]{:S(2)}) collective-permute-start(bf16[192,1024]{1,0:T(8,128)(2,1)S(1)} %get-tuple-element.40.refs_8_), channel_id=1, source_target_pairs={{0,32},{32,64},{64,96},{96,0},{1,33},{33,65},{65,97},{97,1},{2,34}... | collective-permute-start | bytes 1179656 | tf_op jit(solution)/shard_map/ppermute | solution.py:416
  141.4 26.3 %collective-permute-start.2 = (bf16[192,256]{1,0:T(8,128)(2,1)S(1)}, bf16[192,256]{1,0:T(8,128)(2,1)S(1)}, u32[]{:S(2)}, u32[]{:S(2)}) collective-permute-start(bf16[192,256]{1,0:T(8,128)(2,1)S(1)} %get-tuple-element.36), channel_id=1, source_target_pairs={{0,32},{32,64},{64,96},{96,0},{1,33},{33,65},{65,97},{97,1},{2,34}... | collective-permute-start | bytes 294920 | tf_op jit(solution)/shard_map/ppermute | solution.py:416
  141.4 27.1 %collective-permute-start.3 = (bf16[192,256]{1,0:T(8,128)(2,1)S(1)}, bf16[192,256]{1,0:T(8,128)(2,1)S(1)}, u32[]{:S(2)}, u32[]{:S(2)}) collective-permute-start(bf16[192,256]{1,0:T(8,128)(2,1)S(1)} %get-tuple-element.37), channel_id=1, source_target_pairs={{0,64},{32,96},{64,0},{96,32},{1,65},{33,97},{65,1},{97,33},{2,66}... | collective-permute-start | bytes 294920 | tf_op jit(solution)/shard_map/ppermute | solution.py:416
  145.6 24.0 %collective-permute-start.4 = (bf16[192,256]{1,0:T(8,128)(2,1)S(1)}, bf16[192,256]{1,0:T(8,128)(2,1)S(1)}, u32[]{:S(2)}, u32[]{:S(2)}) collective-permute-start(bf16[192,256]{1,0:T(8,128)(2,1)S(1)} %get-tuple-element.38), channel_id=1, source_target_pairs={{0,96},{32,0},{64,32},{96,64},{1,97},{33,1},{65,33},{97,65},{2,98}... | collective-permute-start | bytes 294920 | tf_op jit(solution)/shard_map/ppermute | solution.py:416
  167.7 1.9 collective-permute-start.6
  168.5 2.0 collective-permute-start.7
  169.5 1.3 collective-permute-start.8
  170.8 1.0 copy-start.16
  171.8 1.0 copy-start.21
  172.8 1.0 copy-start.23
  173.8 0.9 copy-start.27
  174.7 12.0 %copy-start.1 = (bf16[64,24,1024]{2,1,0:T(8,128)(2,1)S(1)}, bf16[64,24,1024]{2,1,0:T(8,128)(2,1)}, u32[]{:S(2)}) copy-start(bf16[64,24,1024]{2,1,0:T(8,128)(2,1)} %copy-done) | copy-start | bytes 9437188
  176.5 1.0 copy-start.5
  177.5 33.2 %all-to-all-start.2 = ((bf16[16,32,1024]{2,1,0:T(8,128)(2,1)}), bf16[16,32,1024]{2,1,0:T(8,128)(2,1)}, u32[]{:S(2)}, u32[]{:S(2)}) async-start(bf16[16,32,1024]{2,1,0:T(8,128)(2,1)} %bitcast.19), calls=%async_computation.2 | async-start | bytes 2097152 | tf_op jit(solution)/shard_map/all_to_all | solution.py:448
  183.5 21.9 %collective-permute-start.12 = (bf16[1,1024]{1,0:T(2,128)(2,1)S(1)}, bf16[1,1024]{1,0:T(2,128)(2,1)S(1)}, u32[]{:S(2)}, u32[]{:S(2)}) collective-permute-start(bf16[1,1024]{1,0:T(2,128)(2,1)S(1)} %slice.3), channel_id=1, source_target_pairs={{0,2},{2,4},{4,6},{6,8},{8,10},{10,12},{12,14},{14,16},{16,18},{18... | collective-permute-start | bytes 6152 | tf_op jit(solution)/shard_map/ppermute | solution.py:427
  186.8 1.9 copy-start.10
  188.7 0.9 copy-start.25
  189.6 1.1 copy-start.29
  190.7 1.1 copy-start.31
  191.8 1.1 copy-start.33
  205.4 1.1 copy-start.3
  206.6 1.1 copy-start.19
  (1 other events, 0.8 us)
where the time goes:
time: 214 us; the launch traced here: 213 us
  blocking collectives  80.6 us (38%)
  Pallas kernels  45.9 us (21%)
  waiting for transfers between devices  32.2 us (15%)
  starting transfers between devices  28 us (13%)
  local copies, waits for them, and re-layouts  22.5 us (11%)
  other arithmetic  2.6 us (1%)
    all_to_all x1, blocking collectives, on_device(): got = lax.all_to_all(sent.reshape(NSP, CHUNK, HALF), SP, 0, 0, tiled=True)  52.2 us
    all_to_all x1, blocking collectives, on_device(): lax.all_to_all(back.reshape(NSP, CHUNK, HALF // 2), SP, 0, 0, tiled=True)  28.4 us
    ppermute x6, waiting for transfers between devices, turned(): return lax.ppermute(value, 'z', [(s, (s + steps) % 4) for s in range(4)])  22.3 us
    unnamed x70, local copies, waits for them, and re-layouts  20.6 us
    pallas_call x1, Pallas kernels, expert(): pl.pallas_call(expert_kernel, name='expert', grid_spec=pltpu.PrefetchScal...  17.8 us
    pallas_call x1, Pallas kernels, weight_grads(): pl.pallas_call(weight_kernel, name='weight_grads', grid_spec=pltpu.Prefet...  11.3 us
    ppermute x6, waiting for transfers between devices, swapped(): return lax.ppermute(value, 'tp', [(0, 1), (1, 0)])  9.85 us
    ppermute x6, starting transfers between devices, turned(): return lax.ppermute(value, 'z', [(s, (s + steps) % 4) for s in range(4)])  7.37 us
  transfers between devices with their start and end apart: 15, of which 7 were waited for; matrix products, arithmetic and copies ran while one was open for 1% of the time, Pallas kernels for 9%

commit v1 on v0

v1 whole, which is shorter than its diff:
```python
import jax
import jax.numpy as jnp
import numpy as np
from jax import lax
from jax.experimental import pallas as pl
from jax.experimental.pallas import tpu as pltpu
from jax.sharding import Mesh, PartitionSpec as P

BF = jnp.bfloat16
F32 = jnp.float32
SP = ("z", "y", "x")
TOK = 192
D = 2048
HALF = 1024
BLK = 256
CAP = 12
CHUNK = 24
NSP = 64
SLOTS = NSP * CHUNK
ROWS = NSP * CAP
FF = 512
GROUP = 8 * CHUNK

_perm = np.zeros((GROUP, GROUP), np.float32)
for _s in range(8):
    for _h in range(2):
        for _r in range(CAP):
            _perm[_h * 96 + _s * CAP + _r, _s * CHUNK + _h * CAP + _r] = 1.0


def dot(a, b):
    return lax.dot_general(a, b, (((1,), (0,)), ((), ())), preferred_element_type=F32)


def dot_cols(a, b):
    return lax.dot_general(a, b, (((1,), (1,)), ((), ())), preferred_element_type=F32)


def dot_rows(a, b):
    return lax.dot_general(a, b, (((0,), (0,)), ((), ())), preferred_element_type=F32)


def vm(mib):
    return pltpu.CompilerParams(vmem_limit_bytes=mib * 1024 * 1024)


def lanes(index, width=BLK):
    return pl.ds(pl.multiple_of(index * width, width), width)


def slot_rows(ids_ref):
    lane = lax.broadcasted_iota(jnp.int32, (NSP, TOK), 0)
    ids0, ids1 = ids_ref[0:1, :], ids_ref[1:2, :]
    hot0 = jnp.where(lane == ids0, 1.0, 0.0)
    hot1 = jnp.where(lane == ids1, 1.0, 0.0)
    row = lax.broadcasted_iota(jnp.int32, (TOK, TOK), 0)
    col = lax.broadcasted_iota(jnp.int32, (TOK, TOK), 1)
    before = jnp.where(row < col, 1.0, 0.0).astype(BF)
    rank0 = dot(hot0.astype(BF), before)
    rank1 = dot(hot1.astype(BF), before) + jnp.sum(hot0, axis=1, keepdims=True)
    first0 = jnp.sum(hot0 * rank0, axis=0, keepdims=True)
    first1 = jnp.sum(hot1 * rank1, axis=0, keepdims=True)
    return ids0.astype(F32) * CHUNK + first0, ids1.astype(F32) * CHUNK + first1


def as_column(line):
    row = lax.broadcasted_iota(jnp.int32, (TOK, TOK), 0)
    col = lax.broadcasted_iota(jnp.int32, (TOK, TOK), 1)
    return jnp.sum(jnp.where(row == col, line, 0.0), axis=1, keepdims=True)


def whole(count):
    vmem = pl.BlockSpec(memory_space=pltpu.VMEM)
    return [pl.BlockSpec(memory_space=pltpu.SMEM)] + [vmem] * count


def cost(flops, moved=0):
    return pl.CostEstimate(flops=int(flops), bytes_accessed=int(moved), transcendentals=0)


def pack_kernel(meta, ids_ref, w_ref, x_ref, d_ref, out_ref, sx, s0, s1):
    @pl.when(pl.program_id(0) == 0)
    def _():
        r0, r1 = slot_rows(ids_ref)
        r0, r1 = r0.astype(jnp.int32), r1.astype(jnp.int32)
        slot = lax.broadcasted_iota(jnp.int32, (SLOTS, TOK), 0)
        sx[...] = jnp.where((slot == r0) | (slot == r1), 1.0, 0.0).astype(BF)
        s0[...] = jnp.where(slot == r0 + CAP, 1.0, 0.0).astype(BF)
        s1[...] = jnp.where(slot == r1 + CAP, 1.0, 0.0).astype(BF)

    d = d_ref[...].astype(F32)
    scaled0 = (as_column(w_ref[0:1, :]) * d).astype(BF)
    scaled1 = (as_column(w_ref[1:2, :]) * d).astype(BF)
    out = dot(sx[...], x_ref[...]) + dot(s0[...], scaled0) + dot(s1[...], scaled1)
    out_ref[...] = out.astype(BF)


def pack(meta, ids, weights, stream, d_out):
    return pl.pallas_call(
        pack_kernel,
        name="pack",
        grid_spec=pltpu.PrefetchScalarGridSpec(
            num_scalar_prefetch=1,
            grid=(4,),
            in_specs=[
                pl.BlockSpec((2, TOK), lambda j, m: (0, 0)),
                pl.BlockSpec((2, TOK), lambda j, m: (0, 0)),
                pl.BlockSpec((TOK, BLK), lambda j, m: (0, 2 * j + m[0])),
                pl.BlockSpec((TOK, BLK), lambda j, m: (0, 2 * j + m[0])),
            ],
            out_specs=pl.BlockSpec((SLOTS, BLK), lambda j, m: (0, j)),
            scratch_shapes=[pltpu.VMEM((SLOTS, TOK), BF)] * 3,
        ),
        out_shape=jax.ShapeDtypeStruct((SLOTS, HALF), BF),
        compiler_params=vm(12),
    )(meta, ids, weights, stream, d_out)


def compact(perm, src_ref, xs, cs):
    for g in range(8):
        moved = dot(perm, src_ref[g * GROUP : (g + 1) * GROUP, :]).astype(BF)
        xs[g * 96 : (g + 1) * 96, :] = moved[:96]
        cs[g * 96 : (g + 1) * 96, :] = moved[96:]


def projections(par, xs, cs, wg_ref, wu_ref, wd_ref):
    gate = up = back = 0.0
    for j in range(4):
        mine, part = slice(j * BLK, (j + 1) * BLK), lanes(2 * j + par)
        gate += dot(xs[:, mine], wg_ref[part, :])
        up += dot(xs[:, mine], wu_ref[part, :])
        back += dot_cols(cs[:, mine], wd_ref[:, part])
    return gate, up, back


def returned(par, perm_t, gg_ref, gu_ref, wg_ref, wu_ref, ys, dst_ref):
    gg, gu = gg_ref[...], gu_ref[...]
    for j in range(4):
        part = lanes(2 * j + par)
        y = dot_cols(gg, wg_ref[part, :]) + dot_cols(gu, wu_ref[part, :])
        ys[j // 2, :, (j % 2) * BLK : (j % 2 + 1) * BLK] = y.astype(BF)
    for g in range(8):
        rows = slice(g * 96, (g + 1) * 96)
        both = jnp.concatenate([ys[0, rows, :], ys[1, rows, :]], axis=0)
        dst_ref[g * GROUP : (g + 1) * GROUP, :] = dot(perm_t, both).astype(BF)


def own_kernel(meta, perm_ref, own_ref, wg_ref, wu_ref, wd_ref, pg_ref, pu_ref, pb_ref, xs, cs):
    compact(perm_ref[...], own_ref, xs, cs)
    gate, up, back = projections(meta[0], xs, cs, wg_ref, wu_ref, wd_ref)
    pg_ref[...] = gate
    pu_ref[...] = up
    pb_ref[...] = back


def expert_own(meta, perm, own, wg, wu, wd):
    return pl.pallas_call(
        own_kernel,
        name="expert_own",
        in_specs=whole(5),
        out_specs=[pl.BlockSpec(memory_space=pltpu.VMEM)] * 3,
        out_shape=[jax.ShapeDtypeStruct((ROWS, FF), F32)] * 3,
        scratch_shapes=[pltpu.VMEM((ROWS, HALF), BF)] * 2,
        compiler_params=vm(16),
        cost_estimate=cost(4e9),
    )(meta, perm, own, wg, wu, wd)


def peer_kernel(
    meta, perm_ref, perm_t_ref, peer_ref, wg_ref, wu_ref, wd_ref, pg_ref, pu_ref, pb_ref,
    hid_ref, gg_ref, gu_ref, part_ref, xs, cs, ys,
):
    par = 1 - meta[0]
    compact(perm_ref[...], peer_ref, xs, cs)
    gate, up, back = projections(par, xs, cs, wg_ref, wu_ref, wd_ref)
    gate += pg_ref[...]
    up += pu_ref[...]
    back += pb_ref[...]
    sig = jax.nn.sigmoid(gate)
    act = gate * sig
    hid_ref[...] = (act * up).astype(BF)
    gg_ref[...] = (back * up * sig * (1.0 + gate * (1.0 - sig))).astype(BF)
    gu_ref[...] = (back * act).astype(BF)
    returned(par, perm_t_ref[...], gg_ref, gu_ref, wg_ref, wu_ref, ys, part_ref)


def expert_peer(meta, perm, perm_t, peer, wg, wu, wd, pg, pu, pb):
    return pl.pallas_call(
        peer_kernel,
        name="expert_peer",
        in_specs=whole(9),
        out_specs=[pl.BlockSpec(memory_space=pltpu.VMEM)] * 4,
        out_shape=[jax.ShapeDtypeStruct((ROWS, FF), BF)] * 3
        + [jax.ShapeDtypeStruct((SLOTS, HALF // 2), BF)],
        scratch_shapes=[pltpu.VMEM((ROWS, HALF), BF)] * 2 + [pltpu.VMEM((2, ROWS, HALF // 2), BF)],
        compiler_params=vm(20),
        cost_estimate=cost(6e9),
    )(meta, perm, perm_t, peer, wg, wu, wd, pg, pu, pb)


def back_kernel(meta, perm_t_ref, gg_ref, gu_ref, wg_ref, wu_ref, part_ref, ys):
    returned(meta[0], perm_t_ref[...], gg_ref, gu_ref, wg_ref, wu_ref, ys, part_ref)


def expert_back(meta, perm_t, gg, gu, wg, wu):
    return pl.pallas_call(
        back_kernel,
        name="expert_back",
        in_specs=whole(5),
        out_specs=pl.BlockSpec(memory_space=pltpu.VMEM),
        out_shape=jax.ShapeDtypeStruct((SLOTS, HALF // 2), BF),
        scratch_shapes=[pltpu.VMEM((2, ROWS, HALF // 2), BF)],
        compiler_params=vm(16),
        cost_estimate=cost(3e9),
    )(meta, perm_t, gg, gu, wg, wu)


def weight_kernel(
    meta, perm_ref, own_ref, peer_ref, hid_ref, gg_ref, gu_ref, og_ref, ou_ref, od_ref, xs, cs
):
    h = pl.program_id(1)
    perm = perm_ref[...]
    for g in range(8):
        rows = slice(g * GROUP, (g + 1) * GROUP)
        src = jnp.where(h == 0, own_ref[rows, :], peer_ref[rows, :])
        moved = dot(perm, src).astype(BF)
        xs[g * 96 : (g + 1) * 96, :] = moved[:96]
        cs[g * 96 : (g + 1) * 96, :] = moved[96:]
    x = xs[...]
    og_ref[...] = dot_rows(x, gg_ref[...])
    ou_ref[...] = dot_rows(x, gu_ref[...])
    od_ref[...] = dot_rows(hid_ref[...], cs[...])


def weight_grads(meta, perm, own, peer, hid, gg, gu):
    block = lambda j, h, m: 2 * j + (h + m[0]) % 2
    return pl.pallas_call(
        weight_kernel,
        name="weight_grads",
        grid_spec=pltpu.PrefetchScalarGridSpec(
            num_scalar_prefetch=1,
            grid=(4, 2),
            in_specs=[
                pl.BlockSpec((GROUP, GROUP), lambda j, h, m: (0, 0)),
                pl.BlockSpec((SLOTS, BLK), lambda j, h, m: (0, j)),
                pl.BlockSpec((SLOTS, BLK), lambda j, h, m: (0, j)),
                pl.BlockSpec((ROWS, FF), lambda j, h, m: (0, 0)),
                pl.BlockSpec((ROWS, FF), lambda j, h, m: (0, 0)),
                pl.BlockSpec((ROWS, FF), lambda j, h, m: (0, 0)),
            ],
            out_specs=[
                pl.BlockSpec((BLK, FF), lambda j, h, m: (block(j, h, m), 0)),
                pl.BlockSpec((BLK, FF), lambda j, h, m: (block(j, h, m), 0)),
                pl.BlockSpec((FF, BLK), lambda j, h, m: (0, block(j, h, m))),
            ],
            scratch_shapes=[pltpu.VMEM((ROWS, BLK), BF)] * 2,
        ),
        out_shape=[
            jax.ShapeDtypeStruct((D, FF), F32),
            jax.ShapeDtypeStruct((D, FF), F32),
            jax.ShapeDtypeStruct((FF, D), F32),
        ],
        compiler_params=vm(18),
        cost_estimate=pl.CostEstimate(
            flops=3 * 2 * ROWS * D * FF, bytes_accessed=20_000_000, transcendentals=0
        ),
    )(meta, perm, own, peer, hid, gg, gu)


def combine_kernel(meta, ids_ref, ret_ref, d_ref, dm_ref, b0, b1, b2, b3):
    tp, z = meta[0], meta[1]
    r0, r1 = slot_rows(ids_ref)
    c0, c1 = as_column(r0).astype(jnp.int32), as_column(r1).astype(jnp.int32)
    slot = lax.broadcasted_iota(jnp.int32, (TOK, SLOTS), 1)
    for side in range(2):
        pick = (slot == c0 + side * CAP) | (slot == c1 + side * CAP)
        back = dot(jnp.where(pick, 1.0, 0.0).astype(BF), ret_ref[...])
        for k in range(2):
            j = 2 * side + k
            own = d_ref[:, lanes(2 * j + tp)].astype(F32)
            dm_ref[:, j * BLK : (j + 1) * BLK] = (own + back[:, k * BLK : (k + 1) * BLK]).astype(BF)
    for k, ref in enumerate((b0, b1, b2, b3)):
        ref[...] = dm_ref[:, lanes(lax.rem(z + k, 4))]


def combine(meta, ids, ret, d_out):
    return pl.pallas_call(
        combine_kernel,
        name="combine",
        in_specs=whole(3),
        out_specs=[pl.BlockSpec(memory_space=pltpu.VMEM)] * 5,
        out_shape=[jax.ShapeDtypeStruct((TOK, HALF), BF)]
        + [jax.ShapeDtypeStruct((TOK, BLK), BF)] * 4,
        compiler_params=vm(16),
        cost_estimate=cost(1e9),
    )(meta, ids, ret, d_out)


ROOT = 0.7978845608028654
CUBE = 0.044715


def gelu_parts(x):
    t = jnp.tanh(ROOT * (x + CUBE * x * x * x))
    return 0.5 * x * (1.0 + t), t


def tile_of(line):
    return jnp.concatenate([line[:, k * 128 : (k + 1) * 128] for k in range(8)], axis=0)


def line_of(tile):
    return jnp.concatenate([tile[k : k + 1, :] for k in range(8)], axis=1)


def early_kernel(gate_ref, lru_ref, gated_ref):
    value, _ = gelu_parts(gate_ref[...].astype(F32))
    gated_ref[...] = (value * lru_ref[...].astype(F32)).astype(BF)


def early(gate_pre, lru_out):
    return pl.pallas_call(
        early_kernel,
        name="early",
        out_shape=jax.ShapeDtypeStruct((TOK, HALF), BF),
        compiler_params=vm(4),
        cost_estimate=cost(1e8),
    )(gate_pre, lru_out)


def scan_rows(drive_ref, rate_ref, start, visit):
    carry = start
    for tile in reversed(range(TOK // 8)):
        rows = slice(tile * 8, tile * 8 + 8)
        drive, rate = drive_ref[rows, :], rate_ref[rows, :]
        here, later = [None] * 8, [None] * 8
        for r in reversed(range(8)):
            here[r] = drive[r : r + 1] + carry
            carry = rate[r : r + 1] * here[r]
            later[r] = carry
        if visit is not None:
            visit(rows, jnp.concatenate(here, axis=0), jnp.concatenate(later, axis=0))
    return carry


def drive_kernel(
    meta, own_ref, peer_ref, w_ref, gate_ref, lru_ref, decay_ref,
    dgate_ref, drive_ref, head_ref, rate_ref,
):
    tp = meta[0]
    grad = 0.0
    for ref, par in ((own_ref, tp), (peer_ref, 1 - tp)):
        for j in range(4):
            grad += dot_cols(ref[:, j * BLK : (j + 1) * BLK], w_ref[:, lanes(2 * j + par)])
    x = gate_ref[...].astype(F32)
    value, t = gelu_parts(x)
    slope = 0.5 * (1.0 + t) + 0.5 * x * (1.0 - t * t) * (ROOT * (1.0 + 3.0 * CUBE * x * x))
    dgate_ref[...] = (grad * lru_ref[...].astype(F32) * slope).astype(BF)
    drive_ref[...] = grad * value
    rate_ref[...] = jnp.exp(decay_ref[...])
    head_ref[0:8, :] = tile_of(scan_rows(drive_ref, rate_ref, jnp.zeros((1, HALF), F32), None))
    head_ref[8:16, :] = tile_of(jnp.exp(jnp.sum(decay_ref[...], axis=0, keepdims=True)))


def drive(meta, own, peer, w_out, gate_pre, lru_out, log_decay):
    return pl.pallas_call(
        drive_kernel,
        name="drive",
        in_specs=whole(6),
        out_specs=[pl.BlockSpec(memory_space=pltpu.VMEM)] * 4,
        out_shape=[
            jax.ShapeDtypeStruct((TOK, HALF), BF),
            jax.ShapeDtypeStruct((TOK, HALF), F32),
            jax.ShapeDtypeStruct((16, 128), F32),
            jax.ShapeDtypeStruct((TOK, HALF), F32),
        ],
        compiler_params=vm(16),
        cost_estimate=cost(2e9),
    )(meta, own, peer, w_out, gate_pre, lru_out, log_decay)


def level_kernel(place, h0, h1, h2, h3, total_ref, rest_ref, line):
    for k, ref in enumerate((h0, h1, h2, h3)):
        line[lax.rem(place[0] + k, 4), :, :] = ref[...]
    total = within = jnp.zeros((8, 128), F32)
    product = after = jnp.ones((8, 128), F32)
    for r in reversed(range(4)):
        head, block = line[r, 0:8, :], line[r, 8:16, :]
        total = head + block * total
        product = block * product
        later = place[0] < r
        within = jnp.where(later, total, within)
        after = jnp.where(later, product, after)
    total_ref[0:8, :] = total
    total_ref[8:16, :] = product
    rest_ref[0:8, :] = within
    rest_ref[8:16, :] = after


def level(pair, axis):
    place = lax.axis_index(axis).astype(jnp.int32).reshape(1)
    others = [
        lax.ppermute(pair, axis, [(s, (s - k) % 4) for s in range(4)]) for k in (1, 2, 3)
    ]
    return pl.pallas_call(
        level_kernel,
        in_specs=whole(4),
        out_specs=[pl.BlockSpec(memory_space=pltpu.VMEM)] * 2,
        out_shape=[jax.ShapeDtypeStruct((16, 128), F32)] * 2,
        scratch_shapes=[pltpu.VMEM((4, 16, 128), F32)],
        compiler_params=vm(4),
        cost_estimate=cost(1e7),
    )(place, pair, *others)


def finish_kernel(
    rx, ry, rz, drive_ref, rate_ref, lru_ref, before_ref, dd_ref, dl_ref, prev_ref
):
    inner = ry[0:8, :] + ry[8:16, :] * rz[0:8, :]
    carry = line_of(rx[0:8, :] + rx[8:16, :] * inner)
    state = lru_ref[...].astype(F32)
    first = lax.broadcasted_iota(jnp.int32, (TOK, HALF), 0) == 0
    prev_ref[...] = jnp.where(first, before_ref[...].astype(F32), pltpu.roll(state, 1, 0))

    def visit(rows, here, later):
        dd_ref[rows, :] = here
        dl_ref[rows, :] = later * prev_ref[rows, :]

    scan_rows(drive_ref, rate_ref, carry, visit)


def finish(rests, drive_value, rate, lru_out, before):
    return pl.pallas_call(
        finish_kernel,
        name="finish",
        out_shape=[jax.ShapeDtypeStruct((TOK, HALF), F32)] * 2,
        scratch_shapes=[pltpu.VMEM((TOK, HALF), F32)],
        compiler_params=vm(8),
        cost_estimate=cost(1e9),
    )(*rests, drive_value, rate, lru_out, before)


def outer_kernel(meta, *refs):
    own, peer, gated = refs[0:4], refs[4:8], refs[8:12]
    out_ref = refs[12]
    tp, z = meta[0], meta[1]
    total_own = dot_rows(own[0][...], gated[0][...])
    total_peer = dot_rows(peer[0][:, lanes(z)], gated[0][...])
    for k in range(1, 4):
        total_own += dot_rows(own[k][...], gated[k][...])
        total_peer += dot_rows(peer[k][...], gated[k][...])
    out_ref[lanes(tp), :] = total_own.astype(BF)
    out_ref[lanes(1 - tp), :] = total_peer.astype(BF)


def outer(meta, own, peer, gated):
    return pl.pallas_call(
        outer_kernel,
        name="outer",
        in_specs=whole(12),
        out_specs=pl.BlockSpec(memory_space=pltpu.VMEM),
        out_shape=jax.ShapeDtypeStruct((2 * BLK, HALF), BF),
        compiler_params=vm(12),
        cost_estimate=cost(2e9),
    )(meta, *own, *peer, *gated)


def swapped(value):
    return lax.ppermute(value, "tp", [(0, 1), (1, 0)])


def turned(value, steps):
    return lax.ppermute(value, "z", [(s, (s + steps) % 4) for s in range(4)])


def on_device(
    stream_mid, d_out, route_ids, route_weights, gate_pre, lru_out, log_decay, w_out,
    exp_gate, exp_up, exp_down,
):
    meta = jnp.stack(
        [lax.axis_index("tp"), lax.axis_index("z"), lax.axis_index(SP), lax.axis_index(("y", "x"))]
    ).astype(jnp.int32)
    perm, perm_t = jnp.asarray(_perm, BF), jnp.asarray(_perm.T, BF)
    ids = route_ids.T
    wg, wu, wd = exp_gate[0], exp_up[0], exp_down[0]
    sent = pack(meta, ids, route_weights.T, stream_mid, d_out)
    got = lax.all_to_all(sent.reshape(NSP, CHUNK, HALF), SP, 0, 0, tiled=True)
    got = got.reshape(SLOTS, HALF)
    got_peer = swapped(got)
    gated, last = early(gate_pre, lru_out), lru_out[-1:]
    gated, last, got = lax.optimization_barrier((gated, last, got))
    turns = [turned(gated, k) for k in (1, 2, 3)]
    before = lax.ppermute(last, SP, [(s, s + 1) for s in range(NSP - 1)])
    pg, pu, pb = expert_own(meta, perm, got, wg, wu, wd)
    hid, gg, gu, part_peer = expert_peer(meta, perm, perm_t, got_peer, wg, wu, wd, pg, pu, pb)
    other = swapped(part_peer)
    part_own = expert_back(meta, perm_t, gg, gu, wg, wu)
    back = (part_own.astype(F32) + other.astype(F32)).astype(BF)
    back, before, *turns = lax.optimization_barrier((back, before, *turns))
    ret = lax.all_to_all(back.reshape(NSP, CHUNK, HALF // 2), SP, 0, 0, tiled=True)
    grad_gate, grad_up, grad_down = weight_grads(meta, perm, got, got_peer, hid, gg, gu)
    ret, grad_gate, grad_up, grad_down = lax.optimization_barrier(
        (ret, grad_gate, grad_up, grad_down)
    )
    dm, *blocks = combine(meta, ids, ret.reshape(SLOTS, HALF // 2), d_out)
    dm_peer = swapped(dm)
    own = (blocks[0], *(turned(blocks[k], k) for k in (1, 2, 3)))
    peer = (dm_peer, *(swapped(own[k]) for k in (1, 2, 3)))
    share = outer(meta, own, peer, (gated, *turns))
    shares = lax.all_to_all(share.reshape(16, 32, HALF), ("y", "x"), 0, 0, tiled=True)
    d_gate, drive_value, head, rate = drive(
        meta, dm, dm_peer, w_out, gate_pre, lru_out, log_decay
    )
    line, rest_x = level(head, "x")
    plane, rest_y = level(line, "y")
    _, rest_z = level(plane, "z")
    d_drive, d_log_decay = finish((rest_x, rest_y, rest_z), drive_value, rate, lru_out, before)
    grad_out_proj = jnp.sum(shares.astype(F32), axis=0)
    return (
        grad_gate[None], grad_up[None], grad_down[None], grad_out_proj, d_gate, d_drive, d_log_decay,
    )


def solution(mesh):
    fine = Mesh(mesh.devices.reshape(4, 4, 4, 2), ("z", "y", "x", "tp"))
    tokens = P(SP, None)
    both = P(SP, "tp")
    hidden = P(SP, None, "tp")
    in_specs = (
        tokens, tokens, tokens, tokens, both, both, both, P("tp", None),
        hidden, hidden, P(SP, "tp", None),
    )
    out_specs = (hidden, hidden, P(SP, "tp", None), both, both, both, both)
    return jax.shard_map(
        on_device, mesh=fine, in_specs=in_specs, out_specs=out_specs, check_vma=False
    )
```

time: 214 us -> 191 us (0.89)
  the two profiles are of different devices: /device:TPU:1 before, /device:TPU:0 now
where the time goes in v1:
time: 191 us; the launch traced here: 190 us
  blocking collectives  52.9 us (28%)
  Pallas kernels  43 us (23%)
  waiting for transfers between devices  39.5 us (21%)
  starting transfers between devices  31.6 us (17%)
  local copies, waits for them, and re-layouts  19.4 us (10%)
  other arithmetic  2.55 us (1%)
    all_to_all x1, blocking collectives, on_device(): got = lax.all_to_all(sent.reshape(NSP, CHUNK, HALF), SP, 0, 0, tiled=True)  52.9 us
    unnamed x66, local copies, waits for them, and re-layouts  19.4 us
    ppermute x6, waiting for transfers between devices, turned(): return lax.ppermute(value, 'z', [(s, (s + steps) % 4) for s in range(4)])  16 us
    ppermute x9, waiting for transfers between devices, level(): lax.ppermute(pair, axis, [(s, (s - k) % 4) for s in range(4)])  14.2 us
    ppermute x9, starting transfers between devices, level(): lax.ppermute(pair, axis, [(s, (s - k) % 4) for s in range(4)])  12.1 us
    pallas_call x1, Pallas kernels, weight_grads(): pl.pallas_call(weight_kernel, name='weight_grads', grid_spec=pltpu.Prefet...  11.4 us
    all_to_all x1, waiting for transfers between devices, on_device(): lax.all_to_all(back.reshape(NSP, CHUNK, HALF // 2), SP, 0, 0, tiled=True)  6.76 us
    ppermute x6, starting transfers between devices, turned(): return lax.ppermute(value, 'z', [(s, (s + steps) % 4) for s in range(4)])  6.75 us
  transfers between devices with their start and end apart: 24, of which 14 were waited for; matrix products, arithmetic and copies ran while one was open for 1% of the time, Pallas kernels for 13%

profile of v1, /device:TPU:0, one launch (start us, length us, event | category | flops | bytes accessed | tf_op | source)
XLA Modules:
  0.0 190.0 jit_solution(4533100565304517487)
XLA Ops:
  0.7 1.1 copy-done
  1.9 1.1 copy-done.1
  4.4 6.0 %pack.1 = bf16[1536,1024]{1,0:T(8,128)(2,1)S(1)} custom-call(s32[4]{0:T(128)S(1)} %pad_add_fusion.meta, s32[2,192]{1,0:T(2,128)S(1)} %bitcast.24, f32[2,192]{1,0:T(2,128)S(1)} %bitcast.23, bf16[192,2048]{1,0:T(8,128)(2,1)S(1)} %copy-done, bf16[192,2048]{1,0:T(8,128)(2,1)S(1)} %copy-done.1), custom_call_target="tpu_custom_call" | custom-call | tf_op jit(solution)/shard_map/pack/pallas_call | solution.py:99
  10.4 52.9 %all_to_all.15 = bf16[64,24,1024]{2,1,0:T(8,128)(2,1)S(1)} all-to-all(bf16[64,24,1024]{2,1,0:T(8,128)(2,1)S(1)} %bitcast.19), channel_id=1, replica_groups=mesh['z'=4,'y'=4,'x'=4,'tp'=2] {'z','y','x'}, dimensions={0} | all-to-all | bytes 6291456 | tf_op jit(solution)/shard_map/all_to_all | solution.py:487
  63.8 4.0 %expert_own.1 = (f32[768,512]{1,0:T(8,128)S(1)}, f32[768,512]{1,0:T(8,128)S(1)}, f32[768,512]{1,0:T(8,128)S(1)}) custom-call(s32[4]{0:T(128)S(1)} %pad_add_fusion.meta, bf16[192,192]{1,0:T(8,128)(2,1)S(1)} %copy-done.24, bf16[1536,1024]{1,0:T(8,128)(2,1)S(1)} %bitcast.21, bf16[2048,512]{1,0:T(8,128)(2,1)S(1)} %bitcast.28, bf16[2048,512]{1,0:T(8,128)(2,1)S(1)} %bitcast.31, ...), custom_call_target="tpu_custom_call" | custom-call | flops 4000000000 | tf_op jit(solution)/shard_map/expert_own/pallas_call | solution.py:157
  67.7 1.3 collective-permute-done.peer_ref
  69.0 6.7 %expert_peer.1 = (bf16[768,512]{1,0:T(8,128)(2,1)S(1)}, bf16[768,512]{1,0:T(8,128)(2,1)S(1)}, bf16[768,512]{1,0:T(8,128)(2,1)S(1)}, bf16[1536,512]{1,0:T(8,128)(2,1)S(1)}) custom-call(s32[4]{0:T(128)S(1)} %pad_add_fusion.meta, bf16[192,192]{1,0:T(8,128)(2,1)S(1)} %copy-done.24, bf16[192,192]{1,0:T(8,128)(2,1)S(1)} %copy-done.26, ...), custom_call_target="tpu_custom_call" | custom-call | flops 6000000000 | tf_op jit(solution)/shard_map/expert_peer/pallas_call | solution.py:188
  76.5 1.9 collective-permute-start.4
  78.4 1.0 collective-permute-start.5
  79.4 2.5 %collective-permute-start.2 = (bf16[1,1024]{1,0:T(2,128)(2,1)S(1)}, bf16[1,1024]{1,0:T(2,128)(2,1)S(1)}, u32[]{:S(2)}, u32[]{:S(2)}) collective-permute-start(bf16[1,1024]{1,0:T(2,128)(2,1)S(1)} %slice.3), channel_id=1, source_target_pairs={{0,2},{2,4},{4,6},{6,8},{8,10},{10,12},{12,14},{14,16},{16,18},{18... | collective-permute-start | bytes 6152 | tf_op jit(solution)/shard_map/ppermute | solution.py:493
  81.9 2.8 %expert_back.1 = bf16[1536,512]{1,0:T(8,128)(2,1)S(1)} custom-call(s32[4]{0:T(128)S(1)} %pad_add_fusion.meta, bf16[192,192]{1,0:T(8,128)(2,1)S(1)} %copy-done.26, bf16[768,512]{1,0:T(8,128)(2,1)S(1)} %get-tuple-element.49.gg_ref, bf16[768,512]{1,0:T(8,128)(2,1)S(1)} %get-tuple-element.50.gu_ref, bf16[2048,512]{1,0:T(8,128)(2,1)S(1)} %bitcast.30, ...), custom_call_target="tpu_custom_call" | custom-call | flops 3000000000 | tf_op jit(solution)/shard_map/expert_back/pallas_call | solution.py:206
  84.7 1.6 add_convert_fusion
  86.3 10.7 %collective-permute-done.3.refs_9_ = bf16[192,1024]{1,0:T(8,128)(2,1)S(1)} collective-permute-done((bf16[192,1024]{1,0:T(8,128)(2,1)S(1)}, bf16[192,1024]{1,0:T(8,128)(2,1)S(1)}, u32[]{:S(2)}, u32[]{:S(2)}) %collective-permute-start.3) | collective-permute-done | bytes 393248 | tf_op jit(solution)/shard_map/ppermute | solution.py:473
  99.3 5.5 %all-to-all-start.1 = ((bf16[64,24,512]{2,1,0:T(8,128)(2,1)}), bf16[64,24,512]{2,1,0:T(8,128)(2,1)}, u32[]{:S(2)}, u32[]{:S(2)}) async-start(bf16[64,24,512]{2,1,0:T(8,128)(2,1)} %bitcast.34), calls=%async_computation.1 | async-start | bytes 3145728 | tf_op jit(solution)/shard_map/all_to_all | solution.py:500
  104.8 1.9 copy-done.13
  106.7 0.9 copy-done.25
  107.6 1.1 copy-done.28
  108.7 1.1 copy-done.30
  109.8 1.1 copy-done.32
  111.0 11.4 %weight_grads.1 = (f32[2048,512]{1,0:T(8,128)}, f32[2048,512]{1,0:T(8,128)}, f32[512,2048]{1,0:T(8,128)}) custom-call(s32[4]{0:T(128)S(1)} %pad_add_fusion.meta, bf16[192,192]{1,0:T(8,128)(2,1)S(1)} %copy-done.25, bf16[1536,1024]{1,0:T(8,128)(2,1)S(1)} %bitcast.22, bf16[1536,1024]{1,0:T(8,128)(2,1)S(1)} %copy-done.13, bf16[768,512]{1,0:T(8,128)(2,1)S(1)} %copy-done.32, ...), custom_call_target="tpu_custom_call" | custom-call | flops 4831838208 | bytes 20000000 | tf_op jit(solution)/shard_map/weight_grads/pallas_call | solution.py:237
  122.4 6.8 %all-to-all-done.1 = bf16[64,24,512]{2,1,0:T(8,128)(2,1)} async-done(((bf16[64,24,512]{2,1,0:T(8,128)(2,1)}), bf16[64,24,512]{2,1,0:T(8,128)(2,1)}, u32[]{:S(2)}, u32[]{:S(2)}) %all-to-all-start.1) | async-done | bytes 1572896 | tf_op jit(solution)/shard_map/all_to_all | solution.py:500
  129.1 1.1 copy-done.2
  130.3 2.5 %combine.1 = (bf16[192,1024]{1,0:T(8,128)(2,1)S(1)}, bf16[192,256]{1,0:T(8,128)(2,1)S(1)}, bf16[192,256]{1,0:T(8,128)(2,1)S(1)}, bf16[192,256]{1,0:T(8,128)(2,1)S(1)}, bf16[192,256]{1,0:T(8,128)(2,1)S(1)}) custom-call(s32[4]{0:T(128)S(1)} %pad_add_fusion.meta, s32[2,192]{1,0:T(2,128)S(1)} %bitcast.25, bf16[1536,512]{1,0:T(8,128)(2,1)} %bitcast.15.ret_ref, ...), custom_call_target="tpu_custom_call" | custom-call | flops 1000000000 | tf_op jit(solution)/shard_map/combine/pallas_call | solution.py:287
  133.3 1.9 collective-permute-start.7
  135.2 1.1 collective-permute-start.8
  136.2 5.2 %collective-permute-done.6.refs_1_ = bf16[192,256]{1,0:T(8,128)(2,1)S(1)} collective-permute-done((bf16[192,256]{1,0:T(8,128)(2,1)S(1)}, bf16[192,256]{1,0:T(8,128)(2,1)S(1)}, u32[]{:S(2)}, u32[]{:S(2)}) %collective-permute-start.6) | collective-permute-done | bytes 98336 | tf_op jit(solution)/shard_map/ppermute | solution.py:473
  143.3 1.0 copy-done.7
  144.3 1.0 copy-done.19
  145.3 1.0 copy-done.21
  146.3 1.0 copy-done.23
  147.3 2.8 %outer.1 = bf16[512,1024]{1,0:T(8,128)(2,1)} custom-call(s32[4]{0:T(128)S(1)} %pad_add_fusion.meta, bf16[192,256]{1,0:T(8,128)(2,1)S(1)} %get-tuple-element.63.refs_0_, bf16[192,256]{1,0:T(8,128)(2,1)S(1)} %collective-permute-done.6.refs_1_, bf16[192,256]{1,0:T(8,128)(2,1)S(1)} %collective-permute-done.7.refs_2_, ...), custom_call_target="tpu_custom_call" | custom-call | flops 2000000000 | tf_op jit(solution)/shard_map/outer/pallas_call | solution.py:457
  150.2 4.0 %all-to-all-start.2 = ((bf16[16,32,1024]{2,1,0:T(8,128)(2,1)}), bf16[16,32,1024]{2,1,0:T(8,128)(2,1)S(1)}, u32[]{:S(2)}, u32[]{:S(2)}) async-start(bf16[16,32,1024]{2,1,0:T(8,128)(2,1)} %bitcast.16), calls=%async_computation.2 | async-start | bytes 2097152 | tf_op jit(solution)/shard_map/all_to_all | solution.py:510
  154.2 2.2 %copy-done.11 = bf16[1024,2048]{1,0:T(8,128)(2,1)S(1)} copy-done((bf16[1024,2048]{1,0:T(8,128)(2,1)S(1)}, bf16[1024,2048]{1,0:T(8,128)(2,1)}, u32[]{:S(2)}) %copy-start.11) | copy-done | bytes 4194328
  156.4 3.6 %drive.1 = (bf16[192,1024]{1,0:T(8,128)(2,1)}, f32[192,1024]{1,0:T(8,128)S(1)}, f32[16,128]{1,0:T(8,128)S(1)}, f32[192,1024]{1,0:T(8,128)S(1)}) custom-call(s32[4]{0:T(128)S(1)} %pad_add_fusion.meta, bf16[192,1024]{1,0:T(8,128)(2,1)S(1)} %get-tuple-element.67.own_ref, bf16[192,1024]{1,0:T(8,128)(2,1)S(1)} %collective-permute-done.9.refs_4_.peer_ref, ...), custom_call_target="tpu_custom_call" | custom-call | flops 2000000000 | tf_op jit(solution)/shard_map/drive/pallas_call | solution.py:366
  160.0 2.8 %collective-permute-start.13 = (f32[16,128]{1,0:T(8,128)S(1)}, f32[16,128]{1,0:T(8,128)S(1)}, u32[]{:S(2)}, u32[]{:S(2)}) collective-permute-start(f32[16,128]{1,0:T(8,128)S(1)} %get-tuple-element.72.h0), channel_id=1, source_target_pairs={{0,6},{2,0},{4,2},{6,4},{1,7},{3,1},{5,3},{7,5},{8,14},{10,8},{12,... | collective-permute-start | bytes 24584 | tf_op jit(solution)/shard_map/ppermute | solution.py:403
  162.8 0.8 collective-permute-start.14
  163.6 0.9 collective-permute-start.15
  164.5 3.8 %collective-permute-done.13.h1 = f32[16,128]{1,0:T(8,128)S(1)} collective-permute-done((f32[16,128]{1,0:T(8,128)S(1)}, f32[16,128]{1,0:T(8,128)S(1)}, u32[]{:S(2)}, u32[]{:S(2)}) %collective-permute-start.13) | collective-permute-done | bytes 8224 | tf_op jit(solution)/shard_map/ppermute | solution.py:403
  168.3 2.1 %collective-permute-done.14.h2 = f32[16,128]{1,0:T(8,128)S(1)} collective-permute-done((f32[16,128]{1,0:T(8,128)S(1)}, f32[16,128]{1,0:T(8,128)S(1)}, u32[]{:S(2)}, u32[]{:S(2)}) %collective-permute-start.14) | collective-permute-done | bytes 8224 | tf_op jit(solution)/shard_map/ppermute | solution.py:403
  170.4 2.6 %collective-permute-start.16 = (f32[16,128]{1,0:T(8,128)S(1)}, f32[16,128]{1,0:T(8,128)S(1)}, u32[]{:S(2)}, u32[]{:S(2)}) collective-permute-start(f32[16,128]{1,0:T(8,128)S(1)} %get-tuple-element.74.h0), channel_id=1, source_target_pairs={{0,24},{8,0},{16,8},{24,16},{1,25},{9,1},{17,9},{25,17},{2,26},{10... | collective-permute-start | bytes 24584 | tf_op jit(solution)/shard_map/ppermute | solution.py:403
  173.0 0.8 collective-permute-start.17
  173.8 0.8 collective-permute-start.18
  174.6 3.6 %collective-permute-done.17.h2 = f32[16,128]{1,0:T(8,128)S(1)} collective-permute-done((f32[16,128]{1,0:T(8,128)S(1)}, f32[16,128]{1,0:T(8,128)S(1)}, u32[]{:S(2)}, u32[]{:S(2)}) %collective-permute-start.17) | collective-permute-done | bytes 8224 | tf_op jit(solution)/shard_map/ppermute | solution.py:403
  178.7 2.4 %collective-permute-start.19 = (f32[16,128]{1,0:T(8,128)S(1)}, f32[16,128]{1,0:T(8,128)S(1)}, u32[]{:S(2)}, u32[]{:S(2)}) collective-permute-start(f32[16,128]{1,0:T(8,128)S(1)} %get-tuple-element.76.h0), channel_id=1, source_target_pairs={{0,96},{32,0},{64,32},{96,64},{1,97},{33,1},{65,33},{97,65},{2,98}... | collective-permute-start | bytes 24584 | tf_op jit(solution)/shard_map/ppermute | solution.py:403
  181.1 0.9 collective-permute-start.21
  182.5 3.8 %collective-permute-done.20.h2 = f32[16,128]{1,0:T(8,128)S(1)} collective-permute-done((f32[16,128]{1,0:T(8,128)S(1)}, f32[16,128]{1,0:T(8,128)S(1)}, u32[]{:S(2)}, u32[]{:S(2)}) %collective-permute-start.20) | collective-permute-done | bytes 8224 | tf_op jit(solution)/shard_map/ppermute | solution.py:403
  186.9 2.3 %finish.1 = (f32[192,1024]{1,0:T(8,128)}, f32[192,1024]{1,0:T(8,128)}) custom-call(f32[16,128]{1,0:T(8,128)S(1)} %get-tuple-element.73.rx, f32[16,128]{1,0:T(8,128)S(1)} %get-tuple-element.75.ry, f32[16,128]{1,0:T(8,128)S(1)} %get-tuple-element.77.rz, f32[192,1024]{1,0:T(8,128)S(1)} %get-tuple-element.78.drive_ref, ...), custom_call_target="tpu_custom_call" | custom-call | flops 1000000000 | tf_op jit(solution)/shard_map/finish/pallas_call | solution.py:433
  189.2 0.8 convert_reduce_fusion
  (84 shorter events, 8.9 us)
Async XLA Ops:
  0.7 1.1 copy-start
  1.9 1.1 copy-start.1
  10.3 53.0 %copy-start.3 = (bf16[192,1024]{1,0:T(8,128)(2,1)S(1)}, bf16[192,1024]{1,0:T(8,128)(2,1)}, u32[]{:S(2)}) copy-start(bf16[192,1024]{1,0:T(8,128)(2,1)} %lru_ref.5) | copy-start | bytes 1179652
  10.3 53.0 %copy-start.4 = (bf16[192,1024]{1,0:T(8,128)(2,1)S(1)}, bf16[192,1024]{1,0:T(8,128)(2,1)}, u32[]{:S(2)}) copy-start(bf16[192,1024]{1,0:T(8,128)(2,1)} %gate_ref.3) | copy-start | bytes 1179652
  10.3 53.4 %copy-start.14 = (bf16[1,512,2048]{2,1,0:T(8,128)(2,1)S(1)}, bf16[1,512,2048]{2,1,0:T(8,128)(2,1)}, u32[]{:S(2)}) copy-start(bf16[1,512,2048]{2,1,0:T(8,128)(2,1)} %param.23) | copy-start | bytes 6291460
  10.4 53.4 %copy-start.15 = (bf16[1,2048,512]{2,1,0:T(8,128)(2,1)S(1)}, bf16[1,2048,512]{2,1,0:T(8,128)(2,1)}, u32[]{:S(2)}) copy-start(bf16[1,2048,512]{2,1,0:T(8,128)(2,1)} %param.21) | copy-start | bytes 6291460
  10.4 53.4 %copy-start.16 = (bf16[1,2048,512]{2,1,0:T(8,128)(2,1)S(1)}, bf16[1,2048,512]{2,1,0:T(8,128)(2,1)}, u32[]{:S(2)}) copy-start(bf16[1,2048,512]{2,1,0:T(8,128)(2,1)} %param.22) | copy-start | bytes 6291460
  10.4 53.4 %copy-start.24 = (bf16[192,192]{1,0:T(8,128)(2,1)S(1)}, bf16[192,192]{1,0:T(8,128)(2,1)}, u32[]{:S(2)}) copy-start(bf16[192,192]{1,0:T(8,128)(2,1)} %constant.25.clone.perm_ref) | copy-start | bytes 221188
  63.3 5.7 %collective-permute-start = (bf16[1536,1024]{1,0:T(8,128)(2,1)S(1)}, bf16[1536,1024]{1,0:T(8,128)(2,1)S(1)}, u32[]{:S(2)}, u32[]{:S(2)}) collective-permute-start(bf16[1536,1024]{1,0:T(8,128)(2,1)S(1)} %bitcast.20), channel_id=1, source_target_pairs={{0,1},{1,0},{2,3},{3,2},{4,5},{5,4},{6,7},{7,6},{8,9},{9,8},{10,11... | collective-permute-start | bytes 9437192 | tf_op jit(solution)/shard_map/ppermute | solution.py:469
  63.7 14.7 %copy-start.6 = (bf16[192,1024]{1,0:T(8,128)(2,1)}, bf16[192,1024]{1,0:T(8,128)(2,1)S(1)}, u32[]{:S(2)}) copy-start(bf16[192,1024]{1,0:T(8,128)(2,1)S(1)} %early.1.refs_8_) | copy-start | bytes 1179652
  63.8 5.3 %copy-start.26 = (bf16[192,192]{1,0:T(8,128)(2,1)S(1)}, bf16[192,192]{1,0:T(8,128)(2,1)}, u32[]{:S(2)}) copy-start(bf16[192,192]{1,0:T(8,128)(2,1)} %constant.26.clone.perm_t_ref) | copy-start | bytes 221188
  69.0 6.7 %copy-start.12 = (bf16[1536,1024]{1,0:T(8,128)(2,1)}, bf16[1536,1024]{1,0:T(8,128)(2,1)S(1)}, u32[]{:S(2)}) copy-start(bf16[1536,1024]{1,0:T(8,128)(2,1)S(1)} %collective-permute-done.peer_ref) | copy-start | bytes 9437188
  75.7 8.9 %copy-start.27 = (bf16[768,512]{1,0:T(8,128)(2,1)}, bf16[768,512]{1,0:T(8,128)(2,1)S(1)}, u32[]{:S(2)}) copy-start(bf16[768,512]{1,0:T(8,128)(2,1)S(1)} %get-tuple-element.49.gg_ref) | copy-start | bytes 2359300
  75.8 8.9 %copy-start.29 = (bf16[768,512]{1,0:T(8,128)(2,1)}, bf16[768,512]{1,0:T(8,128)(2,1)S(1)}, u32[]{:S(2)}) copy-start(bf16[768,512]{1,0:T(8,128)(2,1)S(1)} %get-tuple-element.50.gu_ref) | copy-start | bytes 2359300
  75.8 8.9 %copy-start.31 = (bf16[768,512]{1,0:T(8,128)(2,1)}, bf16[768,512]{1,0:T(8,128)(2,1)S(1)}, u32[]{:S(2)}) copy-start(bf16[768,512]{1,0:T(8,128)(2,1)S(1)} %get-tuple-element.55.hid_ref) | copy-start | bytes 2359300
  75.8 8.9 %collective-permute-start.1 = (bf16[1536,512]{1,0:T(8,128)(2,1)S(1)}, bf16[1536,512]{1,0:T(8,128)(2,1)S(1)}, u32[]{:S(2)}, u32[]{:S(2)}) collective-permute-start(bf16[1536,512]{1,0:T(8,128)(2,1)S(1)} %get-tuple-element.51), channel_id=1, source_target_pairs={{0,1},{1,0},{2,3},{3,2},{4,5},{5,4},{6,7},{7,6},{8,9},{9,8},{10,11... | collective-permute-start | bytes 4718600 | tf_op jit(solution)/shard_map/ppermute | solution.py:469
  76.0 21.0 %collective-permute-start.3 = (bf16[192,1024]{1,0:T(8,128)(2,1)S(1)}, bf16[192,1024]{1,0:T(8,128)(2,1)S(1)}, u32[]{:S(2)}, u32[]{:S(2)}) collective-permute-start(bf16[192,1024]{1,0:T(8,128)(2,1)S(1)} %early.1.refs_8_), channel_id=1, source_target_pairs={{0,32},{32,64},{64,96},{96,0},{1,33},{33,65},{65,97},{97,1},{2,34}... | collective-permute-start | bytes 1179656 | tf_op jit(solution)/shard_map/ppermute | solution.py:473
  76.5 21.2 %collective-permute-start.4 = (bf16[192,1024]{1,0:T(8,128)(2,1)S(1)}, bf16[192,1024]{1,0:T(8,128)(2,1)S(1)}, u32[]{:S(2)}, u32[]{:S(2)}) collective-permute-start(bf16[192,1024]{1,0:T(8,128)(2,1)S(1)} %early.1.refs_8_), channel_id=1, source_target_pairs={{0,64},{32,96},{64,0},{96,32},{1,65},{33,97},{65,1},{97,33},{2,66}... | collective-permute-start | bytes 1179656 | tf_op jit(solution)/shard_map/ppermute | solution.py:473
  78.4 20.1 %collective-permute-start.5 = (bf16[192,1024]{1,0:T(8,128)(2,1)S(1)}, bf16[192,1024]{1,0:T(8,128)(2,1)S(1)}, u32[]{:S(2)}, u32[]{:S(2)}) collective-permute-start(bf16[192,1024]{1,0:T(8,128)(2,1)S(1)} %early.1.refs_8_), channel_id=1, source_target_pairs={{0,96},{32,0},{64,32},{96,64},{1,97},{33,1},{65,33},{97,65},{2,98}... | collective-permute-start | bytes 1179656 | tf_op jit(solution)/shard_map/ppermute | solution.py:473
  79.4 6.9 %collective-permute-start.2 = (bf16[1,1024]{1,0:T(2,128)(2,1)S(1)}, bf16[1,1024]{1,0:T(2,128)(2,1)S(1)}, u32[]{:S(2)}, u32[]{:S(2)}) collective-permute-start(bf16[1,1024]{1,0:T(2,128)(2,1)S(1)} %slice.3), channel_id=1, source_target_pairs={{0,2},{2,4},{4,6},{6,8},{8,10},{10,12},{12,14},{14,16},{16,18},{18... | collective-permute-start | bytes 6152 | tf_op jit(solution)/shard_map/ppermute | solution.py:493
  99.3 29.9 %all-to-all-start.1 = ((bf16[64,24,512]{2,1,0:T(8,128)(2,1)}), bf16[64,24,512]{2,1,0:T(8,128)(2,1)}, u32[]{:S(2)}, u32[]{:S(2)}) async-start(bf16[64,24,512]{2,1,0:T(8,128)(2,1)} %bitcast.34), calls=%async_computation.1 | async-start | bytes 3145728 | tf_op jit(solution)/shard_map/all_to_all | solution.py:500
  104.8 1.9 copy-start.13
  107.6 1.1 copy-start.28
  108.7 1.1 copy-start.30
  109.8 1.1 copy-start.32
  111.0 18.2 %copy-start.10 = (s32[192,2]{0,1:T(2,128)S(1)}, s32[192,2]{0,1:T(2,128)}, u32[]{:S(2)}) copy-start(s32[192,2]{0,1:T(2,128)} %param.15) | copy-start | bytes 4612
  129.1 1.1 copy-start.2
  132.8 10.5 %collective-permute-start.9 = (bf16[192,1024]{1,0:T(8,128)(2,1)S(1)}, bf16[192,1024]{1,0:T(8,128)(2,1)S(1)}, u32[]{:S(2)}, u32[]{:S(2)}) collective-permute-start(bf16[192,1024]{1,0:T(8,128)(2,1)S(1)} %get-tuple-element.67.own_ref), channel_id=1, source_target_pairs={{0,1},{1,0},{2,3},{3,2},{4,5},{5,4},{6,7},{7,6},{8,9},{9,8},{10,11... | collective-permute-start | bytes 1179656 | tf_op jit(solution)/shard_map/ppermute | solution.py:469
  132.9 8.5 %collective-permute-start.6 = (bf16[192,256]{1,0:T(8,128)(2,1)S(1)}, bf16[192,256]{1,0:T(8,128)(2,1)S(1)}, u32[]{:S(2)}, u32[]{:S(2)}) collective-permute-start(bf16[192,256]{1,0:T(8,128)(2,1)S(1)} %get-tuple-element.64), channel_id=1, source_target_pairs={{0,32},{32,64},{64,96},{96,0},{1,33},{33,65},{65,97},{97,1},{2,34}... | collective-permute-start | bytes 294920 | tf_op jit(solution)/shard_map/ppermute | solution.py:473
  133.3 8.1 %collective-permute-start.7 = (bf16[192,256]{1,0:T(8,128)(2,1)S(1)}, bf16[192,256]{1,0:T(8,128)(2,1)S(1)}, u32[]{:S(2)}, u32[]{:S(2)}) collective-permute-start(bf16[192,256]{1,0:T(8,128)(2,1)S(1)} %get-tuple-element.65), channel_id=1, source_target_pairs={{0,64},{32,96},{64,0},{96,32},{1,65},{33,97},{65,1},{97,33},{2,66}... | collective-permute-start | bytes 294920 | tf_op jit(solution)/shard_map/ppermute | solution.py:473
  135.2 6.9 %collective-permute-start.8 = (bf16[192,256]{1,0:T(8,128)(2,1)S(1)}, bf16[192,256]{1,0:T(8,128)(2,1)S(1)}, u32[]{:S(2)}, u32[]{:S(2)}) collective-permute-start(bf16[192,256]{1,0:T(8,128)(2,1)S(1)} %get-tuple-element.66), channel_id=1, source_target_pairs={{0,96},{32,0},{64,32},{96,64},{1,97},{33,1},{65,33},{97,65},{2,98}... | collective-permute-start | bytes 294920 | tf_op jit(solution)/shard_map/ppermute | solution.py:473
  141.4 1.3 collective-permute-start.10
  141.4 1.5 collective-permute-start.11
  142.0 1.3 collective-permute-start.12
  143.3 1.0 copy-start.7
  150.1 4.0 %copy-start.5 = (bf16[192,1024]{1,0:T(8,128)(2,1)S(1)}, bf16[192,1024]{1,0:T(8,128)(2,1)}, u32[]{:S(2)}) copy-start(bf16[192,1024]{1,0:T(8,128)(2,1)} %gate_ref.3) | copy-start | bytes 1179652
  150.1 4.0 %copy-start.17 = (f32[192,1024]{1,0:T(8,128)S(1)}, f32[192,1024]{1,0:T(8,128)}, u32[]{:S(2)}) copy-start(f32[192,1024]{1,0:T(8,128)} %decay_ref.1) | copy-start | bytes 2359300
  150.2 39.0 %all-to-all-start.2 = ((bf16[16,32,1024]{2,1,0:T(8,128)(2,1)}), bf16[16,32,1024]{2,1,0:T(8,128)(2,1)S(1)}, u32[]{:S(2)}, u32[]{:S(2)}) async-start(bf16[16,32,1024]{2,1,0:T(8,128)(2,1)} %bitcast.16), calls=%async_computation.2 | async-start | bytes 2097152 | tf_op jit(solution)/shard_map/all_to_all | solution.py:510
  154.2 2.2 %copy-start.11 = (bf16[1024,2048]{1,0:T(8,128)(2,1)S(1)}, bf16[1024,2048]{1,0:T(8,128)(2,1)}, u32[]{:S(2)}) copy-start(bf16[1024,2048]{1,0:T(8,128)(2,1)} %w_ref.1) | copy-start | bytes 12582916
  160.0 8.3 %collective-permute-start.13 = (f32[16,128]{1,0:T(8,128)S(1)}, f32[16,128]{1,0:T(8,128)S(1)}, u32[]{:S(2)}, u32[]{:S(2)}) collective-permute-start(f32[16,128]{1,0:T(8,128)S(1)} %get-tuple-element.72.h0), channel_id=1, source_target_pairs={{0,6},{2,0},{4,2},{6,4},{1,7},{3,1},{5,3},{7,5},{8,14},{10,8},{12,... | collective-permute-start | bytes 24584 | tf_op jit(solution)/shard_map/ppermute | solution.py:403
  162.8 7.6 %collective-permute-start.14 = (f32[16,128]{1,0:T(8,128)S(1)}, f32[16,128]{1,0:T(8,128)S(1)}, u32[]{:S(2)}, u32[]{:S(2)}) collective-permute-start(f32[16,128]{1,0:T(8,128)S(1)} %get-tuple-element.72.h0), channel_id=1, source_target_pairs={{0,4},{2,6},{4,0},{6,2},{1,5},{3,7},{5,1},{7,3},{8,12},{10,14},{12... | collective-permute-start | bytes 24584 | tf_op jit(solution)/shard_map/ppermute | solution.py:403
  163.6 6.7 %collective-permute-start.15 = (f32[16,128]{1,0:T(8,128)S(1)}, f32[16,128]{1,0:T(8,128)S(1)}, u32[]{:S(2)}, u32[]{:S(2)}) collective-permute-start(f32[16,128]{1,0:T(8,128)S(1)} %get-tuple-element.72.h0), channel_id=1, source_target_pairs={{0,2},{2,4},{4,6},{6,0},{1,3},{3,5},{5,7},{7,1},{8,10},{10,12},{12... | collective-permute-start | bytes 24584 | tf_op jit(solution)/shard_map/ppermute | solution.py:403
  170.4 4.2 %collective-permute-start.16 = (f32[16,128]{1,0:T(8,128)S(1)}, f32[16,128]{1,0:T(8,128)S(1)}, u32[]{:S(2)}, u32[]{:S(2)}) collective-permute-start(f32[16,128]{1,0:T(8,128)S(1)} %get-tuple-element.74.h0), channel_id=1, source_target_pairs={{0,24},{8,0},{16,8},{24,16},{1,25},{9,1},{17,9},{25,17},{2,26},{10... | collective-permute-start | bytes 24584 | tf_op jit(solution)/shard_map/ppermute | solution.py:403
  173.0 5.2 %collective-permute-start.17 = (f32[16,128]{1,0:T(8,128)S(1)}, f32[16,128]{1,0:T(8,128)S(1)}, u32[]{:S(2)}, u32[]{:S(2)}) collective-permute-start(f32[16,128]{1,0:T(8,128)S(1)} %get-tuple-element.74.h0), channel_id=1, source_target_pairs={{0,16},{8,24},{16,0},{24,8},{1,17},{9,25},{17,1},{25,9},{2,18},{10... | collective-permute-start | bytes 24584 | tf_op jit(solution)/shard_map/ppermute | solution.py:403
  173.8 4.9 %collective-permute-start.18 = (f32[16,128]{1,0:T(8,128)S(1)}, f32[16,128]{1,0:T(8,128)S(1)}, u32[]{:S(2)}, u32[]{:S(2)}) collective-permute-start(f32[16,128]{1,0:T(8,128)S(1)} %get-tuple-element.74.h0), channel_id=1, source_target_pairs={{0,8},{8,16},{16,24},{24,0},{1,9},{9,17},{17,25},{25,1},{2,10},{10... | collective-permute-start | bytes 24584 | tf_op jit(solution)/shard_map/ppermute | solution.py:403
  178.7 3.8 %collective-permute-start.19 = (f32[16,128]{1,0:T(8,128)S(1)}, f32[16,128]{1,0:T(8,128)S(1)}, u32[]{:S(2)}, u32[]{:S(2)}) collective-permute-start(f32[16,128]{1,0:T(8,128)S(1)} %get-tuple-element.76.h0), channel_id=1, source_target_pairs={{0,96},{32,0},{64,32},{96,64},{1,97},{33,1},{65,33},{97,65},{2,98}... | collective-permute-start | bytes 24584 | tf_op jit(solution)/shard_map/ppermute | solution.py:403
  181.1 5.2 %collective-permute-start.20 = (f32[16,128]{1,0:T(8,128)S(1)}, f32[16,128]{1,0:T(8,128)S(1)}, u32[]{:S(2)}, u32[]{:S(2)}) collective-permute-start(f32[16,128]{1,0:T(8,128)S(1)} %get-tuple-element.76.h0), channel_id=1, source_target_pairs={{0,64},{32,96},{64,0},{96,32},{1,65},{33,97},{65,1},{97,33},{2,66}... | collective-permute-start | bytes 24584 | tf_op jit(solution)/shard_map/ppermute | solution.py:403
  181.1 5.2 %collective-permute-start.21 = (f32[16,128]{1,0:T(8,128)S(1)}, f32[16,128]{1,0:T(8,128)S(1)}, u32[]{:S(2)}, u32[]{:S(2)}) collective-permute-start(f32[16,128]{1,0:T(8,128)S(1)} %get-tuple-element.76.h0), channel_id=1, source_target_pairs={{0,32},{32,64},{64,96},{96,0},{1,33},{33,65},{65,97},{97,1},{2,34}... | collective-permute-start | bytes 24584 | tf_op jit(solution)/shard_map/ppermute | solution.py:403
  (9 other events, 7.5 us)

commit v2 on v1

--- a/solution.py
+++ b/solution.py
@@ -74,46 +74,105 @@
     return [pl.BlockSpec(memory_space=pltpu.SMEM)] + [vmem] * count
 
 
+def in_hbm(*values):
+    return [pltpu.with_memory_space_constraint(v, pltpu.HBM) for v in values]
+
+
+def mixed(*kinds):
+    spaces = {"h": pltpu.HBM, "v": pltpu.VMEM}
+    return [pl.BlockSpec(memory_space=pltpu.SMEM)] + [
+        pl.BlockSpec(memory_space=spaces[k]) for k in "".join(kinds)
+    ]
+
+
+def fetch(pairs, sems):
+    copies = [pltpu.make_async_copy(a, b, sems.at[k]) for k, (a, b) in enumerate(pairs)]
+    for copy in copies:
+        copy.start()
+    return copies
+
+
 def cost(flops, moved=0):
     return pl.CostEstimate(flops=int(flops), bytes_accessed=int(moved), transcendentals=0)
 
 
-def pack_kernel(meta, ids_ref, w_ref, x_ref, d_ref, out_ref, sx, s0, s1):
-    @pl.when(pl.program_id(0) == 0)
-    def _():
-        r0, r1 = slot_rows(ids_ref)
-        r0, r1 = r0.astype(jnp.int32), r1.astype(jnp.int32)
-        slot = lax.broadcasted_iota(jnp.int32, (SLOTS, TOK), 0)
-        sx[...] = jnp.where((slot == r0) | (slot == r1), 1.0, 0.0).astype(BF)
-        s0[...] = jnp.where(slot == r0 + CAP, 1.0, 0.0).astype(BF)
-        s1[...] = jnp.where(slot == r1 + CAP, 1.0, 0.0).astype(BF)
-
-    d = d_ref[...].astype(F32)
-    scaled0 = (as_column(w_ref[0:1, :]) * d).astype(BF)
-    scaled1 = (as_column(w_ref[1:2, :]) * d).astype(BF)
-    out = dot(sx[...], x_ref[...]) + dot(s0[...], scaled0) + dot(s1[...], scaled1)
-    out_ref[...] = out.astype(BF)
+def pack_kernel(meta, ids_hbm, w_hbm, x_hbm, d_hbm, out_ref, ids, w, xs, ds, sems):
+    tp = meta[0]
+    small = [
+        pltpu.make_async_copy(ids_hbm, ids, sems.at[0]),
+        pltpu.make_async_copy(w_hbm, w, sems.at[1]),
+    ]
+    large = []
+    for n, (src, dst) in enumerate(((x_hbm, xs), (d_hbm, ds))):
+        for j in range(4):
+            large.append(
+                pltpu.make_async_copy(
+                    src.at[:, lanes(2 * j + tp)],
+                    dst.at[:, j * BLK : (j + 1) * BLK],
+                    sems.at[2 + 4 * n + j],
+                )
+            )
+    for copy in small + large:
+        copy.start()
+    for copy in small:
+        copy.wait()
+    r0, r1 = slot_rows(ids)
+    r0, r1 = r0.astype(jnp.int32), r1.astype(jnp.int32)
+    slot = lax.broadcasted_iota(jnp.int32, (SLOTS, TOK), 0)
+    sx = jnp.where((slot == r0) | (slot == r1), 1.0, 0.0).astype(BF)
+    s0 = jnp.where(slot == r0 + CAP, 1.0, 0.0).astype(BF)
+    s1 = jnp.where(slot == r1 + CAP, 1.0, 0.0).astype(BF)
+    w0, w1 = as_column(w[0:1, :]), as_column(w[1:2, :])
+    for copy in large:
+        copy.wait()
+    for j in range(4):
+        part = slice(j * BLK, (j + 1) * BLK)
+        d = ds[:, part].astype(F32)
+        scaled0, scaled1 = (w0 * d).astype(BF), (w1 * d).astype(BF)
+        out = dot(sx, xs[:, part]) + dot(s0, scaled0) + dot(s1, scaled1)
+        out_ref[:, part] = out.astype(BF)
 
 
 def pack(meta, ids, weights, stream, d_out):
+    hbm = pl.BlockSpec(memory_space=pltpu.HBM)
     return pl.pallas_call(
         pack_kernel,
         name="pack",
-        grid_spec=pltpu.PrefetchScalarGridSpec(
-            num_scalar_prefetch=1,
-            grid=(4,),
-            in_specs=[
-                pl.BlockSpec((2, TOK), lambda j, m: (0, 0)),
-                pl.BlockSpec((2, TOK), lambda j, m: (0, 0)),
-                pl.BlockSpec((TOK, BLK), lambda j, m: (0, 2 * j + m[0])),
-                pl.BlockSpec((TOK, BLK), lambda j, m: (0, 2 * j + m[0])),
-            ],
-            out_specs=pl.BlockSpec((SLOTS, BLK), lambda j, m: (0, j)),
-            scratch_shapes=[pltpu.VMEM((SLOTS, TOK), BF)] * 3,
-        ),
+        in_specs=[pl.BlockSpec(memory_space=pltpu.SMEM)] + [hbm] * 4,
+        out_specs=pl.BlockSpec(memory_space=pltpu.VMEM),
         out_shape=jax.ShapeDtypeStruct((SLOTS, HALF), BF),
+        scratch_shapes=[
+            pltpu.VMEM((2, TOK), jnp.int32),
+            pltpu.VMEM((2, TOK), F32),
+            pltpu.VMEM((TOK, HALF), BF),
+            pltpu.VMEM((TOK, HALF), BF),
+            pltpu.SemaphoreType.DMA((10,)),
+        ],
         compiler_params=vm(12),
-    )(meta, ids, weights, stream, d_out)
+    )(meta, *in_hbm(ids, weights, stream, d_out))
+
+
+def sum_kernel(a_ref, b_ref, out_hbm, both, sems):
+    copies = []
+    for k in range(4):
+        rows = slice(k * 384, (k + 1) * 384)
+        both[rows, :] = (a_ref[rows, :].astype(F32) + b_ref[rows, :].astype(F32)).astype(BF)
+        copies.append(pltpu.make_async_copy(both.at[rows, :], out_hbm.at[rows, :], sems.at[k]))
+        copies[-1].start()
+    for copy in copies:
+        copy.wait()
+
+
+def part_sum(a, b):
+    return pl.pallas_call(
+        sum_kernel,
+        name="part_sum",
+        in_specs=[pl.BlockSpec(memory_space=pltpu.VMEM)] * 2,
+        out_specs=pl.BlockSpec(memory_space=pltpu.HBM),
+        out_shape=jax.ShapeDtypeStruct((SLOTS, HALF // 2), BF),
+        scratch_shapes=[pltpu.VMEM((SLOTS, HALF // 2), BF), pltpu.SemaphoreType.DMA((4,))],
+        compiler_params=vm(4),
+    )(a, b)
 
 
 def compact(perm, src_ref, xs, cs):
@@ -267,18 +326,33 @@
     )(meta, perm, own, peer, hid, gg, gu)
 
 
-def combine_kernel(meta, ids_ref, ret_ref, d_ref, dm_ref, b0, b1, b2, b3):
+def combine_kernel(
+    meta, ids_hbm, ret_hbm, d_hbm, dm_ref, b0, b1, b2, b3, ids, ret, own, sems
+):
     tp, z = meta[0], meta[1]
-    r0, r1 = slot_rows(ids_ref)
+    cut = SLOTS // 4
+    copies = fetch(
+        [(ids_hbm, ids)]
+        + [(ret_hbm.at[k * cut : (k + 1) * cut, :], ret.at[k * cut : (k + 1) * cut, :]) for k in range(4)]
+        + [(d_hbm.at[:, lanes(2 * j + tp)], own.at[:, j * BLK : (j + 1) * BLK]) for j in range(4)],
+        sems,
+    )
+    copies[0].wait()
+    r0, r1 = slot_rows(ids)
     c0, c1 = as_column(r0).astype(jnp.int32), as_column(r1).astype(jnp.int32)
-    slot = lax.broadcasted_iota(jnp.int32, (TOK, SLOTS), 1)
-    for side in range(2):
-        pick = (slot == c0 + side * CAP) | (slot == c1 + side * CAP)
-        back = dot(jnp.where(pick, 1.0, 0.0).astype(BF), ret_ref[...])
-        for k in range(2):
-            j = 2 * side + k
-            own = d_ref[:, lanes(2 * j + tp)].astype(F32)
-            dm_ref[:, j * BLK : (j + 1) * BLK] = (own + back[:, k * BLK : (k + 1) * BLK]).astype(BF)
+    low = high = 0.0
+    for k in range(4):
+        slot = lax.broadcasted_iota(jnp.int32, (TOK, cut), 1) + k * cut
+        first = jnp.where((slot == c0) | (slot == c1), 1.0, 0.0).astype(BF)
+        second = jnp.where((slot == c0 + CAP) | (slot == c1 + CAP), 1.0, 0.0).astype(BF)
+        copies[1 + k].wait()
+        piece = ret[k * cut : (k + 1) * cut, :]
+        low += dot(first, piece)
+        high += dot(second, piece)
+    for copy in copies[5:]:
+        copy.wait()
+    dm_ref[:, :512] = (own[:, :512].astype(F32) + low).astype(BF)
+    dm_ref[:, 512:] = (own[:, 512:].astype(F32) + high).astype(BF)
     for k, ref in enumerate((b0, b1, b2, b3)):
         ref[...] = dm_ref[:, lanes(lax.rem(z + k, 4))]
 
@@ -287,13 +361,19 @@
     return pl.pallas_call(
         combine_kernel,
         name="combine",
-        in_specs=whole(3),
+        in_specs=mixed("hhh"),
         out_specs=[pl.BlockSpec(memory_space=pltpu.VMEM)] * 5,
         out_shape=[jax.ShapeDtypeStruct((TOK, HALF), BF)]
         + [jax.ShapeDtypeStruct((TOK, BLK), BF)] * 4,
-        compiler_params=vm(16),
+        scratch_shapes=[
+            pltpu.VMEM((2, TOK), jnp.int32),
+            pltpu.VMEM((SLOTS, HALF // 2), BF),
+            pltpu.VMEM((TOK, HALF), BF),
+            pltpu.SemaphoreType.DMA((9,)),
+        ],
+        compiler_params=vm(12),
         cost_estimate=cost(1e9),
-    )(meta, ids, ret, d_out)
+    )(meta, *in_hbm(ids, ret, d_out))
 
 
 ROOT = 0.7978845608028654
@@ -344,29 +424,38 @@
 
 
 def drive_kernel(
-    meta, own_ref, peer_ref, w_ref, gate_ref, lru_ref, decay_ref,
-    dgate_ref, drive_ref, head_ref, rate_ref,
+    meta, own_ref, peer_ref, w_hbm, gate_hbm, lru_hbm, decay_hbm,
+    dgate_ref, drive_ref, head_ref, rate_ref, w, gate, lru, decay, sems,
 ):
     tp = meta[0]
+    parts = [2 * j + tp for j in range(4)] + [2 * j + 1 - tp for j in range(4)]
+    copies = fetch(
+        [(w_hbm.at[:, lanes(part)], w.at[k, :, :]) for k, part in enumerate(parts)]
+        + [(gate_hbm, gate), (lru_hbm, lru), (decay_hbm, decay)],
+        sems,
+    )
     grad = 0.0
-    for ref, par in ((own_ref, tp), (peer_ref, 1 - tp)):
-        for j in range(4):
-            grad += dot_cols(ref[:, j * BLK : (j + 1) * BLK], w_ref[:, lanes(2 * j + par)])
-    x = gate_ref[...].astype(F32)
+    for k in range(8):
+        copies[k].wait()
+        ref, j = (own_ref, peer_ref)[k // 4], k % 4
+        grad += dot_cols(ref[:, j * BLK : (j + 1) * BLK], w[k, :, :])
+    for copy in copies[8:]:
+        copy.wait()
+    x = gate[...].astype(F32)
     value, t = gelu_parts(x)
     slope = 0.5 * (1.0 + t) + 0.5 * x * (1.0 - t * t) * (ROOT * (1.0 + 3.0 * CUBE * x * x))
-    dgate_ref[...] = (grad * lru_ref[...].astype(F32) * slope).astype(BF)
+    dgate_ref[...] = (grad * lru[...].astype(F32) * slope).astype(BF)
     drive_ref[...] = grad * value
-    rate_ref[...] = jnp.exp(decay_ref[...])
+    rate_ref[...] = jnp.exp(decay[...])
     head_ref[0:8, :] = tile_of(scan_rows(drive_ref, rate_ref, jnp.zeros((1, HALF), F32), None))
-    head_ref[8:16, :] = tile_of(jnp.exp(jnp.sum(decay_ref[...], axis=0, keepdims=True)))
+    head_ref[8:16, :] = tile_of(jnp.exp(jnp.sum(decay[...], axis=0, keepdims=True)))
 
 
 def drive(meta, own, peer, w_out, gate_pre, lru_out, log_decay):
     return pl.pallas_call(
         drive_kernel,
         name="drive",
-        in_specs=whole(6),
+        in_specs=mixed("vvhhhh"),
         out_specs=[pl.BlockSpec(memory_space=pltpu.VMEM)] * 4,
         out_shape=[
             jax.ShapeDtypeStruct((TOK, HALF), BF),
@@ -374,50 +463,61 @@
             jax.ShapeDtypeStruct((16, 128), F32),
             jax.ShapeDtypeStruct((TOK, HALF), F32),
         ],
+        scratch_shapes=[
+            pltpu.VMEM((8, HALF, BLK), BF),
+            pltpu.VMEM((TOK, HALF), BF),
+            pltpu.VMEM((TOK, HALF), BF),
+            pltpu.VMEM((TOK, HALF), F32),
+            pltpu.SemaphoreType.DMA((11,)),
+        ],
         compiler_params=vm(16),
         cost_estimate=cost(2e9),
-    )(meta, own, peer, w_out, gate_pre, lru_out, log_decay)
-
-
-def level_kernel(place, h0, h1, h2, h3, total_ref, rest_ref, line):
-    for k, ref in enumerate((h0, h1, h2, h3)):
-        line[lax.rem(place[0] + k, 4), :, :] = ref[...]
-    total = within = jnp.zeros((8, 128), F32)
-    product = after = jnp.ones((8, 128), F32)
-    for r in reversed(range(4)):
-        head, block = line[r, 0:8, :], line[r, 8:16, :]
+    )(meta, own, peer, *in_hbm(w_out, gate_pre, lru_out, log_decay))
+
+
+def link_kernel(meta, shares_ref, within_ref, after_ref, plane_ref):
+    place = meta[3]
+    within = jnp.zeros((8, 128), F32)
+    total = jnp.zeros((8, 128), F32)
+    after = jnp.ones((8, 128), F32)
+    product = jnp.ones((8, 128), F32)
+    for r in reversed(range(16)):
+        tile = shares_ref[r, :, HALF:].astype(F32)
+        head, block = tile[0:8] + tile[8:16], tile[16:24] + tile[24:32]
         total = head + block * total
         product = block * product
-        later = place[0] < r
-        within = jnp.where(later, total, within)
-        after = jnp.where(later, product, after)
-    total_ref[0:8, :] = total
-    total_ref[8:16, :] = product
-    rest_ref[0:8, :] = within
-    rest_ref[8:16, :] = after
-
-
-def level(pair, axis):
-    place = lax.axis_index(axis).astype(jnp.int32).reshape(1)
-    others = [
-        lax.ppermute(pair, axis, [(s, (s - k) % 4) for s in range(4)]) for k in (1, 2, 3)
-    ]
-    return pl.pallas_call(
-        level_kernel,
-        in_specs=whole(4),
-        out_specs=[pl.BlockSpec(memory_space=pltpu.VMEM)] * 2,
-        out_shape=[jax.ShapeDtypeStruct((16, 128), F32)] * 2,
-        scratch_shapes=[pltpu.VMEM((4, 16, 128), F32)],
-        compiler_params=vm(4),
+        within = jnp.where(place < r, total, within)
+        after = jnp.where(place < r, product, after)
+    within_ref[...] = within
+    after_ref[...] = after
+    plane_ref[0:8, :] = total
+    plane_ref[8:16, :] = product
+
+
+def link(meta, shares):
+    return pl.pallas_call(
+        link_kernel,
+        name="link",
+        in_specs=whole(1),
+        out_specs=[pl.BlockSpec(memory_space=pltpu.VMEM)] * 3,
+        out_shape=[
+            jax.ShapeDtypeStruct((8, 128), F32),
+            jax.ShapeDtypeStruct((8, 128), F32),
+            jax.ShapeDtypeStruct((16, 128), F32),
+        ],
+        compiler_params=vm(8),
         cost_estimate=cost(1e7),
-    )(place, pair, *others)
+    )(meta, shares)
 
 
 def finish_kernel(
-    rx, ry, rz, drive_ref, rate_ref, lru_ref, before_ref, dd_ref, dl_ref, prev_ref
+    within_ref, after_ref, p1, p2, p3, drive_ref, rate_ref, lru_ref, before_ref, dd_ref, dl_ref,
+    prev_ref,
 ):
-    inner = ry[0:8, :] + ry[8:16, :] * rz[0:8, :]
-    carry = line_of(rx[0:8, :] + rx[8:16, :] * inner)
+    planes = p3[0:8, :]
+    planes = p2[0:8, :] + p2[8:16, :] * planes
+    planes = p1[0:8, :] + p1[8:16, :] * planes
+    carry = line_of(within_ref[...] + after_ref[...] * planes)
     state = lru_ref[...].astype(F32)
     first = lax.broadcasted_iota(jnp.int32, (TOK, HALF), 0) == 0
     prev_ref[...] = jnp.where(first, before_ref[...].astype(F32), pltpu.roll(state, 1, 0))
@@ -429,40 +529,68 @@
     scan_rows(drive_ref, rate_ref, carry, visit)
 
 
-def finish(rests, drive_value, rate, lru_out, before):
+def finish(within, after, planes, drive_value, rate, lru_out, before):
     return pl.pallas_call(
         finish_kernel,
         name="finish",
         out_shape=[jax.ShapeDtypeStruct((TOK, HALF), F32)] * 2,
         scratch_shapes=[pltpu.VMEM((TOK, HALF), F32)],
         compiler_params=vm(8),
+        cost_estimate=cost(1e8),
+    )(within, after, *planes, drive_value, rate, lru_out, before)
+
+
+def outer_own_kernel(b0, b1, b2, b3, g0, g1, g2, g3, out_ref, moved, sems):
+    copies = fetch([(g, moved.at[k, :, :]) for k, g in enumerate((g0, g1, g2, g3))], sems)
+    total = 0.0
+    for k, ref in enumerate((b0, b1, b2, b3)):
+        copies[k].wait()
+        total += dot_rows(ref[...], moved[k, :, :])
+    out_ref[...] = total.astype(BF)
+
+
+def outer_own(blocks, gated):
+    return pl.pallas_call(
+        outer_own_kernel,
+        name="outer_own",
+        in_specs=mixed("vvvvhhhh")[1:],
+        out_specs=pl.BlockSpec(memory_space=pltpu.VMEM),
+        out_shape=jax.ShapeDtypeStruct((BLK, HALF), BF),
+        scratch_shapes=[pltpu.VMEM((4, TOK, HALF), BF), pltpu.SemaphoreType.DMA((4,))],
+        compiler_params=vm(10),
         cost_estimate=cost(1e9),
-    )(*rests, drive_value, rate, lru_out, before)
-
-
-def outer_kernel(meta, *refs):
-    own, peer, gated = refs[0:4], refs[4:8], refs[8:12]
-    out_ref = refs[12]
+    )(*blocks, *in_hbm(*gated))
+
+
+def outer_kernel(meta, p0, p1, p2, p3, g0, g1, g2, g3, own_ref, head_ref, out_ref, moved, sems):
     tp, z = meta[0], meta[1]
-    total_own = dot_rows(own[0][...], gated[0][...])
-    total_peer = dot_rows(peer[0][:, lanes(z)], gated[0][...])
-    for k in range(1, 4):
-        total_own += dot_rows(own[k][...], gated[k][...])
-        total_peer += dot_rows(peer[k][...], gated[k][...])
-    out_ref[lanes(tp), :] = total_own.astype(BF)
-    out_ref[lanes(1 - tp), :] = total_peer.astype(BF)
-
-
-def outer(meta, own, peer, gated):
+    copies = fetch([(g, moved.at[k, :, :]) for k, g in enumerate((g0, g1, g2, g3))], sems)
+    out_ref[lanes(tp), 0:HALF] = own_ref[...]
+    value = head_ref[...]
+    high = value.astype(BF).astype(F32)
+    low = value - high
+    tile = jnp.concatenate([high[0:8], low[0:8], high[8:16], low[8:16]], axis=0).astype(BF)
+    for k in range(16):
+        out_ref[k * 32 : (k + 1) * 32, HALF:] = tile
+    copies[0].wait()
+    total = dot_rows(p0[:, lanes(z)], moved[0, :, :])
+    for k, ref in ((1, p1), (2, p2), (3, p3)):
+        copies[k].wait()
+        total += dot_rows(ref[...], moved[k, :, :])
+    out_ref[lanes(1 - tp), 0:HALF] = total.astype(BF)
+
+
+def outer(meta, peer, gated, own, head):
     return pl.pallas_call(
         outer_kernel,
         name="outer",
-        in_specs=whole(12),
+        in_specs=mixed("vvvvhhhhvv"),
         out_specs=pl.BlockSpec(memory_space=pltpu.VMEM),
-        out_shape=jax.ShapeDtypeStruct((2 * BLK, HALF), BF),
-        compiler_params=vm(12),
-        cost_estimate=cost(2e9),
-    )(meta, *own, *peer, *gated)
+        out_shape=jax.ShapeDtypeStruct((2 * BLK, HALF + 128), BF),
+        scratch_shapes=[pltpu.VMEM((4, TOK, HALF), BF), pltpu.SemaphoreType.DMA((4,))],
+        compiler_params=vm(10),
+        cost_estimate=cost(1e9),
+    )(meta, *peer, *in_hbm(*gated), own, head)
 
 
 def swapped(value):
@@ -487,35 +615,33 @@
     got = lax.all_to_all(sent.reshape(NSP, CHUNK, HALF), SP, 0, 0, tiled=True)
     got = got.reshape(SLOTS, HALF)
     got_peer = swapped(got)
-    gated, last = early(gate_pre, lru_out), lru_out[-1:]
-    gated, last, got = lax.optimization_barrier((gated, last, got))
-    turns = [turned(gated, k) for k in (1, 2, 3)]
-    before = lax.ppermute(last, SP, [(s, s + 1) for s in range(NSP - 1)])
+    gated = early(gate_pre, lru_out)
+    gated, got = lax.optimization_barrier((gated, got))
+    turn2 = turned(gated, 2)
     pg, pu, pb = expert_own(meta, perm, got, wg, wu, wd)
     hid, gg, gu, part_peer = expert_peer(meta, perm, perm_t, got_peer, wg, wu, wd, pg, pu, pb)
     other = swapped(part_peer)
     part_own = expert_back(meta, perm_t, gg, gu, wg, wu)
-    back = (part_own.astype(F32) + other.astype(F32)).astype(BF)
-    back, before, *turns = lax.optimization_barrier((back, before, *turns))
+    back = part_sum(part_own, other)
+    back, turn2 = lax.optimization_barrier((back, turn2))
     ret = lax.all_to_all(back.reshape(NSP, CHUNK, HALF // 2), SP, 0, 0, tiled=True)
-    grad_gate, grad_up, grad_down = weight_grads(meta, perm, got, got_peer, hid, gg, gu)
-    ret, grad_gate, grad_up, grad_down = lax.optimization_barrier(
-        (ret, grad_gate, grad_up, grad_down)
-    )
+    back, moving, last = lax.optimization_barrier((back, gated, lru_out[-1:]))
+    turn1, turn3 = turned(moving, 1), turned(moving, 3)
+    before = lax.ppermute(last, SP, [(s, s + 1) for s in range(NSP - 1)])
+    grads = weight_grads(meta, perm, got, got_peer, hid, gg, gu)
+    ret, grad_gate, grad_up, grad_down = lax.optimization_barrier((ret, *grads))
     dm, *blocks = combine(meta, ids, ret.reshape(SLOTS, HALF // 2), d_out)
     dm_peer = swapped(dm)
     own = (blocks[0], *(turned(blocks[k], k) for k in (1, 2, 3)))
+    d_gate, drive_value, head, rate = drive(meta, dm, dm_peer, w_out, gate_pre, lru_out, log_decay)
     peer = (dm_peer, *(swapped(own[k]) for k in (1, 2, 3)))
-    share = outer(meta, own, peer, (gated, *turns))
-    shares = lax.all_to_all(share.reshape(16, 32, HALF), ("y", "x"), 0, 0, tiled=True)
-    d_gate, drive_value, head, rate = drive(
-        meta, dm, dm_peer, w_out, gate_pre, lru_out, log_decay
-    )
-    line, rest_x = level(head, "x")
-    plane, rest_y = level(line, "y")
-    _, rest_z = level(plane, "z")
-    d_drive, d_log_decay = finish((rest_x, rest_y, rest_z), drive_value, rate, lru_out, before)
-    grad_out_proj = jnp.sum(shares.astype(F32), axis=0)
+    all_gated = (gated, turn1, turn2, turn3)
+    share = outer(meta, peer, all_gated, outer_own(own, all_gated), head)
+    shares = lax.all_to_all(share.reshape(16, 32, HALF + 128), ("y", "x"), 0, 0, tiled=True)
+    within, after, plane = link(meta, shares)
+    planes = [lax.ppermute(plane, "z", [(s, s - k) for s in range(k, 4)]) for k in (1, 2, 3)]
+    d_drive, d_log_decay = finish(within, after, planes, drive_value, rate, lru_out, before)
+    grad_out_proj = jnp.sum(shares[:, :, :HALF].astype(F32), axis=0)
     return (
         grad_gate[None], grad_up[None], grad_down[None], grad_out_proj, d_gate, d_drive, d_log_decay,
     )

time: 191 us -> 181 us (0.948)
  the two profiles are of different devices: /device:TPU:0 before, /device:TPU:1 now
where the time goes in v2:
time: 181 us; the launch traced here: 179 us
  blocking collectives  52.2 us (29%)
  Pallas kernels  49.7 us (27%)
  waiting for transfers between devices  38.8 us (21%)
  starting transfers between devices  28.9 us (16%)
  local copies, waits for them, and re-layouts  7.76 us (4%)
    all_to_all x1, blocking collectives, on_device(): got = lax.all_to_all(sent.reshape(NSP, CHUNK, HALF), SP, 0, 0, tiled=True)  52.2 us
    all_to_all x1, waiting for transfers between devices, on_device(): lax.all_to_all(share.reshape(16, 32, HALF + 128), ('y', 'x'), 0, 0, tiled...  17.7 us
    ppermute x6, waiting for transfers between devices, turned(): return lax.ppermute(value, 'z', [(s, (s + steps) % 4) for s in range(4)])  12.5 us
    pallas_call x1, Pallas kernels, weight_grads(): pl.pallas_call(weight_kernel, name='weight_grads', grid_spec=pltpu.Prefet...  11.3 us
    unnamed x42, local copies, waits for them, and re-layouts  7.75 us
    pallas_call x1, Pallas kernels, expert_peer(): pl.pallas_call(peer_kernel, name='expert_peer', in_specs=whole(9), out_sp...  6.79 us
    ppermute x6, starting transfers between devices, swapped(): return lax.ppermute(value, 'tp', [(0, 1), (1, 0)])  6.54 us
    pallas_call x1, Pallas kernels, drive(): pl.pallas_call(drive_kernel, name='drive', in_specs=mixed('vvhhhh'), out_...  6.34 us
  transfers between devices with their start and end apart: 18, of which 7 were waited for; matrix products, arithmetic and copies ran while one was open for 0% of the time, Pallas kernels for 18%

profile of v2, /device:TPU:1, one launch (start us, length us, event | category | flops | bytes accessed | tf_op | source)
XLA Modules:
  0.0 179.3 jit_solution(13305726919930024568)
XLA Ops:
  0.6 0.1 pad_add_fusion.meta
  0.7 5.1 %pack.1 = bf16[1536,1024]{1,0:T(8,128)(2,1)S(1)} custom-call(s32[4]{0:T(128)S(1)} %pad_add_fusion.meta, s32[2,192]{1,0:T(2,128)} %bitcast.30, f32[2,192]{1,0:T(2,128)} %bitcast.29, bf16[192,2048]{1,0:T(8,128)(2,1)} %x_hbm.1, bf16[192,2048]{1,0:T(8,128)(2,1)} %d_hbm.3), custom_call_target="tpu_custom_call" | custom-call | tf_op jit(solution)/shard_map/pack/pallas_call | solution.py:138
  5.9 0.0 copy-start.10
  5.9 52.2 %all_to_all.15 = bf16[64,24,1024]{2,1,0:T(8,128)(2,1)S(1)} all-to-all(bf16[64,24,1024]{2,1,0:T(8,128)(2,1)S(1)} %bitcast.17), channel_id=1, replica_groups=mesh['z'=4,'y'=4,'x'=4,'tp'=2] {'z','y','x'}, dimensions={0} | all-to-all | bytes 6291456 | tf_op jit(solution)/shard_map/all_to_all | solution.py:615
  58.2 2.1 %collective-permute-start = (bf16[1536,1024]{1,0:T(8,128)(2,1)S(1)}, bf16[1536,1024]{1,0:T(8,128)(2,1)S(1)}, u32[]{:S(2)}, u32[]{:S(2)}) collective-permute-start(bf16[1536,1024]{1,0:T(8,128)(2,1)S(1)} %bitcast.18), channel_id=1, source_target_pairs={{0,1},{1,0},{2,3},{3,2},{4,5},{5,4},{6,7},{7,6},{8,9},{9,8},{10,11... | collective-permute-start | bytes 9437192 | tf_op jit(solution)/shard_map/ppermute | solution.py:597
  60.3 0.3 early.1.g0
  60.7 4.0 %expert_own.1 = (f32[768,512]{1,0:T(8,128)S(1)}, f32[768,512]{1,0:T(8,128)S(1)}, f32[768,512]{1,0:T(8,128)S(1)}) custom-call(s32[4]{0:T(128)S(1)} %pad_add_fusion.meta, bf16[192,192]{1,0:T(8,128)(2,1)S(1)} %copy-done.10, bf16[1536,1024]{1,0:T(8,128)(2,1)S(1)} %bitcast.19, bf16[2048,512]{1,0:T(8,128)(2,1)S(1)} %bitcast.23, bf16[2048,512]{1,0:T(8,128)(2,1)S(1)} %bitcast.26, ...), custom_call_target="tpu_custom_call" | custom-call | flops 4000000000 | tf_op jit(solution)/shard_map/expert_own/pallas_call | solution.py:216
  64.7 0.9 collective-permute-done.peer_ref
  65.6 6.8 %expert_peer.1 = (bf16[768,512]{1,0:T(8,128)(2,1)S(1)}, bf16[768,512]{1,0:T(8,128)(2,1)S(1)}, bf16[768,512]{1,0:T(8,128)(2,1)S(1)}, bf16[1536,512]{1,0:T(8,128)(2,1)S(1)}) custom-call(s32[4]{0:T(128)S(1)} %pad_add_fusion.meta, bf16[192,192]{1,0:T(8,128)(2,1)S(1)} %copy-done.10, bf16[192,192]{1,0:T(8,128)(2,1)S(1)} %copy-done.12, ...), custom_call_target="tpu_custom_call" | custom-call | flops 6000000000 | tf_op jit(solution)/shard_map/expert_peer/pallas_call | solution.py:247
  72.4 0.5 collective-permute-start.1
  72.9 0.4 collective-permute-start.2
  73.2 2.8 %expert_back.1.a_ref = bf16[1536,512]{1,0:T(8,128)(2,1)S(1)} custom-call(s32[4]{0:T(128)S(1)} %pad_add_fusion.meta, bf16[192,192]{1,0:T(8,128)(2,1)S(1)} %copy-done.12, bf16[768,512]{1,0:T(8,128)(2,1)S(1)} %get-tuple-element.45.gg_ref, bf16[768,512]{1,0:T(8,128)(2,1)S(1)} %get-tuple-element.46.gu_ref, bf16[2048,512]{1,0:T(8,128)(2,1)S(1)} %bitcast.25, ...), custom_call_target="tpu_custom_call" | custom-call | flops 3000000000 | tf_op jit(solution)/shard_map/expert_back/pallas_call | solution.py:265
  76.1 1.3 part_sum.1
  77.4 7.5 %collective-permute-done.2.g2 = bf16[192,1024]{1,0:T(8,128)(2,1)S(1)} collective-permute-done((bf16[192,1024]{1,0:T(8,128)(2,1)S(1)}, bf16[192,1024]{1,0:T(8,128)(2,1)S(1)}, u32[]{:S(2)}, u32[]{:S(2)}) %collective-permute-start.2) | collective-permute-done | bytes 393248 | tf_op jit(solution)/shard_map/ppermute | solution.py:601
  84.9 0.7 copy-done.19
  85.7 5.5 %all-to-all-start.1 = ((bf16[64,24,512]{2,1,0:T(8,128)(2,1)}), bf16[64,24,512]{2,1,0:T(8,128)(2,1)}, u32[]{:S(2)}, u32[]{:S(2)}) async-start(bf16[64,24,512]{2,1,0:T(8,128)(2,1)} %bitcast.11), calls=%async_computation.1 | async-start | bytes 3145728 | tf_op jit(solution)/shard_map/all_to_all | solution.py:627
  91.2 1.2 collective-permute-start.10
  92.4 1.9 %copy-done.6 = bf16[1536,1024]{1,0:T(8,128)(2,1)S(1)} copy-done((bf16[1536,1024]{1,0:T(8,128)(2,1)S(1)}, bf16[1536,1024]{1,0:T(8,128)(2,1)}, u32[]{:S(2)}) %copy-start.6) | copy-done | bytes 3145752
  94.3 0.9 copy-done.11
  95.2 1.1 copy-done.14
  96.3 1.1 copy-done.16
  97.5 1.1 copy-done.18
  98.6 11.3 %weight_grads.1 = (f32[2048,512]{1,0:T(8,128)}, f32[2048,512]{1,0:T(8,128)}, f32[512,2048]{1,0:T(8,128)}) custom-call(s32[4]{0:T(128)S(1)} %pad_add_fusion.meta, bf16[192,192]{1,0:T(8,128)(2,1)S(1)} %copy-done.11, bf16[1536,1024]{1,0:T(8,128)(2,1)S(1)} %bitcast.20, bf16[1536,1024]{1,0:T(8,128)(2,1)S(1)} %copy-done.6, bf16[768,512]{1,0:T(8,128)(2,1)S(1)} %copy-done.18, ...), custom_call_target="tpu_custom_call" | custom-call | flops 4831838208 | bytes 20000000 | tf_op jit(solution)/shard_map/weight_grads/pallas_call | solution.py:296
  110.0 1.7 collective-permute-start.11
  111.7 2.4 %all-to-all-done.1 = bf16[64,24,512]{2,1,0:T(8,128)(2,1)} async-done(((bf16[64,24,512]{2,1,0:T(8,128)(2,1)}), bf16[64,24,512]{2,1,0:T(8,128)(2,1)}, u32[]{:S(2)}, u32[]{:S(2)}) %all-to-all-start.1) | async-done | bytes 1572896 | tf_op jit(solution)/shard_map/all_to_all | solution.py:627
  114.1 3.3 %combine.1 = (bf16[192,1024]{1,0:T(8,128)(2,1)S(1)}, bf16[192,256]{1,0:T(8,128)(2,1)S(1)}, bf16[192,256]{1,0:T(8,128)(2,1)S(1)}, bf16[192,256]{1,0:T(8,128)(2,1)S(1)}, bf16[192,256]{1,0:T(8,128)(2,1)S(1)}) custom-call(s32[4]{0:T(128)S(1)} %pad_add_fusion.meta, s32[2,192]{1,0:T(2,128)} %bitcast.31, bf16[1536,512]{1,0:T(8,128)(2,1)} %bitcast.15.ret_hbm, ...), custom_call_target="tpu_custom_call" | custom-call | flops 1000000000 | tf_op jit(solution)/shard_map/combine/pallas_call | solution.py:361
  117.4 2.4 %collective-permute-start.3 = (bf16[192,1024]{1,0:T(8,128)(2,1)S(1)}, bf16[192,1024]{1,0:T(8,128)(2,1)S(1)}, u32[]{:S(2)}, u32[]{:S(2)}) collective-permute-start(bf16[192,1024]{1,0:T(8,128)(2,1)S(1)} %get-tuple-element.58.own_ref), channel_id=1, source_target_pairs={{0,1},{1,0},{2,3},{3,2},{4,5},{5,4},{6,7},{7,6},{8,9},{9,8},{10,11... | collective-permute-start | bytes 1179656 | tf_op jit(solution)/shard_map/ppermute | solution.py:597
  119.8 0.2 collective-permute-start.4
  120.0 1.6 collective-permute-start.6
  121.6 1.0 collective-permute-start.8
  122.5 4.9 %collective-permute-done.4.b1 = bf16[192,256]{1,0:T(8,128)(2,1)S(1)} collective-permute-done((bf16[192,256]{1,0:T(8,128)(2,1)S(1)}, bf16[192,256]{1,0:T(8,128)(2,1)S(1)}, u32[]{:S(2)}, u32[]{:S(2)}) %collective-permute-start.4) | collective-permute-done | bytes 98336 | tf_op jit(solution)/shard_map/ppermute | solution.py:601
  127.4 0.9 collective-permute-start.5
  128.4 0.6 collective-permute-start.9
  129.0 0.7 copy-done.20
  129.7 2.0 %outer_own.1.own_ref = bf16[256,1024]{1,0:T(8,128)(2,1)S(1)} custom-call(bf16[192,256]{1,0:T(8,128)(2,1)S(1)} %get-tuple-element.64.b0, bf16[192,256]{1,0:T(8,128)(2,1)S(1)} %collective-permute-done.4.b1, bf16[192,256]{1,0:T(8,128)(2,1)S(1)} %collective-permute-done.6.b2, bf16[192,256]{1,0:T(8,128)(2,1)S(1)} %collective-permute-done.8.b3, ...), custom_call_target="tpu_custom_call" | custom-call | flops 1000000000 | tf_op jit(solution)/shard_map/outer_own/pallas_call | solution.py:553
  131.8 6.3 %drive.1 = (bf16[192,1024]{1,0:T(8,128)(2,1)}, f32[192,1024]{1,0:T(8,128)S(1)}, f32[16,128]{1,0:T(8,128)S(1)}, f32[192,1024]{1,0:T(8,128)S(1)}) custom-call(s32[4]{0:T(128)S(1)} %pad_add_fusion.meta, bf16[192,1024]{1,0:T(8,128)(2,1)S(1)} %get-tuple-element.58.own_ref, bf16[192,1024]{1,0:T(8,128)(2,1)S(1)} %collective-permute-done.3.peer_ref.p0, ...), custom_call_target="tpu_custom_call" | custom-call | flops 2000000000 | tf_op jit(solution)/shard_map/drive/pallas_call | solution.py:455
  138.2 3.6 %outer.1 = bf16[512,1152]{1,0:T(8,128)(2,1)} custom-call(s32[4]{0:T(128)S(1)} %pad_add_fusion.meta, bf16[192,1024]{1,0:T(8,128)(2,1)S(1)} %collective-permute-done.3.peer_ref.p0, bf16[192,256]{1,0:T(8,128)(2,1)S(1)} %collective-permute-done.5.p1, bf16[192,256]{1,0:T(8,128)(2,1)S(1)} %collective-permute-done.7.p2, ...), custom_call_target="tpu_custom_call" | custom-call | flops 1000000000 | tf_op jit(solution)/shard_map/outer/pallas_call | solution.py:584
  141.8 3.8 %all-to-all-start.2 = ((bf16[16,32,1152]{2,1,0:T(8,128)(2,1)}), bf16[16,32,1152]{2,1,0:T(8,128)(2,1)S(1)}, u32[]{:S(2)}, u32[]{:S(2)}) async-start(bf16[16,32,1152]{2,1,0:T(8,128)(2,1)} %bitcast.16), calls=%async_computation.2 | async-start | bytes 2359296 | tf_op jit(solution)/shard_map/all_to_all | solution.py:640
  145.6 3.1 %collective-permute-start.15 = (bf16[1,1024]{1,0:T(2,128)(2,1)S(1)}, bf16[1,1024]{1,0:T(2,128)(2,1)S(1)}, u32[]{:S(2)}, u32[]{:S(2)}) collective-permute-start(bf16[1,1024]{1,0:T(2,128)(2,1)S(1)} %slice.6), channel_id=1, source_target_pairs={{0,2},{2,4},{4,6},{6,8},{8,10},{10,12},{12,14},{14,16},{16,18},{18... | collective-permute-start | bytes 6152 | tf_op jit(solution)/shard_map/ppermute | solution.py:630
  148.8 17.7 %all-to-all-done.2.shares_ref = bf16[16,32,1152]{2,1,0:T(8,128)(2,1)S(1)} async-done(((bf16[16,32,1152]{2,1,0:T(8,128)(2,1)}), bf16[16,32,1152]{2,1,0:T(8,128)(2,1)S(1)}, u32[]{:S(2)}, u32[]{:S(2)}) %all-to-all-start.2) | async-done | bytes 1179680 | tf_op jit(solution)/shard_map/all_to_all | solution.py:640
  166.5 0.6 link.1
  167.1 1.3 collective-permute-start.12
  168.4 1.3 collective-permute-start.13
  169.7 1.3 collective-permute-start.14
  171.0 0.8 convert_reduce_fusion
  171.8 2.5 %collective-permute-done.13.p2 = f32[16,128]{1,0:T(8,128)S(1)} collective-permute-done((f32[16,128]{1,0:T(8,128)S(1)}, f32[16,128]{1,0:T(8,128)S(1)}, u32[]{:S(2)}, u32[]{:S(2)}) %collective-permute-start.13) | collective-permute-done | bytes 8224 | tf_op jit(solution)/shard_map/ppermute | solution.py:642
  174.3 2.8 %collective-permute-done.14.p3 = f32[16,128]{1,0:T(8,128)S(1)} collective-permute-done((f32[16,128]{1,0:T(8,128)S(1)}, f32[16,128]{1,0:T(8,128)S(1)}, u32[]{:S(2)}, u32[]{:S(2)}) %collective-permute-start.14) | collective-permute-done | bytes 8224 | tf_op jit(solution)/shard_map/ppermute | solution.py:642
  177.1 2.2 %finish.1 = (f32[192,1024]{1,0:T(8,128)}, f32[192,1024]{1,0:T(8,128)}) custom-call(f32[8,128]{1,0:T(8,128)S(1)} %get-tuple-element.67.within_ref, f32[8,128]{1,0:T(8,128)S(1)} %get-tuple-element.68.after_ref, f32[16,128]{1,0:T(8,128)S(1)} %collective-permute-done.12.p1, f32[16,128]{1,0:T(8,128)S(1)} %collective-permute-done.13.p2, ...), custom_call_target="tpu_custom_call" | custom-call | flops 100000000 | tf_op jit(solution)/shard_map/finish/pallas_call | solution.py:533
  (47 shorter events, 0.1 us)
Async XLA Ops:
  5.9 54.4 %copy-start = (bf16[192,1024]{1,0:T(8,128)(2,1)S(1)}, bf16[192,1024]{1,0:T(8,128)(2,1)}, u32[]{:S(2)}) copy-start(bf16[192,1024]{1,0:T(8,128)(2,1)} %lru_ref.3) | copy-start | bytes 1179652
  5.9 54.4 %copy-start.4 = (bf16[192,1024]{1,0:T(8,128)(2,1)S(1)}, bf16[192,1024]{1,0:T(8,128)(2,1)}, u32[]{:S(2)}) copy-start(bf16[192,1024]{1,0:T(8,128)(2,1)} %gate_hbm.1) | copy-start | bytes 1179652
  5.9 54.7 %copy-start.7 = (bf16[1,512,2048]{2,1,0:T(8,128)(2,1)S(1)}, bf16[1,512,2048]{2,1,0:T(8,128)(2,1)}, u32[]{:S(2)}) copy-start(bf16[1,512,2048]{2,1,0:T(8,128)(2,1)} %param.23) | copy-start | bytes 6291460
  5.9 54.7 %copy-start.8 = (bf16[1,2048,512]{2,1,0:T(8,128)(2,1)S(1)}, bf16[1,2048,512]{2,1,0:T(8,128)(2,1)}, u32[]{:S(2)}) copy-start(bf16[1,2048,512]{2,1,0:T(8,128)(2,1)} %param.21) | copy-start | bytes 6291460
  5.9 54.7 %copy-start.9 = (bf16[1,2048,512]{2,1,0:T(8,128)(2,1)S(1)}, bf16[1,2048,512]{2,1,0:T(8,128)(2,1)}, u32[]{:S(2)}) copy-start(bf16[1,2048,512]{2,1,0:T(8,128)(2,1)} %param.22) | copy-start | bytes 6291460
  5.9 54.7 %copy-start.10 = (bf16[192,192]{1,0:T(8,128)(2,1)S(1)}, bf16[192,192]{1,0:T(8,128)(2,1)}, u32[]{:S(2)}) copy-start(bf16[192,192]{1,0:T(8,128)(2,1)} %constant.25.clone.perm_ref) | copy-start | bytes 221188
  58.2 7.4 %collective-permute-start = (bf16[1536,1024]{1,0:T(8,128)(2,1)S(1)}, bf16[1536,1024]{1,0:T(8,128)(2,1)S(1)}, u32[]{:S(2)}, u32[]{:S(2)}) collective-permute-start(bf16[1536,1024]{1,0:T(8,128)(2,1)S(1)} %bitcast.18), channel_id=1, source_target_pairs={{0,1},{1,0},{2,3},{3,2},{4,5},{5,4},{6,7},{7,6},{8,9},{9,8},{10,11... | collective-permute-start | bytes 9437192 | tf_op jit(solution)/shard_map/ppermute | solution.py:597
  60.6 12.3 %copy-start.2 = (bf16[192,1024]{1,0:T(8,128)(2,1)}, bf16[192,1024]{1,0:T(8,128)(2,1)S(1)}, u32[]{:S(2)}) copy-start(bf16[192,1024]{1,0:T(8,128)(2,1)S(1)} %early.1.g0) | copy-start | bytes 1179652
  60.7 4.9 %copy-start.12 = (bf16[192,192]{1,0:T(8,128)(2,1)S(1)}, bf16[192,192]{1,0:T(8,128)(2,1)}, u32[]{:S(2)}) copy-start(bf16[192,192]{1,0:T(8,128)(2,1)} %constant.26.clone.perm_t_ref) | copy-start | bytes 221188
  65.6 6.8 %copy-start.5 = (bf16[1536,1024]{1,0:T(8,128)(2,1)}, bf16[1536,1024]{1,0:T(8,128)(2,1)S(1)}, u32[]{:S(2)}) copy-start(bf16[1536,1024]{1,0:T(8,128)(2,1)S(1)} %collective-permute-done.peer_ref) | copy-start | bytes 9437188
  72.4 3.6 %copy-start.13 = (bf16[768,512]{1,0:T(8,128)(2,1)}, bf16[768,512]{1,0:T(8,128)(2,1)S(1)}, u32[]{:S(2)}) copy-start(bf16[768,512]{1,0:T(8,128)(2,1)S(1)} %get-tuple-element.45.gg_ref) | copy-start | bytes 2359300
  72.4 3.6 %copy-start.15 = (bf16[768,512]{1,0:T(8,128)(2,1)}, bf16[768,512]{1,0:T(8,128)(2,1)S(1)}, u32[]{:S(2)}) copy-start(bf16[768,512]{1,0:T(8,128)(2,1)S(1)} %get-tuple-element.46.gu_ref) | copy-start | bytes 2359300
  72.4 3.6 %copy-start.17 = (bf16[768,512]{1,0:T(8,128)(2,1)}, bf16[768,512]{1,0:T(8,128)(2,1)S(1)}, u32[]{:S(2)}) copy-start(bf16[768,512]{1,0:T(8,128)(2,1)S(1)} %get-tuple-element.50.hid_ref) | copy-start | bytes 2359300
  72.4 3.6 %collective-permute-start.1 = (bf16[1536,512]{1,0:T(8,128)(2,1)S(1)}, bf16[1536,512]{1,0:T(8,128)(2,1)S(1)}, u32[]{:S(2)}, u32[]{:S(2)}) collective-permute-start(bf16[1536,512]{1,0:T(8,128)(2,1)S(1)} %get-tuple-element.47), channel_id=1, source_target_pairs={{0,1},{1,0},{2,3},{3,2},{4,5},{5,4},{6,7},{7,6},{8,9},{9,8},{10,11... | collective-permute-start | bytes 4718600 | tf_op jit(solution)/shard_map/ppermute | solution.py:597
  72.9 12.0 %collective-permute-start.2 = (bf16[192,1024]{1,0:T(8,128)(2,1)S(1)}, bf16[192,1024]{1,0:T(8,128)(2,1)S(1)}, u32[]{:S(2)}, u32[]{:S(2)}) collective-permute-start(bf16[192,1024]{1,0:T(8,128)(2,1)S(1)} %early.1.g0), channel_id=1, source_target_pairs={{0,64},{32,96},{64,0},{96,32},{1,65},{33,97},{65,1},{97,33},{2,66}... | collective-permute-start | bytes 1179656 | tf_op jit(solution)/shard_map/ppermute | solution.py:601
  84.9 0.7 copy-start.19
  85.7 28.4 %all-to-all-start.1 = ((bf16[64,24,512]{2,1,0:T(8,128)(2,1)}), bf16[64,24,512]{2,1,0:T(8,128)(2,1)}, u32[]{:S(2)}, u32[]{:S(2)}) async-start(bf16[64,24,512]{2,1,0:T(8,128)(2,1)} %bitcast.11), calls=%async_computation.1 | async-start | bytes 3145728 | tf_op jit(solution)/shard_map/all_to_all | solution.py:627
  91.2 30.3 %collective-permute-start.10 = (bf16[192,1024]{1,0:T(8,128)(2,1)}, bf16[192,1024]{1,0:T(8,128)(2,1)}, u32[]{:S(2)}, u32[]{:S(2)}) collective-permute-start(bf16[192,1024]{1,0:T(8,128)(2,1)} %copy-done.2), channel_id=1, source_target_pairs={{0,32},{32,64},{64,96},{96,0},{1,33},{33,65},{65,97},{97,1},{2,34}... | collective-permute-start | bytes 1179656 | tf_op jit(solution)/shard_map/ppermute | solution.py:601
  92.4 1.9 %copy-start.6 = (bf16[1536,1024]{1,0:T(8,128)(2,1)S(1)}, bf16[1536,1024]{1,0:T(8,128)(2,1)}, u32[]{:S(2)}) copy-start(bf16[1536,1024]{1,0:T(8,128)(2,1)} %copy-done.5) | copy-start | bytes 9437188
  94.3 0.9 copy-start.11
  95.2 1.1 copy-start.14
  96.3 1.1 copy-start.16
  97.5 1.1 copy-start.18
  98.6 11.3 %copy-start.3 = (bf16[192,1024]{1,0:T(8,128)(2,1)S(1)}, bf16[192,1024]{1,0:T(8,128)(2,1)}, u32[]{:S(2)}) copy-start(bf16[192,1024]{1,0:T(8,128)(2,1)} %copy-done.2) | copy-start | bytes 1179652
  110.0 19.0 %collective-permute-start.11 = (bf16[192,1024]{1,0:T(8,128)(2,1)S(1)}, bf16[192,1024]{1,0:T(8,128)(2,1)S(1)}, u32[]{:S(2)}, u32[]{:S(2)}) collective-permute-start(bf16[192,1024]{1,0:T(8,128)(2,1)S(1)} %copy-done.3), channel_id=1, source_target_pairs={{0,96},{32,0},{64,32},{96,64},{1,97},{33,1},{65,33},{97,65},{2,98}... | collective-permute-start | bytes 1179656 | tf_op jit(solution)/shard_map/ppermute | solution.py:601
  117.4 14.3 %collective-permute-start.3 = (bf16[192,1024]{1,0:T(8,128)(2,1)S(1)}, bf16[192,1024]{1,0:T(8,128)(2,1)S(1)}, u32[]{:S(2)}, u32[]{:S(2)}) collective-permute-start(bf16[192,1024]{1,0:T(8,128)(2,1)S(1)} %get-tuple-element.58.own_ref), channel_id=1, source_target_pairs={{0,1},{1,0},{2,3},{3,2},{4,5},{5,4},{6,7},{7,6},{8,9},{9,8},{10,11... | collective-permute-start | bytes 1179656 | tf_op jit(solution)/shard_map/ppermute | solution.py:597
  119.8 7.6 %collective-permute-start.4 = (bf16[192,256]{1,0:T(8,128)(2,1)S(1)}, bf16[192,256]{1,0:T(8,128)(2,1)S(1)}, u32[]{:S(2)}, u32[]{:S(2)}) collective-permute-start(bf16[192,256]{1,0:T(8,128)(2,1)S(1)} %get-tuple-element.59), channel_id=1, source_target_pairs={{0,32},{32,64},{64,96},{96,0},{1,33},{33,65},{65,97},{97,1},{2,34}... | collective-permute-start | bytes 294920 | tf_op jit(solution)/shard_map/ppermute | solution.py:601
  120.0 8.4 %collective-permute-start.6 = (bf16[192,256]{1,0:T(8,128)(2,1)S(1)}, bf16[192,256]{1,0:T(8,128)(2,1)S(1)}, u32[]{:S(2)}, u32[]{:S(2)}) collective-permute-start(bf16[192,256]{1,0:T(8,128)(2,1)S(1)} %get-tuple-element.60), channel_id=1, source_target_pairs={{0,64},{32,96},{64,0},{96,32},{1,65},{33,97},{65,1},{97,33},{2,66}... | collective-permute-start | bytes 294920 | tf_op jit(solution)/shard_map/ppermute | solution.py:601
  121.6 6.8 %collective-permute-start.8 = (bf16[192,256]{1,0:T(8,128)(2,1)S(1)}, bf16[192,256]{1,0:T(8,128)(2,1)S(1)}, u32[]{:S(2)}, u32[]{:S(2)}) collective-permute-start(bf16[192,256]{1,0:T(8,128)(2,1)S(1)} %get-tuple-element.61), channel_id=1, source_target_pairs={{0,96},{32,0},{64,32},{96,64},{1,97},{33,1},{65,33},{97,65},{2,98}... | collective-permute-start | bytes 294920 | tf_op jit(solution)/shard_map/ppermute | solution.py:601
  127.4 10.7 %collective-permute-start.5 = (bf16[192,256]{1,0:T(8,128)(2,1)S(1)}, bf16[192,256]{1,0:T(8,128)(2,1)S(1)}, u32[]{:S(2)}, u32[]{:S(2)}) collective-permute-start(bf16[192,256]{1,0:T(8,128)(2,1)S(1)} %collective-permute-done.4.b1), channel_id=1, source_target_pairs={{0,1},{1,0},{2,3},{3,2},{4,5},{5,4},{6,7},{7,6},{8,9},{9,8},{10,11... | collective-permute-start | bytes 294920 | tf_op jit(solution)/shard_map/ppermute | solution.py:597
  128.4 9.8 %collective-permute-start.7 = (bf16[192,256]{1,0:T(8,128)(2,1)S(1)}, bf16[192,256]{1,0:T(8,128)(2,1)S(1)}, u32[]{:S(2)}, u32[]{:S(2)}) collective-permute-start(bf16[192,256]{1,0:T(8,128)(2,1)S(1)} %collective-permute-done.6.b2), channel_id=1, source_target_pairs={{0,1},{1,0},{2,3},{3,2},{4,5},{5,4},{6,7},{7,6},{8,9},{9,8},{10,11... | collective-permute-start | bytes 294920 | tf_op jit(solution)/shard_map/ppermute | solution.py:597
  128.4 9.8 %collective-permute-start.9 = (bf16[192,256]{1,0:T(8,128)(2,1)S(1)}, bf16[192,256]{1,0:T(8,128)(2,1)S(1)}, u32[]{:S(2)}, u32[]{:S(2)}) collective-permute-start(bf16[192,256]{1,0:T(8,128)(2,1)S(1)} %collective-permute-done.8.b3), channel_id=1, source_target_pairs={{0,1},{1,0},{2,3},{3,2},{4,5},{5,4},{6,7},{7,6},{8,9},{9,8},{10,11... | collective-permute-start | bytes 294920 | tf_op jit(solution)/shard_map/ppermute | solution.py:597
  129.0 0.7 copy-start.20
  141.8 35.3 %copy-start.1 = (bf16[192,1024]{1,0:T(8,128)(2,1)S(1)}, bf16[192,1024]{1,0:T(8,128)(2,1)}, u32[]{:S(2)}) copy-start(bf16[192,1024]{1,0:T(8,128)(2,1)} %lru_ref.3) | copy-start | bytes 1179652
  141.8 24.7 %all-to-all-start.2 = ((bf16[16,32,1152]{2,1,0:T(8,128)(2,1)}), bf16[16,32,1152]{2,1,0:T(8,128)(2,1)S(1)}, u32[]{:S(2)}, u32[]{:S(2)}) async-start(bf16[16,32,1152]{2,1,0:T(8,128)(2,1)} %bitcast.16), calls=%async_computation.2 | async-start | bytes 2359296 | tf_op jit(solution)/shard_map/all_to_all | solution.py:640
  145.6 26.2 %collective-permute-start.15 = (bf16[1,1024]{1,0:T(2,128)(2,1)S(1)}, bf16[1,1024]{1,0:T(2,128)(2,1)S(1)}, u32[]{:S(2)}, u32[]{:S(2)}) collective-permute-start(bf16[1,1024]{1,0:T(2,128)(2,1)S(1)} %slice.6), channel_id=1, source_target_pairs={{0,2},{2,4},{4,6},{6,8},{8,10},{10,12},{12,14},{14,16},{16,18},{18... | collective-permute-start | bytes 6152 | tf_op jit(solution)/shard_map/ppermute | solution.py:630
  167.1 4.7 %collective-permute-start.12 = (f32[16,128]{1,0:T(8,128)S(1)}, f32[16,128]{1,0:T(8,128)S(1)}, u32[]{:S(2)}, u32[]{:S(2)}) collective-permute-start(f32[16,128]{1,0:T(8,128)S(1)} %get-tuple-element.69), channel_id=1, source_target_pairs={{32,0},{64,32},{96,64},{33,1},{65,33},{97,65},{34,2},{66,34},{98,6... | collective-permute-start | bytes 24584 | tf_op jit(solution)/shard_map/ppermute | solution.py:642
  168.4 5.9 %collective-permute-start.13 = (f32[16,128]{1,0:T(8,128)S(1)}, f32[16,128]{1,0:T(8,128)S(1)}, u32[]{:S(2)}, u32[]{:S(2)}) collective-permute-start(f32[16,128]{1,0:T(8,128)S(1)} %get-tuple-element.69), channel_id=1, source_target_pairs={{64,0},{96,32},{65,1},{97,33},{66,2},{98,34},{67,3},{99,35},{68,4}... | collective-permute-start | bytes 24584 | tf_op jit(solution)/shard_map/ppermute | solution.py:642
  169.7 7.4 %collective-permute-start.14 = (f32[16,128]{1,0:T(8,128)S(1)}, f32[16,128]{1,0:T(8,128)S(1)}, u32[]{:S(2)}, u32[]{:S(2)}) collective-permute-start(f32[16,128]{1,0:T(8,128)S(1)} %get-tuple-element.69), channel_id=1, source_target_pairs={{96,0},{97,1},{98,2},{99,3},{100,4},{101,5},{102,6},{103,7},{104,8... | collective-permute-start | bytes 24584 | tf_op jit(solution)/shard_map/ppermute | solution.py:642

commit v3 on v2

--- a/solution.py
+++ b/solution.py
@@ -79,7 +79,7 @@
 
 
 def mixed(*kinds):
-    spaces = {"h": pltpu.HBM, "v": pltpu.VMEM}
+    spaces = {"h": pltpu.HBM, "v": pltpu.VMEM, "a": pl.ANY}
     return [pl.BlockSpec(memory_space=pltpu.SMEM)] + [
         pl.BlockSpec(memory_space=spaces[k]) for k in "".join(kinds)
     ]
@@ -323,18 +323,19 @@
         cost_estimate=pl.CostEstimate(
             flops=3 * 2 * ROWS * D * FF, bytes_accessed=20_000_000, transcendentals=0
         ),
-    )(meta, perm, own, peer, hid, gg, gu)
+    )(meta, *in_hbm(perm, own, peer, hid, gg, gu))
 
 
 def combine_kernel(
-    meta, ids_hbm, ret_hbm, d_hbm, dm_ref, b0, b1, b2, b3, ids, ret, own, sems
+    meta, ids_hbm, ret, d_hbm, w_hbm, dm_ref, b0, b1, b2, b3, w_ref, ids, own, sems
 ):
     tp, z = meta[0], meta[1]
     cut = SLOTS // 4
     copies = fetch(
         [(ids_hbm, ids)]
-        + [(ret_hbm.at[k * cut : (k + 1) * cut, :], ret.at[k * cut : (k + 1) * cut, :]) for k in range(4)]
-        + [(d_hbm.at[:, lanes(2 * j + tp)], own.at[:, j * BLK : (j + 1) * BLK]) for j in range(4)],
+        + [(d_hbm.at[:, lanes(2 * j + tp)], own.at[:, j * BLK : (j + 1) * BLK]) for j in range(4)]
+        + [(w_hbm.at[:, lanes(2 * j + tp)], w_ref.at[j, :, :]) for j in range(4)]
+        + [(w_hbm.at[:, lanes(2 * j + 1 - tp)], w_ref.at[4 + j, :, :]) for j in range(4)],
         sems,
     )
     copies[0].wait()
@@ -345,35 +346,36 @@
         slot = lax.broadcasted_iota(jnp.int32, (TOK, cut), 1) + k * cut
         first = jnp.where((slot == c0) | (slot == c1), 1.0, 0.0).astype(BF)
         second = jnp.where((slot == c0 + CAP) | (slot == c1 + CAP), 1.0, 0.0).astype(BF)
-        copies[1 + k].wait()
         piece = ret[k * cut : (k + 1) * cut, :]
         low += dot(first, piece)
         high += dot(second, piece)
-    for copy in copies[5:]:
+    for copy in copies[1:5]:
         copy.wait()
     dm_ref[:, :512] = (own[:, :512].astype(F32) + low).astype(BF)
     dm_ref[:, 512:] = (own[:, 512:].astype(F32) + high).astype(BF)
     for k, ref in enumerate((b0, b1, b2, b3)):
         ref[...] = dm_ref[:, lanes(lax.rem(z + k, 4))]
-
-
-def combine(meta, ids, ret, d_out):
+    for copy in copies[5:]:
+        copy.wait()
+
+
+def combine(meta, ids, ret, d_out, w_out):
     return pl.pallas_call(
         combine_kernel,
         name="combine",
-        in_specs=mixed("hhh"),
-        out_specs=[pl.BlockSpec(memory_space=pltpu.VMEM)] * 5,
+        in_specs=mixed("hvhh"),
+        out_specs=[pl.BlockSpec(memory_space=pltpu.VMEM)] * 6,
         out_shape=[jax.ShapeDtypeStruct((TOK, HALF), BF)]
-        + [jax.ShapeDtypeStruct((TOK, BLK), BF)] * 4,
+        + [jax.ShapeDtypeStruct((TOK, BLK), BF)] * 4
+        + [jax.ShapeDtypeStruct((8, HALF, BLK), BF)],
         scratch_shapes=[
             pltpu.VMEM((2, TOK), jnp.int32),
-            pltpu.VMEM((SLOTS, HALF // 2), BF),
             pltpu.VMEM((TOK, HALF), BF),
-            pltpu.SemaphoreType.DMA((9,)),
+            pltpu.SemaphoreType.DMA((13,)),
         ],
         compiler_params=vm(12),
         cost_estimate=cost(1e9),
-    )(meta, *in_hbm(ids, ret, d_out))
+    )(meta, *in_hbm(ids), ret, *in_hbm(d_out, w_out))
 
 
 ROOT = 0.7978845608028654
@@ -423,56 +425,105 @@
     return carry
 
 
+def prep_kernel(
+    gate_hbm, lru_hbm, decay_hbm, before_ref, value_hbm, slope_hbm, rate_hbm, after_hbm, past_hbm,
+    gate, lru, decay, value, slope, rate, after, past, sems,
+):
+    for copy in fetch([(gate_hbm, gate), (lru_hbm, lru), (decay_hbm, decay)], sems):
+        copy.wait()
+    x = gate[...].astype(F32)
+    state = lru[...].astype(F32)
+    gelu, t = gelu_parts(x)
+    value[...] = gelu
+    out0 = fetch([(value, value_hbm)], sems.at[3:4])
+    grown = 0.5 * (1.0 + t) + 0.5 * x * (1.0 - t * t) * (ROOT * (1.0 + 3.0 * CUBE * x * x))
+    slope[...] = grown * state
+    out1 = fetch([(slope, slope_hbm)], sems.at[4:5])
+    rate[...] = jnp.exp(decay[...])
+    first = lax.broadcasted_iota(jnp.int32, (TOK, HALF), 0) == 0
+    prev = jnp.where(first, before_ref[...].astype(F32), pltpu.roll(state, 1, 0))
+    past[...] = rate[...] * prev
+    out2 = fetch([(rate, rate_hbm), (past, past_hbm)], sems.at[5:7])
+    carry = jnp.ones((1, HALF), F32)
+    for tile in reversed(range(TOK // 8)):
+        rows = slice(tile * 8, tile * 8 + 8)
+        decays, here = rate[rows, :], [None] * 8
+        for r in reversed(range(8)):
+            here[r] = carry
+            carry = decays[r : r + 1] * carry
+        after[rows, :] = jnp.concatenate(here, axis=0)
+    for copy in out0 + out1 + out2 + fetch([(after, after_hbm)], sems.at[7:8]):
+        copy.wait()
+
+
+def prep(gate_pre, lru_out, log_decay, before):
+    bf, wide = pltpu.VMEM((TOK, HALF), BF), pltpu.VMEM((TOK, HALF), F32)
+    return pl.pallas_call(
+        prep_kernel,
+        name="prep",
+        in_specs=mixed("hhhv")[1:],
+        out_specs=[pl.BlockSpec(memory_space=pltpu.HBM)] * 5,
+        out_shape=[pltpu.HBM((TOK, HALF), F32)] * 5,
+        scratch_shapes=[bf, bf] + [wide] * 6 + [pltpu.SemaphoreType.DMA((8,))],
+        compiler_params=vm(12),
+        cost_estimate=cost(1e9),
+    )(*in_hbm(gate_pre, lru_out, log_decay), before)
+
+
 def drive_kernel(
-    meta, own_ref, peer_ref, w_hbm, gate_hbm, lru_hbm, decay_hbm,
-    dgate_ref, drive_ref, head_ref, rate_ref, w, gate, lru, decay, sems,
+    meta, own_ref, peer_ref, w_ref, value_hbm, slope_hbm, rate_hbm, after_hbm, g0, g1, g2, g3,
+    dgate_ref, local_ref, head_ref, moved_ref, value, slope, rate, after, sems,
 ):
-    tp = meta[0]
-    parts = [2 * j + tp for j in range(4)] + [2 * j + 1 - tp for j in range(4)]
     copies = fetch(
-        [(w_hbm.at[:, lanes(part)], w.at[k, :, :]) for k, part in enumerate(parts)]
-        + [(gate_hbm, gate), (lru_hbm, lru), (decay_hbm, decay)],
+        [
+            (value_hbm, value),
+            (slope_hbm, slope),
+            (rate_hbm, rate),
+            (after_hbm.at[0:8, :], after),
+            (g0, moved_ref.at[0, :, :]),
+            (g1, moved_ref.at[1, :, :]),
+            (g2, moved_ref.at[2, :, :]),
+            (g3, moved_ref.at[3, :, :]),
+        ],
         sems,
     )
     grad = 0.0
     for k in range(8):
-        copies[k].wait()
         ref, j = (own_ref, peer_ref)[k // 4], k % 4
-        grad += dot_cols(ref[:, j * BLK : (j + 1) * BLK], w[k, :, :])
-    for copy in copies[8:]:
+        grad += dot_cols(ref[:, j * BLK : (j + 1) * BLK], w_ref[k, :, :])
+    copies[0].wait()
+    local_ref[...] = grad * value[...]
+    copies[1].wait()
+    dgate_ref[...] = (grad * slope[...]).astype(BF)
+    copies[2].wait()
+    copies[3].wait()
+
+    def visit(rows, here, later):
+        local_ref[rows, :] = here
+
+    head_ref[0:8, :] = tile_of(scan_rows(local_ref, rate, jnp.zeros((1, HALF), F32), visit))
+    head_ref[8:16, :] = tile_of(after[0:1, :] * rate[0:1, :])
+    for copy in copies[4:]:
         copy.wait()
-    x = gate[...].astype(F32)
-    value, t = gelu_parts(x)
-    slope = 0.5 * (1.0 + t) + 0.5 * x * (1.0 - t * t) * (ROOT * (1.0 + 3.0 * CUBE * x * x))
-    dgate_ref[...] = (grad * lru[...].astype(F32) * slope).astype(BF)
-    drive_ref[...] = grad * value
-    rate_ref[...] = jnp.exp(decay[...])
-    head_ref[0:8, :] = tile_of(scan_rows(drive_ref, rate_ref, jnp.zeros((1, HALF), F32), None))
-    head_ref[8:16, :] = tile_of(jnp.exp(jnp.sum(decay[...], axis=0, keepdims=True)))
-
-
-def drive(meta, own, peer, w_out, gate_pre, lru_out, log_decay):
+
+
+def drive(meta, own, peer, w, value, slope, rate, after, gated):
+    wide = pltpu.VMEM((TOK, HALF), F32)
     return pl.pallas_call(
         drive_kernel,
         name="drive",
-        in_specs=mixed("vvhhhh"),
+        in_specs=mixed("vvvhhhhaaaa"),
         out_specs=[pl.BlockSpec(memory_space=pltpu.VMEM)] * 4,
         out_shape=[
             jax.ShapeDtypeStruct((TOK, HALF), BF),
             jax.ShapeDtypeStruct((TOK, HALF), F32),
             jax.ShapeDtypeStruct((16, 128), F32),
-            jax.ShapeDtypeStruct((TOK, HALF), F32),
+            jax.ShapeDtypeStruct((4, TOK, HALF), BF),
         ],
-        scratch_shapes=[
-            pltpu.VMEM((8, HALF, BLK), BF),
-            pltpu.VMEM((TOK, HALF), BF),
-            pltpu.VMEM((TOK, HALF), BF),
-            pltpu.VMEM((TOK, HALF), F32),
-            pltpu.SemaphoreType.DMA((11,)),
-        ],
-        compiler_params=vm(16),
+        scratch_shapes=[wide, wide, wide, pltpu.VMEM((8, HALF), F32), pltpu.SemaphoreType.DMA((8,))],
+        compiler_params=vm(12),
         cost_estimate=cost(2e9),
-    )(meta, own, peer, *in_hbm(w_out, gate_pre, lru_out, log_decay))
+    )(meta, own, peer, w, *in_hbm(value, slope, rate, after), *gated)
 
 
 def link_kernel(meta, shares_ref, within_ref, after_ref, plane_ref):
@@ -510,61 +561,49 @@
     )(meta, shares)
 
 
-def finish_kernel(
-    within_ref, after_ref, p1, p2, p3, drive_ref, rate_ref, lru_ref, before_ref, dd_ref, dl_ref,
-    prev_ref,
-):
+def finish_kernel(within_ref, after_ref, p1, p2, p3, local_ref, suffix_ref, past_ref, dd_ref, dl_ref):
     planes = p3[0:8, :]
     planes = p2[0:8, :] + p2[8:16, :] * planes
     planes = p1[0:8, :] + p1[8:16, :] * planes
-    carry = line_of(within_ref[...] + after_ref[...] * planes)
-    state = lru_ref[...].astype(F32)
-    first = lax.broadcasted_iota(jnp.int32, (TOK, HALF), 0) == 0
-    prev_ref[...] = jnp.where(first, before_ref[...].astype(F32), pltpu.roll(state, 1, 0))
-
-    def visit(rows, here, later):
-        dd_ref[rows, :] = here
-        dl_ref[rows, :] = later * prev_ref[rows, :]
-
-    scan_rows(drive_ref, rate_ref, carry, visit)
-
-
-def finish(within, after, planes, drive_value, rate, lru_out, before):
+    incoming = line_of(within_ref[...] + after_ref[...] * planes)
+    for tile in range(TOK // 8):
+        rows = slice(tile * 8, tile * 8 + 8)
+        value = local_ref[rows, :] + suffix_ref[rows, :] * incoming
+        dd_ref[rows, :] = value
+        dl_ref[rows, :] = value * past_ref[rows, :]
+
+
+def finish(within, after, planes, local, suffix, past):
     return pl.pallas_call(
         finish_kernel,
         name="finish",
         out_shape=[jax.ShapeDtypeStruct((TOK, HALF), F32)] * 2,
-        scratch_shapes=[pltpu.VMEM((TOK, HALF), F32)],
         compiler_params=vm(8),
-        cost_estimate=cost(1e8),
-    )(within, after, *planes, drive_value, rate, lru_out, before)
-
-
-def outer_own_kernel(b0, b1, b2, b3, g0, g1, g2, g3, out_ref, moved, sems):
-    copies = fetch([(g, moved.at[k, :, :]) for k, g in enumerate((g0, g1, g2, g3))], sems)
+        cost_estimate=cost(1e9),
+    )(within, after, *planes, local, suffix, past)
+
+
+def outer_own_kernel(b0, b1, b2, b3, moved, out_ref):
     total = 0.0
     for k, ref in enumerate((b0, b1, b2, b3)):
-        copies[k].wait()
         total += dot_rows(ref[...], moved[k, :, :])
     out_ref[...] = total.astype(BF)
 
 
-def outer_own(blocks, gated):
+def outer_own(blocks, moved):
     return pl.pallas_call(
         outer_own_kernel,
         name="outer_own",
-        in_specs=mixed("vvvvhhhh")[1:],
+        in_specs=mixed("vvvvv")[1:],
         out_specs=pl.BlockSpec(memory_space=pltpu.VMEM),
         out_shape=jax.ShapeDtypeStruct((BLK, HALF), BF),
-        scratch_shapes=[pltpu.VMEM((4, TOK, HALF), BF), pltpu.SemaphoreType.DMA((4,))],
-        compiler_params=vm(10),
+        compiler_params=vm(8),
         cost_estimate=cost(1e9),
-    )(*blocks, *in_hbm(*gated))
-
-
-def outer_kernel(meta, p0, p1, p2, p3, g0, g1, g2, g3, own_ref, head_ref, out_ref, moved, sems):
+    )(*blocks, moved)
+
+
+def outer_kernel(meta, p0, p1, p2, p3, moved, own_ref, head_ref, out_ref):
     tp, z = meta[0], meta[1]
-    copies = fetch([(g, moved.at[k, :, :]) for k, g in enumerate((g0, g1, g2, g3))], sems)
     out_ref[lanes(tp), 0:HALF] = own_ref[...]
     value = head_ref[...]
     high = value.astype(BF).astype(F32)
@@ -572,25 +611,22 @@
     tile = jnp.concatenate([high[0:8], low[0:8], high[8:16], low[8:16]], axis=0).astype(BF)
     for k in range(16):
         out_ref[k * 32 : (k + 1) * 32, HALF:] = tile
-    copies[0].wait()
     total = dot_rows(p0[:, lanes(z)], moved[0, :, :])
     for k, ref in ((1, p1), (2, p2), (3, p3)):
-        copies[k].wait()
         total += dot_rows(ref[...], moved[k, :, :])
     out_ref[lanes(1 - tp), 0:HALF] = total.astype(BF)
 
 
-def outer(meta, peer, gated, own, head):
+def outer(meta, peer, moved, own, head):
     return pl.pallas_call(
         outer_kernel,
         name="outer",
-        in_specs=mixed("vvvvhhhhvv"),
+        in_specs=mixed("vvvvvvv"),
         out_specs=pl.BlockSpec(memory_space=pltpu.VMEM),
         out_shape=jax.ShapeDtypeStruct((2 * BLK, HALF + 128), BF),
-        scratch_shapes=[pltpu.VMEM((4, TOK, HALF), BF), pltpu.SemaphoreType.DMA((4,))],
-        compiler_params=vm(10),
+        compiler_params=vm(8),
         cost_estimate=cost(1e9),
-    )(meta, *peer, *in_hbm(*gated), own, head)
+    )(meta, *peer, moved, own, head)
 
 
 def swapped(value):
@@ -628,19 +664,21 @@
     back, moving, last = lax.optimization_barrier((back, gated, lru_out[-1:]))
     turn1, turn3 = turned(moving, 1), turned(moving, 3)
     before = lax.ppermute(last, SP, [(s, s + 1) for s in range(NSP - 1)])
+    value, slope, rate, suffix, past = prep(gate_pre, lru_out, log_decay, before)
     grads = weight_grads(meta, perm, got, got_peer, hid, gg, gu)
-    ret, grad_gate, grad_up, grad_down = lax.optimization_barrier((ret, *grads))
-    dm, *blocks = combine(meta, ids, ret.reshape(SLOTS, HALF // 2), d_out)
+    ret, rate, grad_gate, grad_up, grad_down = lax.optimization_barrier((ret, rate, *grads))
+    dm, *blocks, w = combine(meta, ids, ret.reshape(SLOTS, HALF // 2), d_out, w_out)
     dm_peer = swapped(dm)
     own = (blocks[0], *(turned(blocks[k], k) for k in (1, 2, 3)))
-    d_gate, drive_value, head, rate = drive(meta, dm, dm_peer, w_out, gate_pre, lru_out, log_decay)
+    d_gate, local, head, moved = drive(
+        meta, dm, dm_peer, w, value, slope, rate, suffix, (gated, turn1, turn2, turn3)
+    )
     peer = (dm_peer, *(swapped(own[k]) for k in (1, 2, 3)))
-    all_gated = (gated, turn1, turn2, turn3)
-    share = outer(meta, peer, all_gated, outer_own(own, all_gated), head)
+    share = outer(meta, peer, moved, outer_own(own, moved), head)
     shares = lax.all_to_all(share.reshape(16, 32, HALF + 128), ("y", "x"), 0, 0, tiled=True)
     within, after, plane = link(meta, shares)
     planes = [lax.ppermute(plane, "z", [(s, s - k) for s in range(k, 4)]) for k in (1, 2, 3)]
-    d_drive, d_log_decay = finish(within, after, planes, drive_value, rate, lru_out, before)
+    d_drive, d_log_decay = finish(within, after, planes, local, suffix, past)
     grad_out_proj = jnp.sum(shares[:, :, :HALF].astype(F32), axis=0)
     return (
         grad_gate[None], grad_up[None], grad_down[None], grad_out_proj, d_gate, d_drive, d_log_decay,

time: 181 us -> 175 us (0.967)
  blocking collectives: 52.2 us -> 74.4 us
  waiting for transfers between devices: 38.8 us -> 19 us
  local copies, waits for them, and re-layouts: 7.76 us -> 0.09 us
  starting transfers between devices: 28.9 us -> 26.2 us
    all_to_all x0 -> x1, blocking collectives: none -> 22.2 us  [on_device(): lax.all_to_all(share.reshape(16, 32, HALF + 128), ('y', 'x'), 0, 0, tiled...]
    all_to_all x1 -> x0, waiting for transfers between devices: 17.7 us -> none  [on_device(): lax.all_to_all(share.reshape(16, 32, HALF + 128), ('y', 'x'), 0, 0, tiled...]
    unnamed x42 -> x28, local copies, waits for them, and re-layouts: 7.75 us -> 0.08 us
    all_to_all x1 -> x0, starting transfers between devices: 3.84 us -> none  [on_device(): lax.all_to_all(share.reshape(16, 32, HALF + 128), ('y', 'x'), 0, 0, tiled...]
    pallas_call x1, Pallas kernels: 11.3 us -> 14.4 us  [weight_grads(): pl.pallas_call(weight_kernel, name='weight_grads', grid_spec=pltpu.Prefet...]
    all_to_all x1, waiting for transfers between devices: 2.41 us -> 0.01 us  [on_device(): lax.all_to_all(back.reshape(NSP, CHUNK, HALF // 2), SP, 0, 0, tiled=True)]
    pallas_call x4 -> x5, Pallas kernels: 15.3 us -> 14.1 us  [the longest x1 4.57 us: drive(): pl.pallas_call(drive_kernel, name='drive', in_specs=mixed('vvvhhhhaaaa'),...]
  transfers between devices with their start and end apart: 18 -> 17, of which waited for: 7 -> 6; matrix products, arithmetic and copies ran while one was open for 0% -> 0% of each run, Pallas kernels for 18% -> 21%
where the time goes in v3:
time: 175 us; the launch traced here: 172 us
  blocking collectives  74.4 us (43%)
  Pallas kernels  50.9 us (29%)
  starting transfers between devices  26.2 us (15%)
  waiting for transfers between devices  19 us (11%)
    all_to_all x1, blocking collectives, on_device(): got = lax.all_to_all(sent.reshape(NSP, CHUNK, HALF), SP, 0, 0, tiled=True)  52.2 us
    all_to_all x1, blocking collectives, on_device(): lax.all_to_all(share.reshape(16, 32, HALF + 128), ('y', 'x'), 0, 0, tiled...  22.2 us
    pallas_call x1, Pallas kernels, weight_grads(): pl.pallas_call(weight_kernel, name='weight_grads', grid_spec=pltpu.Prefet...  14.4 us
    ppermute x6, waiting for transfers between devices, turned(): return lax.ppermute(value, 'z', [(s, (s + steps) % 4) for s in range(4)])  12.8 us
    ppermute x6, starting transfers between devices, turned(): return lax.ppermute(value, 'z', [(s, (s + steps) % 4) for s in range(4)])  7.43 us
    pallas_call x1, Pallas kernels, expert_peer(): pl.pallas_call(peer_kernel, name='expert_peer', in_specs=whole(9), out_sp...  7.02 us
    ppermute x6, starting transfers between devices, swapped(): return lax.ppermute(value, 'tp', [(0, 1), (1, 0)])  6.94 us
    ppermute x3, waiting for transfers between devices, on_device(): lax.ppermute(plane, 'z', [(s, s - k) for s in range(k, 4)])  5.3 us
  transfers between devices with their start and end apart: 17, of which 6 were waited for; matrix products, arithmetic and copies ran while one was open for 0% of the time, Pallas kernels for 21%

profile of v3, /device:TPU:1, one launch (start us, length us, event | category | flops | bytes accessed | tf_op | source)
XLA Modules:
  0.0 172.5 jit_solution(5522978674387326258)
XLA Ops:
  0.6 0.1 pad_add_fusion.meta
  0.7 5.1 %pack.1 = bf16[1536,1024]{1,0:T(8,128)(2,1)S(1)} custom-call(s32[4]{0:T(128)S(1)} %pad_add_fusion.meta, s32[2,192]{1,0:T(2,128)} %bitcast.31, f32[2,192]{1,0:T(2,128)} %bitcast.33, bf16[192,2048]{1,0:T(8,128)(2,1)} %x_hbm.1, bf16[192,2048]{1,0:T(8,128)(2,1)} %d_hbm.3), custom_call_target="tpu_custom_call" | custom-call | tf_op jit(solution)/shard_map/pack/pallas_call | solution.py:138
  5.9 0.0 copy-start.2
  5.9 0.0 copy-start.3
  5.9 0.0 copy-start.5
  5.9 0.0 copy-start.6
  5.9 0.0 copy-start.7
  5.9 0.0 copy-start.8
  5.9 52.2 %all_to_all.15 = bf16[64,24,1024]{2,1,0:T(8,128)(2,1)S(1)} all-to-all(bf16[64,24,1024]{2,1,0:T(8,128)(2,1)S(1)} %bitcast.17), channel_id=1, replica_groups=mesh['z'=4,'y'=4,'x'=4,'tp'=2] {'z','y','x'}, dimensions={0} | all-to-all | bytes 6291456 | tf_op jit(solution)/shard_map/all_to_all | solution.py:651
  58.2 2.1 %collective-permute-start = (bf16[1536,1024]{1,0:T(8,128)(2,1)S(1)}, bf16[1536,1024]{1,0:T(8,128)(2,1)S(1)}, u32[]{:S(2)}, u32[]{:S(2)}) collective-permute-start(bf16[1536,1024]{1,0:T(8,128)(2,1)S(1)} %bitcast.20), channel_id=1, source_target_pairs={{0,1},{1,0},{2,3},{3,2},{4,5},{5,4},{6,7},{7,6},{8,9},{9,8},{10,11... | collective-permute-start | bytes 9437192 | tf_op jit(solution)/shard_map/ppermute | solution.py:633
  60.3 0.3 early.1.g0
  60.6 0.0 copy-start.9
  60.7 4.0 %expert_own.1 = (f32[768,512]{1,0:T(8,128)S(1)}, f32[768,512]{1,0:T(8,128)S(1)}, f32[768,512]{1,0:T(8,128)S(1)}) custom-call(s32[4]{0:T(128)S(1)} %pad_add_fusion.meta, bf16[192,192]{1,0:T(8,128)(2,1)S(1)} %copy-done.8, bf16[1536,1024]{1,0:T(8,128)(2,1)S(1)} %bitcast.21, bf16[2048,512]{1,0:T(8,128)(2,1)S(1)} %bitcast.25, bf16[2048,512]{1,0:T(8,128)(2,1)S(1)} %bitcast.28, ...), custom_call_target="tpu_custom_call" | custom-call | flops 4000000000 | tf_op jit(solution)/shard_map/expert_own/pallas_call | solution.py:216
  64.7 0.9 collective-permute-done.peer_ref
  65.6 7.0 %expert_peer.1 = (bf16[768,512]{1,0:T(8,128)(2,1)S(1)}, bf16[768,512]{1,0:T(8,128)(2,1)S(1)}, bf16[768,512]{1,0:T(8,128)(2,1)S(1)}, bf16[1536,512]{1,0:T(8,128)(2,1)S(1)}) custom-call(s32[4]{0:T(128)S(1)} %pad_add_fusion.meta, bf16[192,192]{1,0:T(8,128)(2,1)S(1)} %copy-done.8, bf16[192,192]{1,0:T(8,128)(2,1)S(1)} %copy-done.9, ...), custom_call_target="tpu_custom_call" | custom-call | flops 6000000000 | tf_op jit(solution)/shard_map/expert_peer/pallas_call | solution.py:247
  72.6 0.0 copy-start.11
  72.6 0.4 collective-permute-start.1
  73.1 0.4 collective-permute-start.2
  73.4 2.8 %expert_back.1.a_ref = bf16[1536,512]{1,0:T(8,128)(2,1)S(1)} custom-call(s32[4]{0:T(128)S(1)} %pad_add_fusion.meta, bf16[192,192]{1,0:T(8,128)(2,1)S(1)} %copy-done.9, bf16[768,512]{1,0:T(8,128)(2,1)S(1)} %get-tuple-element.52.gg_ref, bf16[768,512]{1,0:T(8,128)(2,1)S(1)} %get-tuple-element.53.gu_ref, bf16[2048,512]{1,0:T(8,128)(2,1)S(1)} %bitcast.27, ...), custom_call_target="tpu_custom_call" | custom-call | flops 3000000000 | tf_op jit(solution)/shard_map/expert_back/pallas_call | solution.py:265
  76.3 1.3 part_sum.1
  77.6 7.6 %collective-permute-done.2.g2 = bf16[192,1024]{1,0:T(8,128)(2,1)S(1)} collective-permute-done((bf16[192,1024]{1,0:T(8,128)(2,1)S(1)}, bf16[192,1024]{1,0:T(8,128)(2,1)S(1)}, u32[]{:S(2)}, u32[]{:S(2)}) %collective-permute-start.2) | collective-permute-done | bytes 393248 | tf_op jit(solution)/shard_map/ppermute | solution.py:637
  85.1 4.8 %all-to-all-start.1 = ((bf16[64,24,512]{2,1,0:T(8,128)(2,1)}), bf16[64,24,512]{2,1,0:T(8,128)(2,1)S(1)}, u32[]{:S(2)}, u32[]{:S(2)}) async-start(bf16[64,24,512]{2,1,0:T(8,128)(2,1)} %bitcast.11), calls=%async_computation.1 | async-start | bytes 3145728 | tf_op jit(solution)/shard_map/all_to_all | solution.py:663
  89.9 3.1 %collective-permute-start.3 = (bf16[1,1024]{1,0:T(2,128)(2,1)S(1)}, bf16[1,1024]{1,0:T(2,128)(2,1)S(1)}, u32[]{:S(2)}, u32[]{:S(2)}) collective-permute-start(bf16[1,1024]{1,0:T(2,128)(2,1)S(1)} %slice.6), channel_id=1, source_target_pairs={{0,2},{2,4},{4,6},{6,8},{8,10},{10,12},{12,14},{14,16},{16,18},{18... | collective-permute-start | bytes 6152 | tf_op jit(solution)/shard_map/ppermute | solution.py:666
  93.1 14.4 %weight_grads.1 = (f32[2048,512]{1,0:T(8,128)}, f32[2048,512]{1,0:T(8,128)}, f32[512,2048]{1,0:T(8,128)}) custom-call(s32[4]{0:T(128)S(1)} %pad_add_fusion.meta, bf16[192,192]{1,0:T(8,128)(2,1)} %constant.25.clone.perm_ref, bf16[1536,1024]{1,0:T(8,128)(2,1)} %bitcast.22, bf16[1536,1024]{1,0:T(8,128)(2,1)} %copy-done.4, bf16[768,512]{1,0:T(8,128)(2,1)} %copy-done.13, ...), custom_call_target="tpu_custom_call" | custom-call | flops 4831838208 | bytes 20000000 | tf_op jit(solution)/shard_map/weight_grads/pallas_call | solution.py:296
  107.5 1.2 collective-permute-start.11
  108.7 1.5 collective-permute-start.12
  110.2 4.4 %prep.1 = (f32[192,1024]{1,0:T(8,128)}, f32[192,1024]{1,0:T(8,128)}, f32[192,1024]{1,0:T(8,128)}, f32[192,1024]{1,0:T(8,128)}, f32[192,1024]{1,0:T(8,128)}) custom-call(bf16[192,1024]{1,0:T(8,128)(2,1)} %gate_hbm.1, bf16[192,1024]{1,0:T(8,128)(2,1)} %lru_hbm.1, f32[192,1024]{1,0:T(8,128)} %decay_hbm.1, bf16[1,1024]{1,0:T(2,128)(2,1)S(1)} %collective-permute-done.3.before_ref), custom_call_target="tpu_custom_call" | custom-call | flops 1000000000 | tf_op jit(solution)/shard_map/prep/pallas_call | solution.py:461
  114.6 3.1 %combine.1 = (bf16[192,1024]{1,0:T(8,128)(2,1)S(1)}, bf16[192,256]{1,0:T(8,128)(2,1)S(1)}, bf16[192,256]{1,0:T(8,128)(2,1)S(1)}, bf16[192,256]{1,0:T(8,128)(2,1)...) custom-call(s32[4]{0:T(128)S(1)} %pad_add_fusion.meta, s32[2,192]{1,0:T(2,128)} %bitcast.32, ...), custom_call_target="tpu_custom_call" | custom-call | flops 1000000000 | tf_op jit(solution)/shard_map/combine/pallas_call | solution.py:363
  117.7 2.5 %collective-permute-start.4 = (bf16[192,1024]{1,0:T(8,128)(2,1)S(1)}, bf16[192,1024]{1,0:T(8,128)(2,1)S(1)}, u32[]{:S(2)}, u32[]{:S(2)}) collective-permute-start(bf16[192,1024]{1,0:T(8,128)(2,1)S(1)} %get-tuple-element.67.own_ref), channel_id=1, source_target_pairs={{0,1},{1,0},{2,3},{3,2},{4,5},{5,4},{6,7},{7,6},{8,9},{9,8},{10,11... | collective-permute-start | bytes 1179656 | tf_op jit(solution)/shard_map/ppermute | solution.py:633
  120.2 3.0 %collective-permute-start.9 = (bf16[192,256]{1,0:T(8,128)(2,1)S(1)}, bf16[192,256]{1,0:T(8,128)(2,1)S(1)}, u32[]{:S(2)}, u32[]{:S(2)}) collective-permute-start(bf16[192,256]{1,0:T(8,128)(2,1)S(1)} %get-tuple-element.70), channel_id=1, source_target_pairs={{0,96},{32,0},{64,32},{96,64},{1,97},{33,1},{65,33},{97,65},{2,98}... | collective-permute-start | bytes 294920 | tf_op jit(solution)/shard_map/ppermute | solution.py:637
  123.2 1.4 collective-permute-start.7
  124.5 0.7 collective-permute-done.9.b3
  125.3 0.9 collective-permute-start.10
  126.2 4.6 %collective-permute-done.5.b1 = bf16[192,256]{1,0:T(8,128)(2,1)S(1)} collective-permute-done((bf16[192,256]{1,0:T(8,128)(2,1)S(1)}, bf16[192,256]{1,0:T(8,128)(2,1)S(1)}, u32[]{:S(2)}, u32[]{:S(2)}) %collective-permute-start.5) | collective-permute-done | bytes 98336 | tf_op jit(solution)/shard_map/ppermute | solution.py:637
  130.7 1.0 collective-permute-start.6
  131.7 0.0 collective-permute-start.8
  131.7 4.6 %drive.1 = (bf16[192,1024]{1,0:T(8,128)(2,1)}, f32[192,1024]{1,0:T(8,128)S(1)}, f32[16,128]{1,0:T(8,128)S(1)}, bf16[4,192,1024]{2,1,0:T(8,128)(2,1)S(1)}) custom-call(s32[4]{0:T(128)S(1)} %pad_add_fusion.meta, bf16[192,1024]{1,0:T(8,128)(2,1)S(1)} %get-tuple-element.67.own_ref, bf16[192,1024]{1,0:T(8,128)(2,1)S(1)} %collective-permute-done.4.peer_ref.p0, ...), custom_call_target="tpu_custom_call" | custom-call | flops 2000000000 | tf_op jit(solution)/shard_map/drive/pallas_call | solution.py:512
  136.3 0.7 outer_own.1.own_ref
  137.1 1.3 outer.1
  138.4 22.2 %all_to_all.16.shares_ref = bf16[16,32,1152]{2,1,0:T(8,128)(2,1)S(1)} all-to-all(bf16[16,32,1152]{2,1,0:T(8,128)(2,1)S(1)} %bitcast.19), channel_id=1, replica_groups=mesh['z'=4,'y'=4,'x'=4,'tp'=2] {'y','x'}, dimensions={0} | all-to-all | bytes 2359296 | tf_op jit(solution)/shard_map/all_to_all | solution.py:678
  160.6 0.6 link.1
  161.2 1.3 collective-permute-start.13
  162.5 1.3 collective-permute-start.14
  163.8 1.3 collective-permute-start.15
  165.1 0.8 convert_reduce_fusion
  165.9 2.5 %collective-permute-done.14.p2 = f32[16,128]{1,0:T(8,128)S(1)} collective-permute-done((f32[16,128]{1,0:T(8,128)S(1)}, f32[16,128]{1,0:T(8,128)S(1)}, u32[]{:S(2)}, u32[]{:S(2)}) %collective-permute-start.14) | collective-permute-done | bytes 8224 | tf_op jit(solution)/shard_map/ppermute | solution.py:680
  168.4 2.8 %collective-permute-done.15.p3 = f32[16,128]{1,0:T(8,128)S(1)} collective-permute-done((f32[16,128]{1,0:T(8,128)S(1)}, f32[16,128]{1,0:T(8,128)S(1)}, u32[]{:S(2)}, u32[]{:S(2)}) %collective-permute-start.15) | collective-permute-done | bytes 8224 | tf_op jit(solution)/shard_map/ppermute | solution.py:680
  171.2 1.3 finish.1
  (33 shorter events, 0.1 us)
Async XLA Ops:
  5.9 54.4 %copy-start.2 = (bf16[192,1024]{1,0:T(8,128)(2,1)S(1)}, bf16[192,1024]{1,0:T(8,128)(2,1)}, u32[]{:S(2)}) copy-start(bf16[192,1024]{1,0:T(8,128)(2,1)} %lru_hbm.1) | copy-start | bytes 1179652
  5.9 54.4 %copy-start.3 = (bf16[192,1024]{1,0:T(8,128)(2,1)S(1)}, bf16[192,1024]{1,0:T(8,128)(2,1)}, u32[]{:S(2)}) copy-start(bf16[192,1024]{1,0:T(8,128)(2,1)} %gate_hbm.1) | copy-start | bytes 1179652
  5.9 54.7 %copy-start.5 = (bf16[1,512,2048]{2,1,0:T(8,128)(2,1)S(1)}, bf16[1,512,2048]{2,1,0:T(8,128)(2,1)}, u32[]{:S(2)}) copy-start(bf16[1,512,2048]{2,1,0:T(8,128)(2,1)} %param.23) | copy-start | bytes 6291460
  5.9 54.7 %copy-start.6 = (bf16[1,2048,512]{2,1,0:T(8,128)(2,1)S(1)}, bf16[1,2048,512]{2,1,0:T(8,128)(2,1)}, u32[]{:S(2)}) copy-start(bf16[1,2048,512]{2,1,0:T(8,128)(2,1)} %param.21) | copy-start | bytes 6291460
  5.9 54.7 %copy-start.7 = (bf16[1,2048,512]{2,1,0:T(8,128)(2,1)S(1)}, bf16[1,2048,512]{2,1,0:T(8,128)(2,1)}, u32[]{:S(2)}) copy-start(bf16[1,2048,512]{2,1,0:T(8,128)(2,1)} %param.22) | copy-start | bytes 6291460
  5.9 54.7 %copy-start.8 = (bf16[192,192]{1,0:T(8,128)(2,1)S(1)}, bf16[192,192]{1,0:T(8,128)(2,1)}, u32[]{:S(2)}) copy-start(bf16[192,192]{1,0:T(8,128)(2,1)} %constant.25.clone.perm_ref) | copy-start | bytes 221188
  58.1 6.5 %copy-start = (bf16[64,24,1024]{2,1,0:T(8,128)(2,1)}, bf16[64,24,1024]{2,1,0:T(8,128)(2,1)S(1)}, u32[]{:S(2)}) copy-start(bf16[64,24,1024]{2,1,0:T(8,128)(2,1)S(1)} %all_to_all.15) | copy-start | bytes 9437188
  58.2 7.4 %collective-permute-start = (bf16[1536,1024]{1,0:T(8,128)(2,1)S(1)}, bf16[1536,1024]{1,0:T(8,128)(2,1)S(1)}, u32[]{:S(2)}, u32[]{:S(2)}) collective-permute-start(bf16[1536,1024]{1,0:T(8,128)(2,1)S(1)} %bitcast.20), channel_id=1, source_target_pairs={{0,1},{1,0},{2,3},{3,2},{4,5},{5,4},{6,7},{7,6},{8,9},{9,8},{10,11... | collective-permute-start | bytes 9437192 | tf_op jit(solution)/shard_map/ppermute | solution.py:633
  60.6 4.9 %copy-start.9 = (bf16[192,192]{1,0:T(8,128)(2,1)S(1)}, bf16[192,192]{1,0:T(8,128)(2,1)}, u32[]{:S(2)}) copy-start(bf16[192,192]{1,0:T(8,128)(2,1)} %constant.26.clone.perm_t_ref) | copy-start | bytes 221188
  65.6 7.0 %copy-start.4 = (bf16[1536,1024]{1,0:T(8,128)(2,1)}, bf16[1536,1024]{1,0:T(8,128)(2,1)S(1)}, u32[]{:S(2)}) copy-start(bf16[1536,1024]{1,0:T(8,128)(2,1)S(1)} %collective-permute-done.peer_ref) | copy-start | bytes 9437188
  72.6 3.6 %copy-start.11 = (bf16[768,512]{1,0:T(8,128)(2,1)}, bf16[768,512]{1,0:T(8,128)(2,1)S(1)}, u32[]{:S(2)}) copy-start(bf16[768,512]{1,0:T(8,128)(2,1)S(1)} %get-tuple-element.52.gg_ref) | copy-start | bytes 2359300
  72.6 3.6 %copy-start.12 = (bf16[768,512]{1,0:T(8,128)(2,1)}, bf16[768,512]{1,0:T(8,128)(2,1)S(1)}, u32[]{:S(2)}) copy-start(bf16[768,512]{1,0:T(8,128)(2,1)S(1)} %get-tuple-element.53.gu_ref) | copy-start | bytes 2359300
  72.6 3.6 %copy-start.13 = (bf16[768,512]{1,0:T(8,128)(2,1)}, bf16[768,512]{1,0:T(8,128)(2,1)S(1)}, u32[]{:S(2)}) copy-start(bf16[768,512]{1,0:T(8,128)(2,1)S(1)} %get-tuple-element.59.hid_ref) | copy-start | bytes 2359300
  72.6 3.6 %collective-permute-start.1 = (bf16[1536,512]{1,0:T(8,128)(2,1)S(1)}, bf16[1536,512]{1,0:T(8,128)(2,1)S(1)}, u32[]{:S(2)}, u32[]{:S(2)}) collective-permute-start(bf16[1536,512]{1,0:T(8,128)(2,1)S(1)} %get-tuple-element.54), channel_id=1, source_target_pairs={{0,1},{1,0},{2,3},{3,2},{4,5},{5,4},{6,7},{7,6},{8,9},{9,8},{10,11... | collective-permute-start | bytes 4718600 | tf_op jit(solution)/shard_map/ppermute | solution.py:633
  73.1 12.0 %collective-permute-start.2 = (bf16[192,1024]{1,0:T(8,128)(2,1)S(1)}, bf16[192,1024]{1,0:T(8,128)(2,1)S(1)}, u32[]{:S(2)}, u32[]{:S(2)}) collective-permute-start(bf16[192,1024]{1,0:T(8,128)(2,1)S(1)} %early.1.g0), channel_id=1, source_target_pairs={{0,64},{32,96},{64,0},{96,32},{1,65},{33,97},{65,1},{97,33},{2,66}... | collective-permute-start | bytes 1179656 | tf_op jit(solution)/shard_map/ppermute | solution.py:637
  85.1 29.5 %all-to-all-start.1 = ((bf16[64,24,512]{2,1,0:T(8,128)(2,1)}), bf16[64,24,512]{2,1,0:T(8,128)(2,1)S(1)}, u32[]{:S(2)}, u32[]{:S(2)}) async-start(bf16[64,24,512]{2,1,0:T(8,128)(2,1)} %bitcast.11), calls=%async_computation.1 | async-start | bytes 3145728 | tf_op jit(solution)/shard_map/all_to_all | solution.py:663
  89.9 20.2 %collective-permute-start.3 = (bf16[1,1024]{1,0:T(2,128)(2,1)S(1)}, bf16[1,1024]{1,0:T(2,128)(2,1)S(1)}, u32[]{:S(2)}, u32[]{:S(2)}) collective-permute-start(bf16[1,1024]{1,0:T(2,128)(2,1)S(1)} %slice.6), channel_id=1, source_target_pairs={{0,2},{2,4},{4,6},{6,8},{8,10},{10,12},{12,14},{14,16},{16,18},{18... | collective-permute-start | bytes 6152 | tf_op jit(solution)/shard_map/ppermute | solution.py:666
  107.5 15.7 %collective-permute-start.11 = (bf16[192,1024]{1,0:T(8,128)(2,1)S(1)}, bf16[192,1024]{1,0:T(8,128)(2,1)S(1)}, u32[]{:S(2)}, u32[]{:S(2)}) collective-permute-start(bf16[192,1024]{1,0:T(8,128)(2,1)S(1)} %early.1.g0), channel_id=1, source_target_pairs={{0,32},{32,64},{64,96},{96,0},{1,33},{33,65},{65,97},{97,1},{2,34}... | collective-permute-start | bytes 1179656 | tf_op jit(solution)/shard_map/ppermute | solution.py:637
  108.7 23.1 %collective-permute-start.12 = (bf16[192,1024]{1,0:T(8,128)(2,1)S(1)}, bf16[192,1024]{1,0:T(8,128)(2,1)S(1)}, u32[]{:S(2)}, u32[]{:S(2)}) collective-permute-start(bf16[192,1024]{1,0:T(8,128)(2,1)S(1)} %early.1.g0), channel_id=1, source_target_pairs={{0,96},{32,0},{64,32},{96,64},{1,97},{33,1},{65,33},{97,65},{2,98}... | collective-permute-start | bytes 1179656 | tf_op jit(solution)/shard_map/ppermute | solution.py:637
  117.7 14.0 %collective-permute-start.4 = (bf16[192,1024]{1,0:T(8,128)(2,1)S(1)}, bf16[192,1024]{1,0:T(8,128)(2,1)S(1)}, u32[]{:S(2)}, u32[]{:S(2)}) collective-permute-start(bf16[192,1024]{1,0:T(8,128)(2,1)S(1)} %get-tuple-element.67.own_ref), channel_id=1, source_target_pairs={{0,1},{1,0},{2,3},{3,2},{4,5},{5,4},{6,7},{7,6},{8,9},{9,8},{10,11... | collective-permute-start | bytes 1179656 | tf_op jit(solution)/shard_map/ppermute | solution.py:633
  120.2 5.1 %collective-permute-start.9 = (bf16[192,256]{1,0:T(8,128)(2,1)S(1)}, bf16[192,256]{1,0:T(8,128)(2,1)S(1)}, u32[]{:S(2)}, u32[]{:S(2)}) collective-permute-start(bf16[192,256]{1,0:T(8,128)(2,1)S(1)} %get-tuple-element.70), channel_id=1, source_target_pairs={{0,96},{32,0},{64,32},{96,64},{1,97},{33,1},{65,33},{97,65},{2,98}... | collective-permute-start | bytes 294920 | tf_op jit(solution)/shard_map/ppermute | solution.py:637
  123.2 7.6 %collective-permute-start.5 = (bf16[192,256]{1,0:T(8,128)(2,1)S(1)}, bf16[192,256]{1,0:T(8,128)(2,1)S(1)}, u32[]{:S(2)}, u32[]{:S(2)}) collective-permute-start(bf16[192,256]{1,0:T(8,128)(2,1)S(1)} %get-tuple-element.68), channel_id=1, source_target_pairs={{0,32},{32,64},{64,96},{96,0},{1,33},{33,65},{65,97},{97,1},{2,34}... | collective-permute-start | bytes 294920 | tf_op jit(solution)/shard_map/ppermute | solution.py:637
  123.2 8.5 %collective-permute-start.7 = (bf16[192,256]{1,0:T(8,128)(2,1)S(1)}, bf16[192,256]{1,0:T(8,128)(2,1)S(1)}, u32[]{:S(2)}, u32[]{:S(2)}) collective-permute-start(bf16[192,256]{1,0:T(8,128)(2,1)S(1)} %get-tuple-element.69), channel_id=1, source_target_pairs={{0,64},{32,96},{64,0},{96,32},{1,65},{33,97},{65,1},{97,33},{2,66}... | collective-permute-start | bytes 294920 | tf_op jit(solution)/shard_map/ppermute | solution.py:637
  125.3 11.8 %collective-permute-start.10 = (bf16[192,256]{1,0:T(8,128)(2,1)S(1)}, bf16[192,256]{1,0:T(8,128)(2,1)S(1)}, u32[]{:S(2)}, u32[]{:S(2)}) collective-permute-start(bf16[192,256]{1,0:T(8,128)(2,1)S(1)} %collective-permute-done.9.b3), channel_id=1, source_target_pairs={{0,1},{1,0},{2,3},{3,2},{4,5},{5,4},{6,7},{7,6},{8,9},{9,8},{10,11... | collective-permute-start | bytes 294920 | tf_op jit(solution)/shard_map/ppermute | solution.py:633
  130.7 6.3 %collective-permute-start.6 = (bf16[192,256]{1,0:T(8,128)(2,1)S(1)}, bf16[192,256]{1,0:T(8,128)(2,1)S(1)}, u32[]{:S(2)}, u32[]{:S(2)}) collective-permute-start(bf16[192,256]{1,0:T(8,128)(2,1)S(1)} %collective-permute-done.5.b1), channel_id=1, source_target_pairs={{0,1},{1,0},{2,3},{3,2},{4,5},{5,4},{6,7},{7,6},{8,9},{9,8},{10,11... | collective-permute-start | bytes 294920 | tf_op jit(solution)/shard_map/ppermute | solution.py:633
  131.7 5.4 %collective-permute-start.8 = (bf16[192,256]{1,0:T(8,128)(2,1)S(1)}, bf16[192,256]{1,0:T(8,128)(2,1)S(1)}, u32[]{:S(2)}, u32[]{:S(2)}) collective-permute-start(bf16[192,256]{1,0:T(8,128)(2,1)S(1)} %collective-permute-done.7.b2), channel_id=1, source_target_pairs={{0,1},{1,0},{2,3},{3,2},{4,5},{5,4},{6,7},{7,6},{8,9},{9,8},{10,11... | collective-permute-start | bytes 294920 | tf_op jit(solution)/shard_map/ppermute | solution.py:633
  138.4 32.8 %copy-start.1 = (f32[192,1024]{1,0:T(8,128)S(1)}, f32[192,1024]{1,0:T(8,128)}, u32[]{:S(2)}) copy-start(f32[192,1024]{1,0:T(8,128)} %get-tuple-element.75.after_hbm.suffix_ref) | copy-start | bytes 2359300
  138.4 32.8 %copy-start.10 = (f32[192,1024]{1,0:T(8,128)S(1)}, f32[192,1024]{1,0:T(8,128)}, u32[]{:S(2)}) copy-start(f32[192,1024]{1,0:T(8,128)} %get-tuple-element.86.past_ref) | copy-start | bytes 2359300
  161.2 4.7 %collective-permute-start.13 = (f32[16,128]{1,0:T(8,128)S(1)}, f32[16,128]{1,0:T(8,128)S(1)}, u32[]{:S(2)}, u32[]{:S(2)}) collective-permute-start(f32[16,128]{1,0:T(8,128)S(1)} %get-tuple-element.84), channel_id=1, source_target_pairs={{32,0},{64,32},{96,64},{33,1},{65,33},{97,65},{34,2},{66,34},{98,6... | collective-permute-start | bytes 24584 | tf_op jit(solution)/shard_map/ppermute | solution.py:680
  162.5 5.9 %collective-permute-start.14 = (f32[16,128]{1,0:T(8,128)S(1)}, f32[16,128]{1,0:T(8,128)S(1)}, u32[]{:S(2)}, u32[]{:S(2)}) collective-permute-start(f32[16,128]{1,0:T(8,128)S(1)} %get-tuple-element.84), channel_id=1, source_target_pairs={{64,0},{96,32},{65,1},{97,33},{66,2},{98,34},{67,3},{99,35},{68,4}... | collective-permute-start | bytes 24584 | tf_op jit(solution)/shard_map/ppermute | solution.py:680
  163.8 7.4 %collective-permute-start.15 = (f32[16,128]{1,0:T(8,128)S(1)}, f32[16,128]{1,0:T(8,128)S(1)}, u32[]{:S(2)}, u32[]{:S(2)}) collective-permute-start(f32[16,128]{1,0:T(8,128)S(1)} %get-tuple-element.84), channel_id=1, source_target_pairs={{96,0},{97,1},{98,2},{99,3},{100,4},{101,5},{102,6},{103,7},{104,8... | collective-permute-start | bytes 24584 | tf_op jit(solution)/shard_map/ppermute | solution.py:680

commit v4 on v3

--- a/solution.py
+++ b/solution.py
@@ -19,6 +19,7 @@
 SLOTS = NSP * CHUNK
 ROWS = NSP * CAP
 FF = 512
+STRIP = 24
 GROUP = 8 * CHUNK
 
 _perm = np.zeros((GROUP, GROUP), np.float32)
@@ -274,10 +275,40 @@
     )(meta, perm_t, gg, gu, wg, wu)
 
 
+ROOT = 0.7978845608028654
+CUBE = 0.044715
+
+
+def gelu_parts(x):
+    t = jnp.tanh(ROOT * (x + CUBE * x * x * x))
+    return 0.5 * x * (1.0 + t), t
+
+
 def weight_kernel(
-    meta, perm_ref, own_ref, peer_ref, hid_ref, gg_ref, gu_ref, og_ref, ou_ref, od_ref, xs, cs
+    meta, perm_ref, own_ref, peer_ref, hid_ref, gg_ref, gu_ref, gate_ref, lru_ref, decay_ref,
+    og_ref, ou_ref, od_ref, value_ref, slope_ref, rate_ref, after_ref, xs, cs, carry_ref,
 ):
-    h = pl.program_id(1)
+    j, h = pl.program_id(0), pl.program_id(1)
+
+    @pl.when((j == 0) & (h == 0))
+    def _():
+        carry_ref[...] = jnp.ones((1, HALF), F32)
+
+    v = gate_ref[...].astype(F32)
+    value, t = gelu_parts(v)
+    value_ref[...] = value
+    grown = 0.5 * (1.0 + t) + 0.5 * v * (1.0 - t * t) * (ROOT * (1.0 + 3.0 * CUBE * v * v))
+    slope_ref[...] = grown * lru_ref[...].astype(F32)
+    rate_ref[...] = jnp.exp(decay_ref[...])
+    carry = carry_ref[...]
+    for tile in reversed(range(STRIP // 8)):
+        rows = slice(tile * 8, tile * 8 + 8)
+        decays, here = rate_ref[rows, :], [None] * 8
+        for r in reversed(range(8)):
+            here[r] = carry
+            carry = decays[r : r + 1] * carry
+        after_ref[rows, :] = jnp.concatenate(here, axis=0)
+    carry_ref[...] = carry
     perm = perm_ref[...]
     for g in range(8):
         rows = slice(g * GROUP, (g + 1) * GROUP)
@@ -291,7 +322,8 @@
     od_ref[...] = dot_rows(hid_ref[...], cs[...])
 
 
-def weight_grads(meta, perm, own, peer, hid, gg, gu):
+def weight_grads(meta, perm, own, peer, hid, gg, gu, gate_pre, lru_out, log_decay):
+    strip = pl.BlockSpec((STRIP, HALF), lambda j, h, m: (7 - 2 * j - h, 0))
     block = lambda j, h, m: 2 * j + (h + m[0]) % 2
     return pl.pallas_call(
         weight_kernel,
@@ -306,24 +338,27 @@
                 pl.BlockSpec((ROWS, FF), lambda j, h, m: (0, 0)),
                 pl.BlockSpec((ROWS, FF), lambda j, h, m: (0, 0)),
                 pl.BlockSpec((ROWS, FF), lambda j, h, m: (0, 0)),
-            ],
+            ]
+            + [strip] * 3,
             out_specs=[
                 pl.BlockSpec((BLK, FF), lambda j, h, m: (block(j, h, m), 0)),
                 pl.BlockSpec((BLK, FF), lambda j, h, m: (block(j, h, m), 0)),
                 pl.BlockSpec((FF, BLK), lambda j, h, m: (0, block(j, h, m))),
-            ],
-            scratch_shapes=[pltpu.VMEM((ROWS, BLK), BF)] * 2,
+            ]
+            + [strip] * 4,
+            scratch_shapes=[pltpu.VMEM((ROWS, BLK), BF)] * 2 + [pltpu.VMEM((1, HALF), F32)],
         ),
         out_shape=[
             jax.ShapeDtypeStruct((D, FF), F32),
             jax.ShapeDtypeStruct((D, FF), F32),
             jax.ShapeDtypeStruct((FF, D), F32),
-        ],
+        ]
+        + [pltpu.HBM((TOK, HALF), F32)] * 4,
         compiler_params=vm(18),
         cost_estimate=pl.CostEstimate(
             flops=3 * 2 * ROWS * D * FF, bytes_accessed=20_000_000, transcendentals=0
         ),
-    )(meta, *in_hbm(perm, own, peer, hid, gg, gu))
+    )(meta, *in_hbm(perm, own, peer, hid, gg, gu, gate_pre, lru_out, log_decay))
 
 
 def combine_kernel(
@@ -334,8 +369,7 @@
     copies = fetch(
         [(ids_hbm, ids)]
         + [(d_hbm.at[:, lanes(2 * j + tp)], own.at[:, j * BLK : (j + 1) * BLK]) for j in range(4)]
-        + [(w_hbm.at[:, lanes(2 * j + tp)], w_ref.at[j, :, :]) for j in range(4)]
-        + [(w_hbm.at[:, lanes(2 * j + 1 - tp)], w_ref.at[4 + j, :, :]) for j in range(4)],
+        + [(w_hbm.at[:, lanes(2 * j + tp)], w_ref.at[j, :, :]) for j in range(4)],
         sems,
     )
     copies[0].wait()
@@ -367,24 +401,15 @@
         out_specs=[pl.BlockSpec(memory_space=pltpu.VMEM)] * 6,
         out_shape=[jax.ShapeDtypeStruct((TOK, HALF), BF)]
         + [jax.ShapeDtypeStruct((TOK, BLK), BF)] * 4
-        + [jax.ShapeDtypeStruct((8, HALF, BLK), BF)],
+        + [jax.ShapeDtypeStruct((4, HALF, BLK), BF)],
         scratch_shapes=[
             pltpu.VMEM((2, TOK), jnp.int32),
             pltpu.VMEM((TOK, HALF), BF),
-            pltpu.SemaphoreType.DMA((13,)),
+            pltpu.SemaphoreType.DMA((9,)),
         ],
         compiler_params=vm(12),
         cost_estimate=cost(1e9),
     )(meta, *in_hbm(ids), ret, *in_hbm(d_out, w_out))
-
-
-ROOT = 0.7978845608028654
-CUBE = 0.044715
-
-
-def gelu_parts(x):
-    t = jnp.tanh(ROOT * (x + CUBE * x * x * x))
-    return 0.5 * x * (1.0 + t), t
 
 
 def tile_of(line):
@@ -425,94 +450,49 @@
     return carry
 
 
-def prep_kernel(
-    gate_hbm, lru_hbm, decay_hbm, before_ref, value_hbm, slope_hbm, rate_hbm, after_hbm, past_hbm,
-    gate, lru, decay, value, slope, rate, after, past, sems,
+def drive_kernel(
+    meta, own_ref, peer_ref, w_ref, w_hbm, value_hbm, slope_hbm, rate_hbm, after_hbm, g0, g1, g2, g3,
+    dgate_ref, local_ref, head_ref, moved_ref, w, value, slope, rate, after, sems,
 ):
-    for copy in fetch([(gate_hbm, gate), (lru_hbm, lru), (decay_hbm, decay)], sems):
-        copy.wait()
-    x = gate[...].astype(F32)
-    state = lru[...].astype(F32)
-    gelu, t = gelu_parts(x)
-    value[...] = gelu
-    out0 = fetch([(value, value_hbm)], sems.at[3:4])
-    grown = 0.5 * (1.0 + t) + 0.5 * x * (1.0 - t * t) * (ROOT * (1.0 + 3.0 * CUBE * x * x))
-    slope[...] = grown * state
-    out1 = fetch([(slope, slope_hbm)], sems.at[4:5])
-    rate[...] = jnp.exp(decay[...])
-    first = lax.broadcasted_iota(jnp.int32, (TOK, HALF), 0) == 0
-    prev = jnp.where(first, before_ref[...].astype(F32), pltpu.roll(state, 1, 0))
-    past[...] = rate[...] * prev
-    out2 = fetch([(rate, rate_hbm), (past, past_hbm)], sems.at[5:7])
-    carry = jnp.ones((1, HALF), F32)
-    for tile in reversed(range(TOK // 8)):
-        rows = slice(tile * 8, tile * 8 + 8)
-        decays, here = rate[rows, :], [None] * 8
-        for r in reversed(range(8)):
-            here[r] = carry
-            carry = decays[r : r + 1] * carry
-        after[rows, :] = jnp.concatenate(here, axis=0)
-    for copy in out0 + out1 + out2 + fetch([(after, after_hbm)], sems.at[7:8]):
-        copy.wait()
-
-
-def prep(gate_pre, lru_out, log_decay, before):
-    bf, wide = pltpu.VMEM((TOK, HALF), BF), pltpu.VMEM((TOK, HALF), F32)
-    return pl.pallas_call(
-        prep_kernel,
-        name="prep",
-        in_specs=mixed("hhhv")[1:],
-        out_specs=[pl.BlockSpec(memory_space=pltpu.HBM)] * 5,
-        out_shape=[pltpu.HBM((TOK, HALF), F32)] * 5,
-        scratch_shapes=[bf, bf] + [wide] * 6 + [pltpu.SemaphoreType.DMA((8,))],
-        compiler_params=vm(12),
-        cost_estimate=cost(1e9),
-    )(*in_hbm(gate_pre, lru_out, log_decay), before)
-
-
-def drive_kernel(
-    meta, own_ref, peer_ref, w_ref, value_hbm, slope_hbm, rate_hbm, after_hbm, g0, g1, g2, g3,
-    dgate_ref, local_ref, head_ref, moved_ref, value, slope, rate, after, sems,
-):
+    tp = meta[0]
     copies = fetch(
-        [
+        [(w_hbm.at[:, lanes(2 * j + 1 - tp)], w.at[j, :, :]) for j in range(4)]
+        + [
             (value_hbm, value),
-            (slope_hbm, slope),
             (rate_hbm, rate),
             (after_hbm.at[0:8, :], after),
-            (g0, moved_ref.at[0, :, :]),
-            (g1, moved_ref.at[1, :, :]),
-            (g2, moved_ref.at[2, :, :]),
-            (g3, moved_ref.at[3, :, :]),
+            (slope_hbm, slope),
         ],
         sems,
     )
     grad = 0.0
-    for k in range(8):
-        ref, j = (own_ref, peer_ref)[k // 4], k % 4
-        grad += dot_cols(ref[:, j * BLK : (j + 1) * BLK], w_ref[k, :, :])
-    copies[0].wait()
+    for j in range(4):
+        grad += dot_cols(own_ref[:, j * BLK : (j + 1) * BLK], w_ref[j, :, :])
+    for j in range(4):
+        copies[j].wait()
+        grad += dot_cols(peer_ref[:, j * BLK : (j + 1) * BLK], w[j, :, :])
+    copies[4].wait()
     local_ref[...] = grad * value[...]
-    copies[1].wait()
+    for copy in copies[5:]:
+        copy.wait()
+    late = fetch([(g, moved_ref.at[k, :, :]) for k, g in enumerate((g0, g1, g2, g3))], sems.at[8:12])
     dgate_ref[...] = (grad * slope[...]).astype(BF)
-    copies[2].wait()
-    copies[3].wait()
 
     def visit(rows, here, later):
         local_ref[rows, :] = here
 
     head_ref[0:8, :] = tile_of(scan_rows(local_ref, rate, jnp.zeros((1, HALF), F32), visit))
     head_ref[8:16, :] = tile_of(after[0:1, :] * rate[0:1, :])
-    for copy in copies[4:]:
+    for copy in late:
         copy.wait()
 
 
-def drive(meta, own, peer, w, value, slope, rate, after, gated):
+def drive(meta, own, peer, w, w_out, value, slope, rate, after, gated):
     wide = pltpu.VMEM((TOK, HALF), F32)
     return pl.pallas_call(
         drive_kernel,
         name="drive",
-        in_specs=mixed("vvvhhhhaaaa"),
+        in_specs=mixed("vvvhhhhhaaaa"),
         out_specs=[pl.BlockSpec(memory_space=pltpu.VMEM)] * 4,
         out_shape=[
             jax.ShapeDtypeStruct((TOK, HALF), BF),
@@ -520,10 +500,11 @@
             jax.ShapeDtypeStruct((16, 128), F32),
             jax.ShapeDtypeStruct((4, TOK, HALF), BF),
         ],
-        scratch_shapes=[wide, wide, wide, pltpu.VMEM((8, HALF), F32), pltpu.SemaphoreType.DMA((8,))],
+        scratch_shapes=[pltpu.VMEM((4, HALF, BLK), BF), wide, wide, wide]
+        + [pltpu.VMEM((8, HALF), F32), pltpu.SemaphoreType.DMA((12,))],
         compiler_params=vm(12),
         cost_estimate=cost(2e9),
-    )(meta, own, peer, w, *in_hbm(value, slope, rate, after), *gated)
+    )(meta, own, peer, w, *in_hbm(w_out, value, slope, rate, after), *gated)
 
 
 def link_kernel(meta, shares_ref, within_ref, after_ref, plane_ref):
@@ -561,26 +542,29 @@
     )(meta, shares)
 
 
-def finish_kernel(within_ref, after_ref, p1, p2, p3, local_ref, suffix_ref, past_ref, dd_ref, dl_ref):
+def finish_kernel(
+    within_ref, after_ref, p1, p2, p3, local_ref, suffix_ref, rate_ref, lru_ref, before_ref,
+    dd_ref, dl_ref,
+):
     planes = p3[0:8, :]
     planes = p2[0:8, :] + p2[8:16, :] * planes
     planes = p1[0:8, :] + p1[8:16, :] * planes
     incoming = line_of(within_ref[...] + after_ref[...] * planes)
-    for tile in range(TOK // 8):
-        rows = slice(tile * 8, tile * 8 + 8)
-        value = local_ref[rows, :] + suffix_ref[rows, :] * incoming
-        dd_ref[rows, :] = value
-        dl_ref[rows, :] = value * past_ref[rows, :]
-
-
-def finish(within, after, planes, local, suffix, past):
+    value = local_ref[...] + suffix_ref[...] * incoming
+    dd_ref[...] = value
+    first = lax.broadcasted_iota(jnp.int32, (TOK, HALF), 0) == 0
+    state = pltpu.roll(lru_ref[...].astype(F32), 1, 0)
+    dl_ref[...] = value * rate_ref[...] * jnp.where(first, before_ref[...].astype(F32), state)
+
+
+def finish(within, after, planes, local, suffix, rate, lru_out, before):
     return pl.pallas_call(
         finish_kernel,
         name="finish",
         out_shape=[jax.ShapeDtypeStruct((TOK, HALF), F32)] * 2,
         compiler_params=vm(8),
         cost_estimate=cost(1e9),
-    )(within, after, *planes, local, suffix, past)
+    )(within, after, *planes, local, suffix, rate, lru_out, before)
 
 
 def outer_own_kernel(b0, b1, b2, b3, moved, out_ref):
@@ -664,21 +648,25 @@
     back, moving, last = lax.optimization_barrier((back, gated, lru_out[-1:]))
     turn1, turn3 = turned(moving, 1), turned(moving, 3)
     before = lax.ppermute(last, SP, [(s, s + 1) for s in range(NSP - 1)])
-    value, slope, rate, suffix, past = prep(gate_pre, lru_out, log_decay, before)
-    grads = weight_grads(meta, perm, got, got_peer, hid, gg, gu)
-    ret, rate, grad_gate, grad_up, grad_down = lax.optimization_barrier((ret, rate, *grads))
+    grads = weight_grads(
+        meta, perm, got, got_peer, hid, gg, gu, gate_pre, lru_out, log_decay
+    )
+    ret, *grads = lax.optimization_barrier((ret, *grads))
+    grad_gate, grad_up, grad_down, value, slope, rate, suffix = grads
     dm, *blocks, w = combine(meta, ids, ret.reshape(SLOTS, HALF // 2), d_out, w_out)
     dm_peer = swapped(dm)
     own = (blocks[0], *(turned(blocks[k], k) for k in (1, 2, 3)))
     d_gate, local, head, moved = drive(
-        meta, dm, dm_peer, w, value, slope, rate, suffix, (gated, turn1, turn2, turn3)
+        meta, dm, dm_peer, w, w_out, value, slope, rate, suffix, (gated, turn1, turn2, turn3)
     )
     peer = (dm_peer, *(swapped(own[k]) for k in (1, 2, 3)))
     share = outer(meta, peer, moved, outer_own(own, moved), head)
     shares = lax.all_to_all(share.reshape(16, 32, HALF + 128), ("y", "x"), 0, 0, tiled=True)
     within, after, plane = link(meta, shares)
     planes = [lax.ppermute(plane, "z", [(s, s - k) for s in range(k, 4)]) for k in (1, 2, 3)]
-    d_drive, d_log_decay = finish(within, after, planes, local, suffix, past)
+    d_drive, d_log_decay = finish(
+        within, after, planes, local, suffix, rate, lru_out, before
+    )
     grad_out_proj = jnp.sum(shares[:, :, :HALF].astype(F32), axis=0)
     return (
         grad_gate[None], grad_up[None], grad_down[None], grad_out_proj, d_gate, d_drive, d_log_decay,

time: 175 us -> 174 us (level)
  blocking collectives: 74.4 us -> 52.2 us
  waiting for transfers between devices: 19 us -> 39.7 us
  starting transfers between devices: 26.2 us -> 28.5 us
    all_to_all x1 -> x0, blocking collectives: 22.2 us -> none  [on_device(): lax.all_to_all(share.reshape(16, 32, HALF + 128), ('y', 'x'), 0, 0, tiled...]
    all_to_all x0 -> x1, waiting for transfers between devices: none -> 17.2 us  [on_device(): lax.all_to_all(share.reshape(16, 32, HALF + 128), ('y', 'x'), 0, 0, tiled...]
    all_to_all x1, waiting for transfers between devices: 0.01 us -> 3.87 us  [on_device(): lax.all_to_all(back.reshape(NSP, CHUNK, HALF // 2), SP, 0, 0, tiled=True)]
    all_to_all x0 -> x1, starting transfers between devices: none -> 3.84 us  [on_device(): lax.all_to_all(share.reshape(16, 32, HALF + 128), ('y', 'x'), 0, 0, tiled...]
    pallas_call x2 -> x1, Pallas kernels: 8.99 us -> 5.88 us  [drive(): pl.pallas_call(drive_kernel, name='drive', in_specs=mixed('vvvhhhhhaaaa')...]
  transfers between devices with their start and end apart: 17 -> 18, of which waited for: 6 -> 7; matrix products, arithmetic and copies ran while one was open for 0% -> 0% of each run, Pallas kernels for 21% -> 20%
where the time goes in v4:
time: 174 us; the launch traced here: 172 us
  blocking collectives  52.2 us (30%)
  Pallas kernels  49.9 us (29%)
  waiting for transfers between devices  39.7 us (23%)
  starting transfers between devices  28.5 us (16%)
    all_to_all x1, blocking collectives, on_device(): got = lax.all_to_all(sent.reshape(NSP, CHUNK, HALF), SP, 0, 0, tiled=True)  52.2 us
    all_to_all x1, waiting for transfers between devices, on_device(): lax.all_to_all(share.reshape(16, 32, HALF + 128), ('y', 'x'), 0, 0, tiled...  17.2 us
    pallas_call x1, Pallas kernels, weight_grads(): pl.pallas_call(weight_kernel, name='weight_grads', grid_spec=pltpu.Prefet...  15.9 us
    ppermute x6, waiting for transfers between devices, turned(): return lax.ppermute(value, 'z', [(s, (s + steps) % 4) for s in range(4)])  12.5 us
    pallas_call x1, Pallas kernels, expert_peer(): pl.pallas_call(peer_kernel, name='expert_peer', in_specs=whole(9), out_sp...  7.02 us
    ppermute x6, starting transfers between devices, swapped(): return lax.ppermute(value, 'tp', [(0, 1), (1, 0)])  6.8 us
    ppermute x6, starting transfers between devices, turned(): return lax.ppermute(value, 'z', [(s, (s + steps) % 4) for s in range(4)])  6.08 us
    pallas_call x1, Pallas kernels, drive(): pl.pallas_call(drive_kernel, name='drive', in_specs=mixed('vvvhhhhhaaaa')...  5.88 us
  transfers between devices with their start and end apart: 18, of which 7 were waited for; matrix products, arithmetic and copies ran while one was open for 0% of the time, Pallas kernels for 20%

profile of v4, /device:TPU:1, one launch (start us, length us, event | category | flops | bytes accessed | tf_op | source)
XLA Modules:
  0.0 172.3 jit_solution(14341079173340362033)
XLA Ops:
  0.6 0.1 pad_add_fusion.meta
  0.7 5.1 %pack.1 = bf16[1536,1024]{1,0:T(8,128)(2,1)S(1)} custom-call(s32[4]{0:T(128)S(1)} %pad_add_fusion.meta, s32[2,192]{1,0:T(2,128)} %bitcast.30, f32[2,192]{1,0:T(2,128)} %bitcast.32, bf16[192,2048]{1,0:T(8,128)(2,1)} %x_hbm.1, bf16[192,2048]{1,0:T(8,128)(2,1)} %d_hbm.3), custom_call_target="tpu_custom_call" | custom-call | tf_op jit(solution)/shard_map/pack/pallas_call | solution.py:139
  5.9 0.0 copy-start.3
  5.9 0.0 copy-start.5
  5.9 0.0 copy-start.7
  5.9 0.0 copy-start.8
  5.9 0.0 copy-start.9
  5.9 0.0 copy-start.12
  5.9 52.2 %all_to_all.15 = bf16[64,24,1024]{2,1,0:T(8,128)(2,1)S(1)} all-to-all(bf16[64,24,1024]{2,1,0:T(8,128)(2,1)S(1)} %bitcast.17), channel_id=1, replica_groups=mesh['z'=4,'y'=4,'x'=4,'tp'=2] {'z','y','x'}, dimensions={0} | all-to-all | bytes 6291456 | tf_op jit(solution)/shard_map/all_to_all | solution.py:635
  58.2 2.1 %collective-permute-start = (bf16[1536,1024]{1,0:T(8,128)(2,1)S(1)}, bf16[1536,1024]{1,0:T(8,128)(2,1)S(1)}, u32[]{:S(2)}, u32[]{:S(2)}) collective-permute-start(bf16[1536,1024]{1,0:T(8,128)(2,1)S(1)} %bitcast.19), channel_id=1, source_target_pairs={{0,1},{1,0},{2,3},{3,2},{4,5},{5,4},{6,7},{7,6},{8,9},{9,8},{10,11... | collective-permute-start | bytes 9437192 | tf_op jit(solution)/shard_map/ppermute | solution.py:617
  60.3 0.3 early.1.g0
  60.6 0.0 copy-start.13
  60.7 4.0 %expert_own.1 = (f32[768,512]{1,0:T(8,128)S(1)}, f32[768,512]{1,0:T(8,128)S(1)}, f32[768,512]{1,0:T(8,128)S(1)}) custom-call(s32[4]{0:T(128)S(1)} %pad_add_fusion.meta, bf16[192,192]{1,0:T(8,128)(2,1)S(1)} %copy-done.12, bf16[1536,1024]{1,0:T(8,128)(2,1)S(1)} %bitcast.20, bf16[2048,512]{1,0:T(8,128)(2,1)S(1)} %bitcast.24, bf16[2048,512]{1,0:T(8,128)(2,1)S(1)} %bitcast.27, ...), custom_call_target="tpu_custom_call" | custom-call | flops 4000000000 | tf_op jit(solution)/shard_map/expert_own/pallas_call | solution.py:217
  64.7 0.9 collective-permute-done.peer_ref
  65.6 7.0 %expert_peer.1 = (bf16[768,512]{1,0:T(8,128)(2,1)S(1)}, bf16[768,512]{1,0:T(8,128)(2,1)S(1)}, bf16[768,512]{1,0:T(8,128)(2,1)S(1)}, bf16[1536,512]{1,0:T(8,128)(2,1)S(1)}) custom-call(s32[4]{0:T(128)S(1)} %pad_add_fusion.meta, bf16[192,192]{1,0:T(8,128)(2,1)S(1)} %copy-done.12, bf16[192,192]{1,0:T(8,128)(2,1)S(1)} %copy-done.13, ...), custom_call_target="tpu_custom_call" | custom-call | flops 6000000000 | tf_op jit(solution)/shard_map/expert_peer/pallas_call | solution.py:248
  72.6 0.0 copy-start.14
  72.6 0.4 collective-permute-start.1
  73.1 0.4 collective-permute-start.2
  73.4 2.8 %expert_back.1.a_ref = bf16[1536,512]{1,0:T(8,128)(2,1)S(1)} custom-call(s32[4]{0:T(128)S(1)} %pad_add_fusion.meta, bf16[192,192]{1,0:T(8,128)(2,1)S(1)} %copy-done.13, bf16[768,512]{1,0:T(8,128)(2,1)S(1)} %get-tuple-element.54.gg_ref, bf16[768,512]{1,0:T(8,128)(2,1)S(1)} %get-tuple-element.55.gu_ref, bf16[2048,512]{1,0:T(8,128)(2,1)S(1)} %bitcast.26, ...), custom_call_target="tpu_custom_call" | custom-call | flops 3000000000 | tf_op jit(solution)/shard_map/expert_back/pallas_call | solution.py:266
  76.3 1.3 part_sum.1
  77.6 7.5 %collective-permute-done.2.g2 = bf16[192,1024]{1,0:T(8,128)(2,1)S(1)} collective-permute-done((bf16[192,1024]{1,0:T(8,128)(2,1)S(1)}, bf16[192,1024]{1,0:T(8,128)(2,1)S(1)}, u32[]{:S(2)}, u32[]{:S(2)}) %collective-permute-start.2) | collective-permute-done | bytes 393248 | tf_op jit(solution)/shard_map/ppermute | solution.py:621
  85.1 4.8 %all-to-all-start.1 = ((bf16[64,24,512]{2,1,0:T(8,128)(2,1)}), bf16[64,24,512]{2,1,0:T(8,128)(2,1)S(1)}, u32[]{:S(2)}, u32[]{:S(2)}) async-start(bf16[64,24,512]{2,1,0:T(8,128)(2,1)} %bitcast.11), calls=%async_computation.1 | async-start | bytes 3145728 | tf_op jit(solution)/shard_map/all_to_all | solution.py:647
  89.9 1.3 collective-permute-start.10
  91.2 15.9 %weight_grads.1 = (f32[2048,512]{1,0:T(8,128)}, f32[2048,512]{1,0:T(8,128)}, f32[512,2048]{1,0:T(8,128)}, f32[192,1024]{1,0:T(8,128)}, f32[192,1024]{1,0:T(8,128...) custom-call(s32[4]{0:T(128)S(1)} %pad_add_fusion.meta, bf16[192,192]{1,0:T(8,128)(2,1)} %constant.25.clone.perm_ref, ...), custom_call_target="tpu_custom_call" | custom-call | flops 4831838208 | bytes 20000000 | tf_op jit(solution)/shard_map/weight_grads/pallas_call | solution.py:328
  107.1 1.7 %collective-permute-start.11 = (bf16[192,1024]{1,0:T(8,128)(2,1)S(1)}, bf16[192,1024]{1,0:T(8,128)(2,1)S(1)}, u32[]{:S(2)}, u32[]{:S(2)}) collective-permute-start(bf16[192,1024]{1,0:T(8,128)(2,1)S(1)} %early.1.g0), channel_id=1, source_target_pairs={{0,96},{32,0},{64,32},{96,64},{1,97},{33,1},{65,33},{97,65},{2,98}... | collective-permute-start | bytes 1179656 | tf_op jit(solution)/shard_map/ppermute | solution.py:621
  108.8 3.9 %all-to-all-done.1 = bf16[64,24,512]{2,1,0:T(8,128)(2,1)S(1)} async-done(((bf16[64,24,512]{2,1,0:T(8,128)(2,1)}), bf16[64,24,512]{2,1,0:T(8,128)(2,1)S(1)}, u32[]{:S(2)}, u32[]{:S(2)}) %all-to-all-start.1) | async-done | bytes 1572896 | tf_op jit(solution)/shard_map/all_to_all | solution.py:647
  112.7 2.7 %combine.1 = (bf16[192,1024]{1,0:T(8,128)(2,1)S(1)}, bf16[192,256]{1,0:T(8,128)(2,1)S(1)}, bf16[192,256]{1,0:T(8,128)(2,1)S(1)}, bf16[192,256]{1,0:T(8,128)(2,1)...) custom-call(s32[4]{0:T(128)S(1)} %pad_add_fusion.meta, s32[2,192]{1,0:T(2,128)} %bitcast.31, ...), custom_call_target="tpu_custom_call" | custom-call | flops 1000000000 | tf_op jit(solution)/shard_map/combine/pallas_call | solution.py:397
  115.4 2.7 %collective-permute-start.3 = (bf16[192,1024]{1,0:T(8,128)(2,1)S(1)}, bf16[192,1024]{1,0:T(8,128)(2,1)S(1)}, u32[]{:S(2)}, u32[]{:S(2)}) collective-permute-start(bf16[192,1024]{1,0:T(8,128)(2,1)S(1)} %get-tuple-element.71.own_ref), channel_id=1, source_target_pairs={{0,1},{1,0},{2,3},{3,2},{4,5},{5,4},{6,7},{7,6},{8,9},{9,8},{10,11... | collective-permute-start | bytes 1179656 | tf_op jit(solution)/shard_map/ppermute | solution.py:617
  118.1 0.1 collective-permute-start.4
  118.2 1.6 collective-permute-start.6
  119.8 1.0 collective-permute-start.8
  120.8 4.9 %collective-permute-done.4.b1 = bf16[192,256]{1,0:T(8,128)(2,1)S(1)} collective-permute-done((bf16[192,256]{1,0:T(8,128)(2,1)S(1)}, bf16[192,256]{1,0:T(8,128)(2,1)S(1)}, u32[]{:S(2)}, u32[]{:S(2)}) %collective-permute-start.4) | collective-permute-done | bytes 98336 | tf_op jit(solution)/shard_map/ppermute | solution.py:621
  125.7 0.9 collective-permute-start.5
  126.6 0.6 collective-permute-start.9
  127.2 5.9 %drive.1 = (bf16[192,1024]{1,0:T(8,128)(2,1)}, f32[192,1024]{1,0:T(8,128)S(1)}, f32[16,128]{1,0:T(8,128)S(1)}, bf16[4,192,1024]{2,1,0:T(8,128)(2,1)S(1)}) custom-call(s32[4]{0:T(128)S(1)} %pad_add_fusion.meta, bf16[192,1024]{1,0:T(8,128)(2,1)S(1)} %get-tuple-element.71.own_ref, bf16[192,1024]{1,0:T(8,128)(2,1)S(1)} %collective-permute-done.3.peer_ref.p0, ...), custom_call_target="tpu_custom_call" | custom-call | flops 2000000000 | tf_op jit(solution)/shard_map/drive/pallas_call | solution.py:492
  133.1 0.7 outer_own.1.own_ref
  133.9 2.3 %outer.1 = bf16[512,1152]{1,0:T(8,128)(2,1)} custom-call(s32[4]{0:T(128)S(1)} %pad_add_fusion.meta, bf16[192,1024]{1,0:T(8,128)(2,1)S(1)} %collective-permute-done.3.peer_ref.p0, bf16[192,256]{1,0:T(8,128)(2,1)S(1)} %collective-permute-done.5.p1, bf16[192,256]{1,0:T(8,128)(2,1)S(1)} %collective-permute-done.7.p2, ...), custom_call_target="tpu_custom_call" | custom-call | flops 1000000000 | tf_op jit(solution)/shard_map/outer/pallas_call | solution.py:605
  136.2 3.8 %all-to-all-start.2 = ((bf16[16,32,1152]{2,1,0:T(8,128)(2,1)}), bf16[16,32,1152]{2,1,0:T(8,128)(2,1)S(1)}, u32[]{:S(2)}, u32[]{:S(2)}) async-start(bf16[16,32,1152]{2,1,0:T(8,128)(2,1)} %bitcast.16), calls=%async_computation.2 | async-start | bytes 2359296 | tf_op jit(solution)/shard_map/all_to_all | solution.py:664
  140.1 3.1 %collective-permute-start.15 = (bf16[1,1024]{1,0:T(2,128)(2,1)S(1)}, bf16[1,1024]{1,0:T(2,128)(2,1)S(1)}, u32[]{:S(2)}, u32[]{:S(2)}) collective-permute-start(bf16[1,1024]{1,0:T(2,128)(2,1)S(1)} %slice.6), channel_id=1, source_target_pairs={{0,2},{2,4},{4,6},{6,8},{8,10},{10,12},{12,14},{14,16},{16,18},{18... | collective-permute-start | bytes 6152 | tf_op jit(solution)/shard_map/ppermute | solution.py:650
  143.2 17.2 %all-to-all-done.2.shares_ref = bf16[16,32,1152]{2,1,0:T(8,128)(2,1)S(1)} async-done(((bf16[16,32,1152]{2,1,0:T(8,128)(2,1)}), bf16[16,32,1152]{2,1,0:T(8,128)(2,1)S(1)}, u32[]{:S(2)}, u32[]{:S(2)}) %all-to-all-start.2) | async-done | bytes 1179680 | tf_op jit(solution)/shard_map/all_to_all | solution.py:664
  160.4 0.6 link.1
  161.0 1.3 collective-permute-start.12
  162.3 1.3 collective-permute-start.13
  163.6 1.3 collective-permute-start.14
  164.9 0.8 convert_reduce_fusion
  165.7 2.5 %collective-permute-done.13.p2 = f32[16,128]{1,0:T(8,128)S(1)} collective-permute-done((f32[16,128]{1,0:T(8,128)S(1)}, f32[16,128]{1,0:T(8,128)S(1)}, u32[]{:S(2)}, u32[]{:S(2)}) %collective-permute-start.13) | collective-permute-done | bytes 8224 | tf_op jit(solution)/shard_map/ppermute | solution.py:666
  168.2 2.8 %collective-permute-done.14.p3 = f32[16,128]{1,0:T(8,128)S(1)} collective-permute-done((f32[16,128]{1,0:T(8,128)S(1)}, f32[16,128]{1,0:T(8,128)S(1)}, u32[]{:S(2)}, u32[]{:S(2)}) %collective-permute-start.14) | collective-permute-done | bytes 8224 | tf_op jit(solution)/shard_map/ppermute | solution.py:666
  171.0 1.3 finish.1
  (39 shorter events, 0.1 us)
Async XLA Ops:
  5.9 54.4 %copy-start.3 = (bf16[192,1024]{1,0:T(8,128)(2,1)S(1)}, bf16[192,1024]{1,0:T(8,128)(2,1)}, u32[]{:S(2)}) copy-start(bf16[192,1024]{1,0:T(8,128)(2,1)} %lru_ref.5) | copy-start | bytes 1179652
  5.9 54.4 %copy-start.5 = (bf16[192,1024]{1,0:T(8,128)(2,1)S(1)}, bf16[192,1024]{1,0:T(8,128)(2,1)}, u32[]{:S(2)}) copy-start(bf16[192,1024]{1,0:T(8,128)(2,1)} %gate_ref.3) | copy-start | bytes 1179652
  5.9 54.7 %copy-start.7 = (bf16[1,512,2048]{2,1,0:T(8,128)(2,1)S(1)}, bf16[1,512,2048]{2,1,0:T(8,128)(2,1)}, u32[]{:S(2)}) copy-start(bf16[1,512,2048]{2,1,0:T(8,128)(2,1)} %param.23) | copy-start | bytes 6291460
  5.9 54.7 %copy-start.8 = (bf16[1,2048,512]{2,1,0:T(8,128)(2,1)S(1)}, bf16[1,2048,512]{2,1,0:T(8,128)(2,1)}, u32[]{:S(2)}) copy-start(bf16[1,2048,512]{2,1,0:T(8,128)(2,1)} %param.21) | copy-start | bytes 6291460
  5.9 54.7 %copy-start.9 = (bf16[1,2048,512]{2,1,0:T(8,128)(2,1)S(1)}, bf16[1,2048,512]{2,1,0:T(8,128)(2,1)}, u32[]{:S(2)}) copy-start(bf16[1,2048,512]{2,1,0:T(8,128)(2,1)} %param.22) | copy-start | bytes 6291460
  5.9 54.7 %copy-start.12 = (bf16[192,192]{1,0:T(8,128)(2,1)S(1)}, bf16[192,192]{1,0:T(8,128)(2,1)}, u32[]{:S(2)}) copy-start(bf16[192,192]{1,0:T(8,128)(2,1)} %constant.25.clone.perm_ref) | copy-start | bytes 221188
  58.1 6.5 %copy-start = (bf16[64,24,1024]{2,1,0:T(8,128)(2,1)}, bf16[64,24,1024]{2,1,0:T(8,128)(2,1)S(1)}, u32[]{:S(2)}) copy-start(bf16[64,24,1024]{2,1,0:T(8,128)(2,1)S(1)} %all_to_all.15) | copy-start | bytes 9437188
  58.2 7.4 %collective-permute-start = (bf16[1536,1024]{1,0:T(8,128)(2,1)S(1)}, bf16[1536,1024]{1,0:T(8,128)(2,1)S(1)}, u32[]{:S(2)}, u32[]{:S(2)}) collective-permute-start(bf16[1536,1024]{1,0:T(8,128)(2,1)S(1)} %bitcast.19), channel_id=1, source_target_pairs={{0,1},{1,0},{2,3},{3,2},{4,5},{5,4},{6,7},{7,6},{8,9},{9,8},{10,11... | collective-permute-start | bytes 9437192 | tf_op jit(solution)/shard_map/ppermute | solution.py:617
  60.6 4.9 %copy-start.13 = (bf16[192,192]{1,0:T(8,128)(2,1)S(1)}, bf16[192,192]{1,0:T(8,128)(2,1)}, u32[]{:S(2)}) copy-start(bf16[192,192]{1,0:T(8,128)(2,1)} %constant.26.clone.perm_t_ref) | copy-start | bytes 221188
  65.6 7.0 %copy-start.6 = (bf16[1536,1024]{1,0:T(8,128)(2,1)}, bf16[1536,1024]{1,0:T(8,128)(2,1)S(1)}, u32[]{:S(2)}) copy-start(bf16[1536,1024]{1,0:T(8,128)(2,1)S(1)} %collective-permute-done.peer_ref) | copy-start | bytes 9437188
  72.6 3.6 %copy-start.14 = (bf16[768,512]{1,0:T(8,128)(2,1)}, bf16[768,512]{1,0:T(8,128)(2,1)S(1)}, u32[]{:S(2)}) copy-start(bf16[768,512]{1,0:T(8,128)(2,1)S(1)} %get-tuple-element.54.gg_ref) | copy-start | bytes 2359300
  72.6 3.6 %copy-start.15 = (bf16[768,512]{1,0:T(8,128)(2,1)}, bf16[768,512]{1,0:T(8,128)(2,1)S(1)}, u32[]{:S(2)}) copy-start(bf16[768,512]{1,0:T(8,128)(2,1)S(1)} %get-tuple-element.55.gu_ref) | copy-start | bytes 2359300
  72.6 3.6 %copy-start.16 = (bf16[768,512]{1,0:T(8,128)(2,1)}, bf16[768,512]{1,0:T(8,128)(2,1)S(1)}, u32[]{:S(2)}) copy-start(bf16[768,512]{1,0:T(8,128)(2,1)S(1)} %get-tuple-element.59.hid_ref) | copy-start | bytes 2359300
  72.6 3.6 %collective-permute-start.1 = (bf16[1536,512]{1,0:T(8,128)(2,1)S(1)}, bf16[1536,512]{1,0:T(8,128)(2,1)S(1)}, u32[]{:S(2)}, u32[]{:S(2)}) collective-permute-start(bf16[1536,512]{1,0:T(8,128)(2,1)S(1)} %get-tuple-element.56), channel_id=1, source_target_pairs={{0,1},{1,0},{2,3},{3,2},{4,5},{5,4},{6,7},{7,6},{8,9},{9,8},{10,11... | collective-permute-start | bytes 4718600 | tf_op jit(solution)/shard_map/ppermute | solution.py:617
  73.1 12.0 %collective-permute-start.2 = (bf16[192,1024]{1,0:T(8,128)(2,1)S(1)}, bf16[192,1024]{1,0:T(8,128)(2,1)S(1)}, u32[]{:S(2)}, u32[]{:S(2)}) collective-permute-start(bf16[192,1024]{1,0:T(8,128)(2,1)S(1)} %early.1.g0), channel_id=1, source_target_pairs={{0,64},{32,96},{64,0},{96,32},{1,65},{33,97},{65,1},{97,33},{2,66}... | collective-permute-start | bytes 1179656 | tf_op jit(solution)/shard_map/ppermute | solution.py:621
  85.1 27.6 %all-to-all-start.1 = ((bf16[64,24,512]{2,1,0:T(8,128)(2,1)}), bf16[64,24,512]{2,1,0:T(8,128)(2,1)S(1)}, u32[]{:S(2)}, u32[]{:S(2)}) async-start(bf16[64,24,512]{2,1,0:T(8,128)(2,1)} %bitcast.11), calls=%async_computation.1 | async-start | bytes 3145728 | tf_op jit(solution)/shard_map/all_to_all | solution.py:647
  89.9 29.9 %collective-permute-start.10 = (bf16[192,1024]{1,0:T(8,128)(2,1)S(1)}, bf16[192,1024]{1,0:T(8,128)(2,1)S(1)}, u32[]{:S(2)}, u32[]{:S(2)}) collective-permute-start(bf16[192,1024]{1,0:T(8,128)(2,1)S(1)} %early.1.g0), channel_id=1, source_target_pairs={{0,32},{32,64},{64,96},{96,0},{1,33},{33,65},{65,97},{97,1},{2,34}... | collective-permute-start | bytes 1179656 | tf_op jit(solution)/shard_map/ppermute | solution.py:621
  107.1 20.1 %collective-permute-start.11 = (bf16[192,1024]{1,0:T(8,128)(2,1)S(1)}, bf16[192,1024]{1,0:T(8,128)(2,1)S(1)}, u32[]{:S(2)}, u32[]{:S(2)}) collective-permute-start(bf16[192,1024]{1,0:T(8,128)(2,1)S(1)} %early.1.g0), channel_id=1, source_target_pairs={{0,96},{32,0},{64,32},{96,64},{1,97},{33,1},{65,33},{97,65},{2,98}... | collective-permute-start | bytes 1179656 | tf_op jit(solution)/shard_map/ppermute | solution.py:621
  115.4 11.8 %collective-permute-start.3 = (bf16[192,1024]{1,0:T(8,128)(2,1)S(1)}, bf16[192,1024]{1,0:T(8,128)(2,1)S(1)}, u32[]{:S(2)}, u32[]{:S(2)}) collective-permute-start(bf16[192,1024]{1,0:T(8,128)(2,1)S(1)} %get-tuple-element.71.own_ref), channel_id=1, source_target_pairs={{0,1},{1,0},{2,3},{3,2},{4,5},{5,4},{6,7},{7,6},{8,9},{9,8},{10,11... | collective-permute-start | bytes 1179656 | tf_op jit(solution)/shard_map/ppermute | solution.py:617
  118.1 7.6 %collective-permute-start.4 = (bf16[192,256]{1,0:T(8,128)(2,1)S(1)}, bf16[192,256]{1,0:T(8,128)(2,1)S(1)}, u32[]{:S(2)}, u32[]{:S(2)}) collective-permute-start(bf16[192,256]{1,0:T(8,128)(2,1)S(1)} %get-tuple-element.72), channel_id=1, source_target_pairs={{0,32},{32,64},{64,96},{96,0},{1,33},{33,65},{65,97},{97,1},{2,34}... | collective-permute-start | bytes 294920 | tf_op jit(solution)/shard_map/ppermute | solution.py:621
  118.2 8.4 %collective-permute-start.6 = (bf16[192,256]{1,0:T(8,128)(2,1)S(1)}, bf16[192,256]{1,0:T(8,128)(2,1)S(1)}, u32[]{:S(2)}, u32[]{:S(2)}) collective-permute-start(bf16[192,256]{1,0:T(8,128)(2,1)S(1)} %get-tuple-element.73), channel_id=1, source_target_pairs={{0,64},{32,96},{64,0},{96,32},{1,65},{33,97},{65,1},{97,33},{2,66}... | collective-permute-start | bytes 294920 | tf_op jit(solution)/shard_map/ppermute | solution.py:621
  119.8 6.8 %collective-permute-start.8 = (bf16[192,256]{1,0:T(8,128)(2,1)S(1)}, bf16[192,256]{1,0:T(8,128)(2,1)S(1)}, u32[]{:S(2)}, u32[]{:S(2)}) collective-permute-start(bf16[192,256]{1,0:T(8,128)(2,1)S(1)} %get-tuple-element.74), channel_id=1, source_target_pairs={{0,96},{32,0},{64,32},{96,64},{1,97},{33,1},{65,33},{97,65},{2,98}... | collective-permute-start | bytes 294920 | tf_op jit(solution)/shard_map/ppermute | solution.py:621
  125.7 8.2 %collective-permute-start.5 = (bf16[192,256]{1,0:T(8,128)(2,1)S(1)}, bf16[192,256]{1,0:T(8,128)(2,1)S(1)}, u32[]{:S(2)}, u32[]{:S(2)}) collective-permute-start(bf16[192,256]{1,0:T(8,128)(2,1)S(1)} %collective-permute-done.4.b1), channel_id=1, source_target_pairs={{0,1},{1,0},{2,3},{3,2},{4,5},{5,4},{6,7},{7,6},{8,9},{9,8},{10,11... | collective-permute-start | bytes 294920 | tf_op jit(solution)/shard_map/ppermute | solution.py:617
  126.6 7.3 %collective-permute-start.7 = (bf16[192,256]{1,0:T(8,128)(2,1)S(1)}, bf16[192,256]{1,0:T(8,128)(2,1)S(1)}, u32[]{:S(2)}, u32[]{:S(2)}) collective-permute-start(bf16[192,256]{1,0:T(8,128)(2,1)S(1)} %collective-permute-done.6.b2), channel_id=1, source_target_pairs={{0,1},{1,0},{2,3},{3,2},{4,5},{5,4},{6,7},{7,6},{8,9},{9,8},{10,11... | collective-permute-start | bytes 294920 | tf_op jit(solution)/shard_map/ppermute | solution.py:617
  126.6 7.3 %collective-permute-start.9 = (bf16[192,256]{1,0:T(8,128)(2,1)S(1)}, bf16[192,256]{1,0:T(8,128)(2,1)S(1)}, u32[]{:S(2)}, u32[]{:S(2)}) collective-permute-start(bf16[192,256]{1,0:T(8,128)(2,1)S(1)} %collective-permute-done.8.b3), channel_id=1, source_target_pairs={{0,1},{1,0},{2,3},{3,2},{4,5},{5,4},{6,7},{7,6},{8,9},{9,8},{10,11... | collective-permute-start | bytes 294920 | tf_op jit(solution)/shard_map/ppermute | solution.py:617
  133.1 3.1 %copy-start.10 = (f32[192,1024]{1,0:T(8,128)}, f32[192,1024]{1,0:T(8,128)S(1)}, u32[]{:S(2)}) copy-start(f32[192,1024]{1,0:T(8,128)S(1)} %get-tuple-element.89.local_ref) | copy-start | bytes 2359300
  136.2 34.8 %copy-start.1 = (f32[192,1024]{1,0:T(8,128)S(1)}, f32[192,1024]{1,0:T(8,128)}, u32[]{:S(2)}) copy-start(f32[192,1024]{1,0:T(8,128)} %get-tuple-element.78.rate_hbm.rate_ref) | copy-start | bytes 2359300
  136.2 34.8 %copy-start.2 = (f32[192,1024]{1,0:T(8,128)S(1)}, f32[192,1024]{1,0:T(8,128)}, u32[]{:S(2)}) copy-start(f32[192,1024]{1,0:T(8,128)} %get-tuple-element.79.after_hbm.suffix_ref) | copy-start | bytes 2359300
  136.2 34.8 %copy-start.4 = (bf16[192,1024]{1,0:T(8,128)(2,1)S(1)}, bf16[192,1024]{1,0:T(8,128)(2,1)}, u32[]{:S(2)}) copy-start(bf16[192,1024]{1,0:T(8,128)(2,1)} %lru_ref.5) | copy-start | bytes 1179652
  136.2 24.2 %all-to-all-start.2 = ((bf16[16,32,1152]{2,1,0:T(8,128)(2,1)}), bf16[16,32,1152]{2,1,0:T(8,128)(2,1)S(1)}, u32[]{:S(2)}, u32[]{:S(2)}) async-start(bf16[16,32,1152]{2,1,0:T(8,128)(2,1)} %bitcast.16), calls=%async_computation.2 | async-start | bytes 2359296 | tf_op jit(solution)/shard_map/all_to_all | solution.py:664
  140.1 25.6 %collective-permute-start.15 = (bf16[1,1024]{1,0:T(2,128)(2,1)S(1)}, bf16[1,1024]{1,0:T(2,128)(2,1)S(1)}, u32[]{:S(2)}, u32[]{:S(2)}) collective-permute-start(bf16[1,1024]{1,0:T(2,128)(2,1)S(1)} %slice.6), channel_id=1, source_target_pairs={{0,2},{2,4},{4,6},{6,8},{8,10},{10,12},{12,14},{14,16},{16,18},{18... | collective-permute-start | bytes 6152 | tf_op jit(solution)/shard_map/ppermute | solution.py:650
  160.4 10.6 %copy-start.11 = (f32[192,1024]{1,0:T(8,128)S(1)}, f32[192,1024]{1,0:T(8,128)}, u32[]{:S(2)}) copy-start(f32[192,1024]{1,0:T(8,128)} %copy-done.10) | copy-start | bytes 2359300
  161.0 4.7 %collective-permute-start.12 = (f32[16,128]{1,0:T(8,128)S(1)}, f32[16,128]{1,0:T(8,128)S(1)}, u32[]{:S(2)}, u32[]{:S(2)}) collective-permute-start(f32[16,128]{1,0:T(8,128)S(1)} %get-tuple-element.88), channel_id=1, source_target_pairs={{32,0},{64,32},{96,64},{33,1},{65,33},{97,65},{34,2},{66,34},{98,6... | collective-permute-start | bytes 24584 | tf_op jit(solution)/shard_map/ppermute | solution.py:666
  162.3 5.9 %collective-permute-start.13 = (f32[16,128]{1,0:T(8,128)S(1)}, f32[16,128]{1,0:T(8,128)S(1)}, u32[]{:S(2)}, u32[]{:S(2)}) collective-permute-start(f32[16,128]{1,0:T(8,128)S(1)} %get-tuple-element.88), channel_id=1, source_target_pairs={{64,0},{96,32},{65,1},{97,33},{66,2},{98,34},{67,3},{99,35},{68,4}... | collective-permute-start | bytes 24584 | tf_op jit(solution)/shard_map/ppermute | solution.py:666
  163.6 7.4 %collective-permute-start.14 = (f32[16,128]{1,0:T(8,128)S(1)}, f32[16,128]{1,0:T(8,128)S(1)}, u32[]{:S(2)}, u32[]{:S(2)}) collective-permute-start(f32[16,128]{1,0:T(8,128)S(1)} %get-tuple-element.88), channel_id=1, source_target_pairs={{96,0},{97,1},{98,2},{99,3},{100,4},{101,5},{102,6},{103,7},{104,8... | collective-permute-start | bytes 24584 | tf_op jit(solution)/shard_map/ppermute | solution.py:666

commit v5 on v4

--- a/solution.py
+++ b/solution.py
@@ -183,13 +183,13 @@
         cs[g * 96 : (g + 1) * 96, :] = moved[96:]
 
 
-def projections(par, xs, cs, wg_ref, wu_ref, wd_ref):
+def projections(par, xs, cs, wg_ref, wu_ref, wd_ref, units=slice(None)):
     gate = up = back = 0.0
     for j in range(4):
         mine, part = slice(j * BLK, (j + 1) * BLK), lanes(2 * j + par)
-        gate += dot(xs[:, mine], wg_ref[part, :])
-        up += dot(xs[:, mine], wu_ref[part, :])
-        back += dot_cols(cs[:, mine], wd_ref[:, part])
+        gate += dot(xs[:, mine], wg_ref[part, units])
+        up += dot(xs[:, mine], wu_ref[part, units])
+        back += dot_cols(cs[:, mine], wd_ref[units, part])
     return gate, up, back
 
 
@@ -232,15 +232,17 @@
 ):
     par = 1 - meta[0]
     compact(perm_ref[...], peer_ref, xs, cs)
-    gate, up, back = projections(par, xs, cs, wg_ref, wu_ref, wd_ref)
-    gate += pg_ref[...]
-    up += pu_ref[...]
-    back += pb_ref[...]
-    sig = jax.nn.sigmoid(gate)
-    act = gate * sig
-    hid_ref[...] = (act * up).astype(BF)
-    gg_ref[...] = (back * up * sig * (1.0 + gate * (1.0 - sig))).astype(BF)
-    gu_ref[...] = (back * act).astype(BF)
+    for half in range(2):
+        units = slice(half * BLK, (half + 1) * BLK)
+        gate, up, back = projections(par, xs, cs, wg_ref, wu_ref, wd_ref, units)
+        gate += pg_ref[:, units]
+        up += pu_ref[:, units]
+        back += pb_ref[:, units]
+        sig = jax.nn.sigmoid(gate)
+        act = gate * sig
+        hid_ref[:, units] = (act * up).astype(BF)
+        gg_ref[:, units] = (back * up * sig * (1.0 + gate * (1.0 - sig))).astype(BF)
+        gu_ref[:, units] = (back * act).astype(BF)
     returned(par, perm_t_ref[...], gg_ref, gu_ref, wg_ref, wu_ref, ys, part_ref)
 
 
@@ -369,7 +371,8 @@
     copies = fetch(
         [(ids_hbm, ids)]
         + [(d_hbm.at[:, lanes(2 * j + tp)], own.at[:, j * BLK : (j + 1) * BLK]) for j in range(4)]
-        + [(w_hbm.at[:, lanes(2 * j + tp)], w_ref.at[j, :, :]) for j in range(4)],
+        + [(w_hbm.at[:, lanes(2 * j + tp)], w_ref.at[j, :, :]) for j in range(4)]
+        + [(w_hbm.at[:, lanes(2 * j + 1 - tp)], w_ref.at[4 + j, :, :]) for j in range(4)],
         sems,
     )
     copies[0].wait()
@@ -401,11 +404,11 @@
         out_specs=[pl.BlockSpec(memory_space=pltpu.VMEM)] * 6,
         out_shape=[jax.ShapeDtypeStruct((TOK, HALF), BF)]
         + [jax.ShapeDtypeStruct((TOK, BLK), BF)] * 4
-        + [jax.ShapeDtypeStruct((4, HALF, BLK), BF)],
+        + [jax.ShapeDtypeStruct((8, HALF, BLK), BF)],
         scratch_shapes=[
             pltpu.VMEM((2, TOK), jnp.int32),
             pltpu.VMEM((TOK, HALF), BF),
-            pltpu.SemaphoreType.DMA((9,)),
+            pltpu.SemaphoreType.DMA((13,)),
         ],
         compiler_params=vm(12),
         cost_estimate=cost(1e9),
@@ -451,31 +454,27 @@
 
 
 def drive_kernel(
-    meta, own_ref, peer_ref, w_ref, w_hbm, value_hbm, slope_hbm, rate_hbm, after_hbm, g0, g1, g2, g3,
-    dgate_ref, local_ref, head_ref, moved_ref, w, value, slope, rate, after, sems,
+    meta, own_ref, peer_ref, w_ref, value_hbm, slope_hbm, rate_hbm, after_hbm, g0, g1, g2, g3,
+    dgate_ref, local_ref, head_ref, moved_ref, value, slope, rate, after, sems,
 ):
-    tp = meta[0]
     copies = fetch(
-        [(w_hbm.at[:, lanes(2 * j + 1 - tp)], w.at[j, :, :]) for j in range(4)]
-        + [
+        [
             (value_hbm, value),
             (rate_hbm, rate),
             (after_hbm.at[0:8, :], after),
             (slope_hbm, slope),
-        ],
+        ]
+        + [(g, moved_ref.at[k, :, :]) for k, g in enumerate((g0, g1, g2, g3))],
         sems,
     )
     grad = 0.0
-    for j in range(4):
-        grad += dot_cols(own_ref[:, j * BLK : (j + 1) * BLK], w_ref[j, :, :])
-    for j in range(4):
-        copies[j].wait()
-        grad += dot_cols(peer_ref[:, j * BLK : (j + 1) * BLK], w[j, :, :])
-    copies[4].wait()
+    for k in range(8):
+        ref, j = (own_ref, peer_ref)[k // 4], k % 4
+        grad += dot_cols(ref[:, j * BLK : (j + 1) * BLK], w_ref[k, :, :])
+    copies[0].wait()
     local_ref[...] = grad * value[...]
-    for copy in copies[5:]:
+    for copy in copies[1:4]:
         copy.wait()
-    late = fetch([(g, moved_ref.at[k, :, :]) for k, g in enumerate((g0, g1, g2, g3))], sems.at[8:12])
     dgate_ref[...] = (grad * slope[...]).astype(BF)
 
     def visit(rows, here, later):
@@ -483,16 +482,16 @@
 
     head_ref[0:8, :] = tile_of(scan_rows(local_ref, rate, jnp.zeros((1, HALF), F32), visit))
     head_ref[8:16, :] = tile_of(after[0:1, :] * rate[0:1, :])
-    for copy in late:
+    for copy in copies[4:]:
         copy.wait()
 
 
-def drive(meta, own, peer, w, w_out, value, slope, rate, after, gated):
+def drive(meta, own, peer, w, value, slope, rate, after, gated):
     wide = pltpu.VMEM((TOK, HALF), F32)
     return pl.pallas_call(
         drive_kernel,
         name="drive",
-        in_specs=mixed("vvvhhhhhaaaa"),
+        in_specs=mixed("vvvhhhhaaaa"),
         out_specs=[pl.BlockSpec(memory_space=pltpu.VMEM)] * 4,
         out_shape=[
             jax.ShapeDtypeStruct((TOK, HALF), BF),
@@ -500,11 +499,10 @@
             jax.ShapeDtypeStruct((16, 128), F32),
             jax.ShapeDtypeStruct((4, TOK, HALF), BF),
         ],
-        scratch_shapes=[pltpu.VMEM((4, HALF, BLK), BF), wide, wide, wide]
-        + [pltpu.VMEM((8, HALF), F32), pltpu.SemaphoreType.DMA((12,))],
+        scratch_shapes=[wide, wide, wide, pltpu.VMEM((8, HALF), F32), pltpu.SemaphoreType.DMA((8,))],
         compiler_params=vm(12),
         cost_estimate=cost(2e9),
-    )(meta, own, peer, w, *in_hbm(w_out, value, slope, rate, after), *gated)
+    )(meta, own, peer, w, *in_hbm(value, slope, rate, after), *gated)
 
 
 def link_kernel(meta, shares_ref, within_ref, after_ref, plane_ref):
@@ -657,7 +655,7 @@
     dm_peer = swapped(dm)
     own = (blocks[0], *(turned(blocks[k], k) for k in (1, 2, 3)))
     d_gate, local, head, moved = drive(
-        meta, dm, dm_peer, w, w_out, value, slope, rate, suffix, (gated, turn1, turn2, turn3)
+        meta, dm, dm_peer, w, value, slope, rate, suffix, (gated, turn1, turn2, turn3)
     )
     peer = (dm_peer, *(swapped(own[k]) for k in (1, 2, 3)))
     share = outer(meta, peer, moved, outer_own(own, moved), head)

time: 174 us -> 173 us (level)
  transfers between devices with their start and end apart: 18 -> 18, of which waited for: 7 -> 7; matrix products, arithmetic and copies ran while one was open for 0% -> 0% of each run, Pallas kernels for 20% -> 19%
where the time goes in v5:
time: 173 us; the launch traced here: 171 us
  blocking collectives  52.2 us (30%)
  Pallas kernels  48.5 us (28%)
  waiting for transfers between devices  40.2 us (23%)
  starting transfers between devices  28.5 us (16%)
    all_to_all x1, blocking collectives, on_device(): got = lax.all_to_all(sent.reshape(NSP, CHUNK, HALF), SP, 0, 0, tiled=True)  52.2 us
    all_to_all x1, waiting for transfers between devices, on_device(): lax.all_to_all(share.reshape(16, 32, HALF + 128), ('y', 'x'), 0, 0, tiled...  17.7 us
    pallas_call x1, Pallas kernels, weight_grads(): pl.pallas_call(weight_kernel, name='weight_grads', grid_spec=pltpu.Prefet...  15.9 us
    ppermute x6, waiting for transfers between devices, turned(): return lax.ppermute(value, 'z', [(s, (s + steps) % 4) for s in range(4)])  12.5 us
    ppermute x6, starting transfers between devices, swapped(): return lax.ppermute(value, 'tp', [(0, 1), (1, 0)])  6.8 us
    pallas_call x1, Pallas kernels, expert_peer(): pl.pallas_call(peer_kernel, name='expert_peer', in_specs=whole(9), out_sp...  6.58 us
    ppermute x6, starting transfers between devices, turned(): return lax.ppermute(value, 'z', [(s, (s + steps) % 4) for s in range(4)])  6.06 us
    ppermute x3, waiting for transfers between devices, on_device(): lax.ppermute(plane, 'z', [(s, s - k) for s in range(k, 4)])  5.29 us
  transfers between devices with their start and end apart: 18, of which 7 were waited for; matrix products, arithmetic and copies ran while one was open for 0% of the time, Pallas kernels for 19%

profile of v5, /device:TPU:1, one launch (start us, length us, event | category | flops | bytes accessed | tf_op | source)
XLA Modules:
  0.0 171.5 jit_solution(16809138853233915802)
XLA Ops:
  0.6 0.1 pad_add_fusion.meta
  0.7 5.1 %pack.1 = bf16[1536,1024]{1,0:T(8,128)(2,1)S(1)} custom-call(s32[4]{0:T(128)S(1)} %pad_add_fusion.meta, s32[2,192]{1,0:T(2,128)} %bitcast.30, f32[2,192]{1,0:T(2,128)} %bitcast.32, bf16[192,2048]{1,0:T(8,128)(2,1)} %x_hbm.1, bf16[192,2048]{1,0:T(8,128)(2,1)} %d_hbm.3), custom_call_target="tpu_custom_call" | custom-call | tf_op jit(solution)/shard_map/pack/pallas_call | solution.py:139
  5.9 0.0 copy-start.3
  5.9 0.0 copy-start.5
  5.9 0.0 copy-start.7
  5.9 0.0 copy-start.8
  5.9 0.0 copy-start.9
  5.9 0.0 copy-start.12
  5.9 52.2 %all_to_all.15 = bf16[64,24,1024]{2,1,0:T(8,128)(2,1)S(1)} all-to-all(bf16[64,24,1024]{2,1,0:T(8,128)(2,1)S(1)} %bitcast.17), channel_id=1, replica_groups=mesh['z'=4,'y'=4,'x'=4,'tp'=2] {'z','y','x'}, dimensions={0} | all-to-all | bytes 6291456 | tf_op jit(solution)/shard_map/all_to_all | solution.py:633
  58.2 2.1 %collective-permute-start = (bf16[1536,1024]{1,0:T(8,128)(2,1)S(1)}, bf16[1536,1024]{1,0:T(8,128)(2,1)S(1)}, u32[]{:S(2)}, u32[]{:S(2)}) collective-permute-start(bf16[1536,1024]{1,0:T(8,128)(2,1)S(1)} %bitcast.19), channel_id=1, source_target_pairs={{0,1},{1,0},{2,3},{3,2},{4,5},{5,4},{6,7},{7,6},{8,9},{9,8},{10,11... | collective-permute-start | bytes 9437192 | tf_op jit(solution)/shard_map/ppermute | solution.py:615
  60.3 0.3 early.1.g0
  60.6 0.0 copy-start.13
  60.7 4.0 %expert_own.1 = (f32[768,512]{1,0:T(8,128)S(1)}, f32[768,512]{1,0:T(8,128)S(1)}, f32[768,512]{1,0:T(8,128)S(1)}) custom-call(s32[4]{0:T(128)S(1)} %pad_add_fusion.meta, bf16[192,192]{1,0:T(8,128)(2,1)S(1)} %copy-done.12, bf16[1536,1024]{1,0:T(8,128)(2,1)S(1)} %bitcast.20, bf16[2048,512]{1,0:T(8,128)(2,1)S(1)} %bitcast.24, bf16[2048,512]{1,0:T(8,128)(2,1)S(1)} %bitcast.27, ...), custom_call_target="tpu_custom_call" | custom-call | flops 4000000000 | tf_op jit(solution)/shard_map/expert_own/pallas_call | solution.py:217
  64.7 0.9 collective-permute-done.peer_ref
  65.6 6.6 %expert_peer.1 = (bf16[768,512]{1,0:T(8,128)(2,1)S(1)}, bf16[768,512]{1,0:T(8,128)(2,1)S(1)}, bf16[768,512]{1,0:T(8,128)(2,1)S(1)}, bf16[1536,512]{1,0:T(8,128)(2,1)S(1)}) custom-call(s32[4]{0:T(128)S(1)} %pad_add_fusion.meta, bf16[192,192]{1,0:T(8,128)(2,1)S(1)} %copy-done.12, bf16[192,192]{1,0:T(8,128)(2,1)S(1)} %copy-done.13, ...), custom_call_target="tpu_custom_call" | custom-call | flops 6000000000 | tf_op jit(solution)/shard_map/expert_peer/pallas_call | solution.py:250
  72.2 0.0 copy-start.14
  72.2 0.4 collective-permute-start.1
  72.6 0.4 collective-permute-start.2
  73.0 2.8 %expert_back.1.a_ref = bf16[1536,512]{1,0:T(8,128)(2,1)S(1)} custom-call(s32[4]{0:T(128)S(1)} %pad_add_fusion.meta, bf16[192,192]{1,0:T(8,128)(2,1)S(1)} %copy-done.13, bf16[768,512]{1,0:T(8,128)(2,1)S(1)} %get-tuple-element.54.gg_ref, bf16[768,512]{1,0:T(8,128)(2,1)S(1)} %get-tuple-element.55.gu_ref, bf16[2048,512]{1,0:T(8,128)(2,1)S(1)} %bitcast.26, ...), custom_call_target="tpu_custom_call" | custom-call | flops 3000000000 | tf_op jit(solution)/shard_map/expert_back/pallas_call | solution.py:268
  75.8 1.3 part_sum.1
  77.1 7.5 %collective-permute-done.2.g2 = bf16[192,1024]{1,0:T(8,128)(2,1)S(1)} collective-permute-done((bf16[192,1024]{1,0:T(8,128)(2,1)S(1)}, bf16[192,1024]{1,0:T(8,128)(2,1)S(1)}, u32[]{:S(2)}, u32[]{:S(2)}) %collective-permute-start.2) | collective-permute-done | bytes 393248 | tf_op jit(solution)/shard_map/ppermute | solution.py:619
  84.7 4.8 %all-to-all-start.1 = ((bf16[64,24,512]{2,1,0:T(8,128)(2,1)}), bf16[64,24,512]{2,1,0:T(8,128)(2,1)S(1)}, u32[]{:S(2)}, u32[]{:S(2)}) async-start(bf16[64,24,512]{2,1,0:T(8,128)(2,1)} %bitcast.11), calls=%async_computation.1 | async-start | bytes 3145728 | tf_op jit(solution)/shard_map/all_to_all | solution.py:645
  89.5 1.3 collective-permute-start.10
  90.8 15.9 %weight_grads.1 = (f32[2048,512]{1,0:T(8,128)}, f32[2048,512]{1,0:T(8,128)}, f32[512,2048]{1,0:T(8,128)}, f32[192,1024]{1,0:T(8,128)}, f32[192,1024]{1,0:T(8,128...) custom-call(s32[4]{0:T(128)S(1)} %pad_add_fusion.meta, bf16[192,192]{1,0:T(8,128)(2,1)} %constant.25.clone.perm_ref, ...), custom_call_target="tpu_custom_call" | custom-call | flops 4831838208 | bytes 20000000 | tf_op jit(solution)/shard_map/weight_grads/pallas_call | solution.py:330
  106.7 1.7 %collective-permute-start.11 = (bf16[192,1024]{1,0:T(8,128)(2,1)S(1)}, bf16[192,1024]{1,0:T(8,128)(2,1)S(1)}, u32[]{:S(2)}, u32[]{:S(2)}) collective-permute-start(bf16[192,1024]{1,0:T(8,128)(2,1)S(1)} %early.1.g0), channel_id=1, source_target_pairs={{0,96},{32,0},{64,32},{96,64},{1,97},{33,1},{65,33},{97,65},{2,98}... | collective-permute-start | bytes 1179656 | tf_op jit(solution)/shard_map/ppermute | solution.py:619
  108.4 3.9 %all-to-all-done.1 = bf16[64,24,512]{2,1,0:T(8,128)(2,1)S(1)} async-done(((bf16[64,24,512]{2,1,0:T(8,128)(2,1)}), bf16[64,24,512]{2,1,0:T(8,128)(2,1)S(1)}, u32[]{:S(2)}, u32[]{:S(2)}) %all-to-all-start.1) | async-done | bytes 1572896 | tf_op jit(solution)/shard_map/all_to_all | solution.py:645
  112.3 3.1 %combine.1 = (bf16[192,1024]{1,0:T(8,128)(2,1)S(1)}, bf16[192,256]{1,0:T(8,128)(2,1)S(1)}, bf16[192,256]{1,0:T(8,128)(2,1)S(1)}, bf16[192,256]{1,0:T(8,128)(2,1)...) custom-call(s32[4]{0:T(128)S(1)} %pad_add_fusion.meta, s32[2,192]{1,0:T(2,128)} %bitcast.31, ...), custom_call_target="tpu_custom_call" | custom-call | flops 1000000000 | tf_op jit(solution)/shard_map/combine/pallas_call | solution.py:400
  115.3 2.7 %collective-permute-start.3 = (bf16[192,1024]{1,0:T(8,128)(2,1)S(1)}, bf16[192,1024]{1,0:T(8,128)(2,1)S(1)}, u32[]{:S(2)}, u32[]{:S(2)}) collective-permute-start(bf16[192,1024]{1,0:T(8,128)(2,1)S(1)} %get-tuple-element.71.own_ref), channel_id=1, source_target_pairs={{0,1},{1,0},{2,3},{3,2},{4,5},{5,4},{6,7},{7,6},{8,9},{9,8},{10,11... | collective-permute-start | bytes 1179656 | tf_op jit(solution)/shard_map/ppermute | solution.py:615
  118.0 0.1 collective-permute-start.4
  118.2 1.6 collective-permute-start.6
  119.7 1.0 collective-permute-start.8
  120.7 4.9 %collective-permute-done.4.b1 = bf16[192,256]{1,0:T(8,128)(2,1)S(1)} collective-permute-done((bf16[192,256]{1,0:T(8,128)(2,1)S(1)}, bf16[192,256]{1,0:T(8,128)(2,1)S(1)}, u32[]{:S(2)}, u32[]{:S(2)}) %collective-permute-start.4) | collective-permute-done | bytes 98336 | tf_op jit(solution)/shard_map/ppermute | solution.py:619
  125.6 0.9 collective-permute-start.5
  126.6 0.6 collective-permute-start.9
  127.2 4.6 %drive.1 = (bf16[192,1024]{1,0:T(8,128)(2,1)}, f32[192,1024]{1,0:T(8,128)S(1)}, f32[16,128]{1,0:T(8,128)S(1)}, bf16[4,192,1024]{2,1,0:T(8,128)(2,1)S(1)}) custom-call(s32[4]{0:T(128)S(1)} %pad_add_fusion.meta, bf16[192,1024]{1,0:T(8,128)(2,1)S(1)} %get-tuple-element.71.own_ref, bf16[192,1024]{1,0:T(8,128)(2,1)S(1)} %collective-permute-done.3.peer_ref.p0, ...), custom_call_target="tpu_custom_call" | custom-call | flops 2000000000 | tf_op jit(solution)/shard_map/drive/pallas_call | solution.py:491
  131.8 0.7 outer_own.1.own_ref
  132.5 2.3 %outer.1 = bf16[512,1152]{1,0:T(8,128)(2,1)} custom-call(s32[4]{0:T(128)S(1)} %pad_add_fusion.meta, bf16[192,1024]{1,0:T(8,128)(2,1)S(1)} %collective-permute-done.3.peer_ref.p0, bf16[192,256]{1,0:T(8,128)(2,1)S(1)} %collective-permute-done.5.p1, bf16[192,256]{1,0:T(8,128)(2,1)S(1)} %collective-permute-done.7.p2, ...), custom_call_target="tpu_custom_call" | custom-call | flops 1000000000 | tf_op jit(solution)/shard_map/outer/pallas_call | solution.py:603
  134.9 3.8 %all-to-all-start.2 = ((bf16[16,32,1152]{2,1,0:T(8,128)(2,1)}), bf16[16,32,1152]{2,1,0:T(8,128)(2,1)S(1)}, u32[]{:S(2)}, u32[]{:S(2)}) async-start(bf16[16,32,1152]{2,1,0:T(8,128)(2,1)} %bitcast.16), calls=%async_computation.2 | async-start | bytes 2359296 | tf_op jit(solution)/shard_map/all_to_all | solution.py:662
  138.7 3.1 %collective-permute-start.15 = (bf16[1,1024]{1,0:T(2,128)(2,1)S(1)}, bf16[1,1024]{1,0:T(2,128)(2,1)S(1)}, u32[]{:S(2)}, u32[]{:S(2)}) collective-permute-start(bf16[1,1024]{1,0:T(2,128)(2,1)S(1)} %slice.6), channel_id=1, source_target_pairs={{0,2},{2,4},{4,6},{6,8},{8,10},{10,12},{12,14},{14,16},{16,18},{18... | collective-permute-start | bytes 6152 | tf_op jit(solution)/shard_map/ppermute | solution.py:648
  141.9 17.7 %all-to-all-done.2.shares_ref = bf16[16,32,1152]{2,1,0:T(8,128)(2,1)S(1)} async-done(((bf16[16,32,1152]{2,1,0:T(8,128)(2,1)}), bf16[16,32,1152]{2,1,0:T(8,128)(2,1)S(1)}, u32[]{:S(2)}, u32[]{:S(2)}) %all-to-all-start.2) | async-done | bytes 1179680 | tf_op jit(solution)/shard_map/all_to_all | solution.py:662
  159.6 0.6 link.1
  160.1 1.3 collective-permute-start.12
  161.4 1.3 collective-permute-start.13
  162.7 1.3 collective-permute-start.14
  164.0 0.8 convert_reduce_fusion
  164.9 2.5 %collective-permute-done.13.p2 = f32[16,128]{1,0:T(8,128)S(1)} collective-permute-done((f32[16,128]{1,0:T(8,128)S(1)}, f32[16,128]{1,0:T(8,128)S(1)}, u32[]{:S(2)}, u32[]{:S(2)}) %collective-permute-start.13) | collective-permute-done | bytes 8224 | tf_op jit(solution)/shard_map/ppermute | solution.py:664
  167.3 2.8 %collective-permute-done.14.p3 = f32[16,128]{1,0:T(8,128)S(1)} collective-permute-done((f32[16,128]{1,0:T(8,128)S(1)}, f32[16,128]{1,0:T(8,128)S(1)}, u32[]{:S(2)}, u32[]{:S(2)}) %collective-permute-start.14) | collective-permute-done | bytes 8224 | tf_op jit(solution)/shard_map/ppermute | solution.py:664
  170.2 1.3 finish.1
  (39 shorter events, 0.1 us)
Async XLA Ops:
  5.9 54.4 %copy-start.3 = (bf16[192,1024]{1,0:T(8,128)(2,1)S(1)}, bf16[192,1024]{1,0:T(8,128)(2,1)}, u32[]{:S(2)}) copy-start(bf16[192,1024]{1,0:T(8,128)(2,1)} %lru_ref.5) | copy-start | bytes 1179652
  5.9 54.4 %copy-start.5 = (bf16[192,1024]{1,0:T(8,128)(2,1)S(1)}, bf16[192,1024]{1,0:T(8,128)(2,1)}, u32[]{:S(2)}) copy-start(bf16[192,1024]{1,0:T(8,128)(2,1)} %gate_ref.3) | copy-start | bytes 1179652
  5.9 54.7 %copy-start.7 = (bf16[1,512,2048]{2,1,0:T(8,128)(2,1)S(1)}, bf16[1,512,2048]{2,1,0:T(8,128)(2,1)}, u32[]{:S(2)}) copy-start(bf16[1,512,2048]{2,1,0:T(8,128)(2,1)} %param.23) | copy-start | bytes 6291460
  5.9 54.7 %copy-start.8 = (bf16[1,2048,512]{2,1,0:T(8,128)(2,1)S(1)}, bf16[1,2048,512]{2,1,0:T(8,128)(2,1)}, u32[]{:S(2)}) copy-start(bf16[1,2048,512]{2,1,0:T(8,128)(2,1)} %param.21) | copy-start | bytes 6291460
  5.9 54.7 %copy-start.9 = (bf16[1,2048,512]{2,1,0:T(8,128)(2,1)S(1)}, bf16[1,2048,512]{2,1,0:T(8,128)(2,1)}, u32[]{:S(2)}) copy-start(bf16[1,2048,512]{2,1,0:T(8,128)(2,1)} %param.22) | copy-start | bytes 6291460
  5.9 54.7 %copy-start.12 = (bf16[192,192]{1,0:T(8,128)(2,1)S(1)}, bf16[192,192]{1,0:T(8,128)(2,1)}, u32[]{:S(2)}) copy-start(bf16[192,192]{1,0:T(8,128)(2,1)} %constant.25.clone.perm_ref) | copy-start | bytes 221188
  58.1 6.5 %copy-start = (bf16[64,24,1024]{2,1,0:T(8,128)(2,1)}, bf16[64,24,1024]{2,1,0:T(8,128)(2,1)S(1)}, u32[]{:S(2)}) copy-start(bf16[64,24,1024]{2,1,0:T(8,128)(2,1)S(1)} %all_to_all.15) | copy-start | bytes 9437188
  58.2 7.4 %collective-permute-start = (bf16[1536,1024]{1,0:T(8,128)(2,1)S(1)}, bf16[1536,1024]{1,0:T(8,128)(2,1)S(1)}, u32[]{:S(2)}, u32[]{:S(2)}) collective-permute-start(bf16[1536,1024]{1,0:T(8,128)(2,1)S(1)} %bitcast.19), channel_id=1, source_target_pairs={{0,1},{1,0},{2,3},{3,2},{4,5},{5,4},{6,7},{7,6},{8,9},{9,8},{10,11... | collective-permute-start | bytes 9437192 | tf_op jit(solution)/shard_map/ppermute | solution.py:615
  60.6 4.9 %copy-start.13 = (bf16[192,192]{1,0:T(8,128)(2,1)S(1)}, bf16[192,192]{1,0:T(8,128)(2,1)}, u32[]{:S(2)}) copy-start(bf16[192,192]{1,0:T(8,128)(2,1)} %constant.26.clone.perm_t_ref) | copy-start | bytes 221188
  65.6 6.6 %copy-start.6 = (bf16[1536,1024]{1,0:T(8,128)(2,1)}, bf16[1536,1024]{1,0:T(8,128)(2,1)S(1)}, u32[]{:S(2)}) copy-start(bf16[1536,1024]{1,0:T(8,128)(2,1)S(1)} %collective-permute-done.peer_ref) | copy-start | bytes 9437188
  72.2 3.6 %copy-start.14 = (bf16[768,512]{1,0:T(8,128)(2,1)}, bf16[768,512]{1,0:T(8,128)(2,1)S(1)}, u32[]{:S(2)}) copy-start(bf16[768,512]{1,0:T(8,128)(2,1)S(1)} %get-tuple-element.54.gg_ref) | copy-start | bytes 2359300
  72.2 3.6 %copy-start.15 = (bf16[768,512]{1,0:T(8,128)(2,1)}, bf16[768,512]{1,0:T(8,128)(2,1)S(1)}, u32[]{:S(2)}) copy-start(bf16[768,512]{1,0:T(8,128)(2,1)S(1)} %get-tuple-element.55.gu_ref) | copy-start | bytes 2359300
  72.2 3.6 %copy-start.16 = (bf16[768,512]{1,0:T(8,128)(2,1)}, bf16[768,512]{1,0:T(8,128)(2,1)S(1)}, u32[]{:S(2)}) copy-start(bf16[768,512]{1,0:T(8,128)(2,1)S(1)} %get-tuple-element.59.hid_ref) | copy-start | bytes 2359300
  72.2 3.6 %collective-permute-start.1 = (bf16[1536,512]{1,0:T(8,128)(2,1)S(1)}, bf16[1536,512]{1,0:T(8,128)(2,1)S(1)}, u32[]{:S(2)}, u32[]{:S(2)}) collective-permute-start(bf16[1536,512]{1,0:T(8,128)(2,1)S(1)} %get-tuple-element.56), channel_id=1, source_target_pairs={{0,1},{1,0},{2,3},{3,2},{4,5},{5,4},{6,7},{7,6},{8,9},{9,8},{10,11... | collective-permute-start | bytes 4718600 | tf_op jit(solution)/shard_map/ppermute | solution.py:615
  72.6 12.0 %collective-permute-start.2 = (bf16[192,1024]{1,0:T(8,128)(2,1)S(1)}, bf16[192,1024]{1,0:T(8,128)(2,1)S(1)}, u32[]{:S(2)}, u32[]{:S(2)}) collective-permute-start(bf16[192,1024]{1,0:T(8,128)(2,1)S(1)} %early.1.g0), channel_id=1, source_target_pairs={{0,64},{32,96},{64,0},{96,32},{1,65},{33,97},{65,1},{97,33},{2,66}... | collective-permute-start | bytes 1179656 | tf_op jit(solution)/shard_map/ppermute | solution.py:619
  84.7 27.6 %all-to-all-start.1 = ((bf16[64,24,512]{2,1,0:T(8,128)(2,1)}), bf16[64,24,512]{2,1,0:T(8,128)(2,1)S(1)}, u32[]{:S(2)}, u32[]{:S(2)}) async-start(bf16[64,24,512]{2,1,0:T(8,128)(2,1)} %bitcast.11), calls=%async_computation.1 | async-start | bytes 3145728 | tf_op jit(solution)/shard_map/all_to_all | solution.py:645
  89.5 30.2 %collective-permute-start.10 = (bf16[192,1024]{1,0:T(8,128)(2,1)S(1)}, bf16[192,1024]{1,0:T(8,128)(2,1)S(1)}, u32[]{:S(2)}, u32[]{:S(2)}) collective-permute-start(bf16[192,1024]{1,0:T(8,128)(2,1)S(1)} %early.1.g0), channel_id=1, source_target_pairs={{0,32},{32,64},{64,96},{96,0},{1,33},{33,65},{65,97},{97,1},{2,34}... | collective-permute-start | bytes 1179656 | tf_op jit(solution)/shard_map/ppermute | solution.py:619
  106.7 20.5 %collective-permute-start.11 = (bf16[192,1024]{1,0:T(8,128)(2,1)S(1)}, bf16[192,1024]{1,0:T(8,128)(2,1)S(1)}, u32[]{:S(2)}, u32[]{:S(2)}) collective-permute-start(bf16[192,1024]{1,0:T(8,128)(2,1)S(1)} %early.1.g0), channel_id=1, source_target_pairs={{0,96},{32,0},{64,32},{96,64},{1,97},{33,1},{65,33},{97,65},{2,98}... | collective-permute-start | bytes 1179656 | tf_op jit(solution)/shard_map/ppermute | solution.py:619
  115.3 11.8 %collective-permute-start.3 = (bf16[192,1024]{1,0:T(8,128)(2,1)S(1)}, bf16[192,1024]{1,0:T(8,128)(2,1)S(1)}, u32[]{:S(2)}, u32[]{:S(2)}) collective-permute-start(bf16[192,1024]{1,0:T(8,128)(2,1)S(1)} %get-tuple-element.71.own_ref), channel_id=1, source_target_pairs={{0,1},{1,0},{2,3},{3,2},{4,5},{5,4},{6,7},{7,6},{8,9},{9,8},{10,11... | collective-permute-start | bytes 1179656 | tf_op jit(solution)/shard_map/ppermute | solution.py:615
  118.0 7.6 %collective-permute-start.4 = (bf16[192,256]{1,0:T(8,128)(2,1)S(1)}, bf16[192,256]{1,0:T(8,128)(2,1)S(1)}, u32[]{:S(2)}, u32[]{:S(2)}) collective-permute-start(bf16[192,256]{1,0:T(8,128)(2,1)S(1)} %get-tuple-element.72), channel_id=1, source_target_pairs={{0,32},{32,64},{64,96},{96,0},{1,33},{33,65},{65,97},{97,1},{2,34}... | collective-permute-start | bytes 294920 | tf_op jit(solution)/shard_map/ppermute | solution.py:619
  118.2 8.4 %collective-permute-start.6 = (bf16[192,256]{1,0:T(8,128)(2,1)S(1)}, bf16[192,256]{1,0:T(8,128)(2,1)S(1)}, u32[]{:S(2)}, u32[]{:S(2)}) collective-permute-start(bf16[192,256]{1,0:T(8,128)(2,1)S(1)} %get-tuple-element.73), channel_id=1, source_target_pairs={{0,64},{32,96},{64,0},{96,32},{1,65},{33,97},{65,1},{97,33},{2,66}... | collective-permute-start | bytes 294920 | tf_op jit(solution)/shard_map/ppermute | solution.py:619
  119.7 6.8 %collective-permute-start.8 = (bf16[192,256]{1,0:T(8,128)(2,1)S(1)}, bf16[192,256]{1,0:T(8,128)(2,1)S(1)}, u32[]{:S(2)}, u32[]{:S(2)}) collective-permute-start(bf16[192,256]{1,0:T(8,128)(2,1)S(1)} %get-tuple-element.74), channel_id=1, source_target_pairs={{0,96},{32,0},{64,32},{96,64},{1,97},{33,1},{65,33},{97,65},{2,98}... | collective-permute-start | bytes 294920 | tf_op jit(solution)/shard_map/ppermute | solution.py:619
  125.6 6.9 %collective-permute-start.5 = (bf16[192,256]{1,0:T(8,128)(2,1)S(1)}, bf16[192,256]{1,0:T(8,128)(2,1)S(1)}, u32[]{:S(2)}, u32[]{:S(2)}) collective-permute-start(bf16[192,256]{1,0:T(8,128)(2,1)S(1)} %collective-permute-done.4.b1), channel_id=1, source_target_pairs={{0,1},{1,0},{2,3},{3,2},{4,5},{5,4},{6,7},{7,6},{8,9},{9,8},{10,11... | collective-permute-start | bytes 294920 | tf_op jit(solution)/shard_map/ppermute | solution.py:615
  126.6 6.0 %collective-permute-start.7 = (bf16[192,256]{1,0:T(8,128)(2,1)S(1)}, bf16[192,256]{1,0:T(8,128)(2,1)S(1)}, u32[]{:S(2)}, u32[]{:S(2)}) collective-permute-start(bf16[192,256]{1,0:T(8,128)(2,1)S(1)} %collective-permute-done.6.b2), channel_id=1, source_target_pairs={{0,1},{1,0},{2,3},{3,2},{4,5},{5,4},{6,7},{7,6},{8,9},{9,8},{10,11... | collective-permute-start | bytes 294920 | tf_op jit(solution)/shard_map/ppermute | solution.py:615
  126.6 6.0 %collective-permute-start.9 = (bf16[192,256]{1,0:T(8,128)(2,1)S(1)}, bf16[192,256]{1,0:T(8,128)(2,1)S(1)}, u32[]{:S(2)}, u32[]{:S(2)}) collective-permute-start(bf16[192,256]{1,0:T(8,128)(2,1)S(1)} %collective-permute-done.8.b3), channel_id=1, source_target_pairs={{0,1},{1,0},{2,3},{3,2},{4,5},{5,4},{6,7},{7,6},{8,9},{9,8},{10,11... | collective-permute-start | bytes 294920 | tf_op jit(solution)/shard_map/ppermute | solution.py:615
  131.8 3.1 %copy-start.10 = (f32[192,1024]{1,0:T(8,128)}, f32[192,1024]{1,0:T(8,128)S(1)}, u32[]{:S(2)}) copy-start(f32[192,1024]{1,0:T(8,128)S(1)} %get-tuple-element.89.local_ref) | copy-start | bytes 2359300
  134.9 35.3 %copy-start.1 = (f32[192,1024]{1,0:T(8,128)S(1)}, f32[192,1024]{1,0:T(8,128)}, u32[]{:S(2)}) copy-start(f32[192,1024]{1,0:T(8,128)} %get-tuple-element.78.rate_hbm.rate_ref) | copy-start | bytes 2359300
  134.9 35.3 %copy-start.2 = (f32[192,1024]{1,0:T(8,128)S(1)}, f32[192,1024]{1,0:T(8,128)}, u32[]{:S(2)}) copy-start(f32[192,1024]{1,0:T(8,128)} %get-tuple-element.79.after_hbm.suffix_ref) | copy-start | bytes 2359300
  134.9 35.3 %copy-start.4 = (bf16[192,1024]{1,0:T(8,128)(2,1)S(1)}, bf16[192,1024]{1,0:T(8,128)(2,1)}, u32[]{:S(2)}) copy-start(bf16[192,1024]{1,0:T(8,128)(2,1)} %lru_ref.5) | copy-start | bytes 1179652
  134.9 24.7 %all-to-all-start.2 = ((bf16[16,32,1152]{2,1,0:T(8,128)(2,1)}), bf16[16,32,1152]{2,1,0:T(8,128)(2,1)S(1)}, u32[]{:S(2)}, u32[]{:S(2)}) async-start(bf16[16,32,1152]{2,1,0:T(8,128)(2,1)} %bitcast.16), calls=%async_computation.2 | async-start | bytes 2359296 | tf_op jit(solution)/shard_map/all_to_all | solution.py:662
  138.7 26.1 %collective-permute-start.15 = (bf16[1,1024]{1,0:T(2,128)(2,1)S(1)}, bf16[1,1024]{1,0:T(2,128)(2,1)S(1)}, u32[]{:S(2)}, u32[]{:S(2)}) collective-permute-start(bf16[1,1024]{1,0:T(2,128)(2,1)S(1)} %slice.6), channel_id=1, source_target_pairs={{0,2},{2,4},{4,6},{6,8},{8,10},{10,12},{12,14},{14,16},{16,18},{18... | collective-permute-start | bytes 6152 | tf_op jit(solution)/shard_map/ppermute | solution.py:648
  159.6 10.6 %copy-start.11 = (f32[192,1024]{1,0:T(8,128)S(1)}, f32[192,1024]{1,0:T(8,128)}, u32[]{:S(2)}) copy-start(f32[192,1024]{1,0:T(8,128)} %copy-done.10) | copy-start | bytes 2359300
  160.1 4.7 %collective-permute-start.12 = (f32[16,128]{1,0:T(8,128)S(1)}, f32[16,128]{1,0:T(8,128)S(1)}, u32[]{:S(2)}, u32[]{:S(2)}) collective-permute-start(f32[16,128]{1,0:T(8,128)S(1)} %get-tuple-element.88), channel_id=1, source_target_pairs={{32,0},{64,32},{96,64},{33,1},{65,33},{97,65},{34,2},{66,34},{98,6... | collective-permute-start | bytes 24584 | tf_op jit(solution)/shard_map/ppermute | solution.py:664
  161.4 5.9 %collective-permute-start.13 = (f32[16,128]{1,0:T(8,128)S(1)}, f32[16,128]{1,0:T(8,128)S(1)}, u32[]{:S(2)}, u32[]{:S(2)}) collective-permute-start(f32[16,128]{1,0:T(8,128)S(1)} %get-tuple-element.88), channel_id=1, source_target_pairs={{64,0},{96,32},{65,1},{97,33},{66,2},{98,34},{67,3},{99,35},{68,4}... | collective-permute-start | bytes 24584 | tf_op jit(solution)/shard_map/ppermute | solution.py:664
  162.7 7.4 %collective-permute-start.14 = (f32[16,128]{1,0:T(8,128)S(1)}, f32[16,128]{1,0:T(8,128)S(1)}, u32[]{:S(2)}, u32[]{:S(2)}) collective-permute-start(f32[16,128]{1,0:T(8,128)S(1)} %get-tuple-element.88), channel_id=1, source_target_pairs={{96,0},{97,1},{98,2},{99,3},{100,4},{101,5},{102,6},{103,7},{104,8... | collective-permute-start | bytes 24584 | tf_op jit(solution)/shard_map/ppermute | solution.py:664
